TPU v7x, 256 devices: a whole 4x4x8 slice. The times are simulated.
256 devices in a mesh: ep: 64 (over z, y, core), tp: 4 (over x).
Axes of the slice: x: 4, y: 4, z: 8, core: 2. Of those that a mesh axis runs over, the one named last changes fastest.
Arguments:
- tokens: bfloat16 [2048, 2048], P('ep', 'tp'), may hold values from -33 to 33
- previous: bfloat16 [2048, 2048], P('ep', 'tp'), may hold values from -6 to 6
- first_norm_gain: float32 [2048], replicated, may hold values from 0.1 to 1.9
- token_shift_share: float32 [5, 2048], replicated, may hold values from 0 to 1
- receptance_weight: bfloat16 [2048, 1024], P(None, 'tp'), may hold values from -0.125 to 0.125
- key_weight: bfloat16 [2048, 1024], P(None, 'tp'), may hold values from -0.125 to 0.125
- value_weight: bfloat16 [2048, 1024], P(None, 'tp'), may hold values from -0.125 to 0.125
- decay_down_map: bfloat16 [2048, 128], replicated, may hold values from -0.125 to 0.125
- decay_up_map: bfloat16 [128, 1024], replicated, may hold values from -0.5 to 0.5
- decay_offset: float32 [1024], P('tp'), may hold values from -4 to 1
- strength_down_map: bfloat16 [2048, 128], replicated, may hold values from -0.125 to 0.125
- strength_up_map: bfloat16 [128, 1024], replicated, may hold values from -0.5 to 0.5
- removal_key_scale: float32 [1024], P('tp'), may hold values from 0.3 to 3
- key_damping: float32 [1024], P('tp'), may hold values from 0.1 to 1.9
- self_term_weight: float32 [16, 64], P('tp'), may hold values from -0.6 to 0.6
- head_norm_gain: float32 [1024], P('tp'), may hold values from 0.1 to 1.9
- output_weight: bfloat16 [1024, 2048], P('tp'), may hold values from -0.1875 to 0.1875
- state: float32 [2048, 16, 64, 64], P('ep', 'tp'), may hold values from -6 to 6
- second_norm_gain: float32 [2048], replicated, may hold values from 0.1 to 1.9
- routes: int32 [2048, 4], P('ep'), may hold values from 0 to 63, all different within a row; in each aligned block of 32 rows (0 to 31, 32 to 63, ...) at most 3 rows name the same one
- chosen_expert_weight: float32 [2048, 4], P('ep'), may hold values from 0.1 to 1
- expert_gate_weight: bfloat16 [64, 2048, 1024], P('ep', None, 'tp'), may hold values from -0.5 to 0.5
- expert_up_weight: bfloat16 [64, 2048, 1024], P('ep', None, 'tp'), may hold values from -0.5 to 0.5
- expert_down_weight: bfloat16 [64, 1024, 2048], P('ep', 'tp'), may hold values from -0.046875 to 0.046875
Outputs:
- layer_out: bfloat16 [2048, 2048], P('ep', 'tp')
- new_state: float32 [2048, 16, 64, 64], P('ep', 'tp')
Inputs may be any that keep to these rules, and one draw needn't show every extreme that they name: `routes`: each row names 4 different experts. Among the rows of one index of ep no expert is named by more than 3 rows, and in every draw some expert is named by exactly 3 rows of some index of ep.
All inputs are finite; a program needn't handle non-finite values.
Results may differ from a plain program's by a relative error of at most 0.015.
Values may be sent and summed in bfloat16 or wider, within the bound.
No kernel may reach another device: no remote copies, remote signals or barrier semaphores. Data moves between devices by JAX's collectives and lax.ppermute only.
A program may use at most 64 MiB of HBM per device.

v0:
```python
import jax
import jax.numpy as jnp
from jax import lax
from jax.sharding import PartitionSpec as P

NORM_EPS = 1e-06
GROUP_EPS = 0.00064
KEY_EPS = 1e-06
GATE_LIMIT = 7.0
GATE_SLOPE = 1.702


def in_one_piece(arrays, axis, dim, along):
    widths = [a.shape[along] for a in arrays]
    both = jnp.concatenate(arrays, axis=along)
    result = lax.all_gather(both, axis, axis=dim, tiled=True)
    return tuple(jnp.split(result, [sum(widths[:k]) for k in range(1, len(widths))], axis=along))


def sent_to_all(value, axis):
    devices = lax.axis_size(axis)
    return lax.all_to_all(
        jnp.broadcast_to(value[None], (devices, *value.shape)), axis, 0, 0, tiled=True
    )


def of_everyone(value, axis):
    return sent_to_all(value, axis).astype(jnp.float32).sum(axis=0)


def cut_along(value, dim, devices):
    shape = value.shape
    tiles = value.reshape(*shape[:dim], devices, shape[dim] // devices, *shape[dim + 1 :])
    return jnp.moveaxis(tiles, dim, 0)


def summed_on_arrival(value, axis, dim):
    tiles = cut_along(value, dim, lax.axis_size(axis))
    arrived = lax.all_to_all(tiles, axis, split_axis=0, concat_axis=0, tiled=True)
    return arrived.astype(jnp.float32).sum(axis=0)


def in_order(tiles, dim):
    tiles = jnp.moveaxis(tiles, 0, dim)
    shape = tiles.shape
    return tiles.reshape(*shape[:dim], shape[dim] * shape[dim + 1], *shape[dim + 2 :])


def gather_directly(value, axis, dim):
    tiles = sent_to_all(value, axis)
    return in_order(tiles, dim)


def row_rescale(values, gain):
    return values * lax.rsqrt(jnp.mean(values * values, axis=-1, keepdims=True) + NORM_EPS) * gain


def head_combiner(
    present_rows,
    prior_rows,
    first_norm_gain,
    token_shift_share,
    receptance_weight,
    key_weight,
    value_weight,
    decay_down_map,
    decay_up_map,
    decay_offset,
    strength_down_map,
    strength_up_map,
    removal_key_scale,
    key_damping,
    self_term_weight,
    head_norm_gain,
    state,
):
    sequence_count = present_rows.shape[0]
    head_number = state.shape[1]
    head_extent = state.shape[2]
    normed = row_rescale(present_rows.astype(jnp.float32), first_norm_gain)
    before = prior_rows.astype(jnp.float32)

    def shifted(role):
        return (normed + (before - normed) * token_shift_share[role]).astype(jnp.bfloat16)

    def project(inputs, weight):
        return jnp.dot(inputs, weight, preferred_element_type=jnp.float32)

    def by_heads(values):
        return values.reshape(sequence_count, head_number, head_extent)

    receptance_rows = by_heads(project(shifted(0), receptance_weight))
    key_rows = by_heads(project(shifted(1), key_weight))
    value_matrix = by_heads(project(shifted(2), value_weight))
    decay_low = jnp.tanh(project(shifted(3), decay_down_map)).astype(jnp.bfloat16)
    decay_pre = decay_offset + project(decay_low, decay_up_map)
    decay = by_heads(jnp.exp(-jnp.exp(-jax.nn.softplus(-decay_pre) - 0.5)))
    alpha_low = project(shifted(4), strength_down_map).astype(jnp.bfloat16)
    alpha = by_heads(jax.nn.sigmoid(project(alpha_low, strength_up_map)))
    removal = key_rows * removal_key_scale.reshape(head_number, head_extent)
    removal = removal * lax.rsqrt(jnp.sum(removal * removal, axis=-1, keepdims=True) + KEY_EPS)
    blended_rows = key_rows * (1.0 + (alpha - 1.0) * key_damping.reshape(head_number, head_extent))
    along = jnp.einsum("shij,shj->shi", state, removal)
    new_state = (
        state * decay[:, :, None, :]
        - along[..., None] * (removal * alpha)[:, :, None, :]
        + value_matrix[..., None] * blended_rows[:, :, None, :]
    )
    readout = jnp.einsum("shij,shj->shi", new_state, receptance_rows)
    centered = readout - jnp.mean(readout, axis=-1, keepdims=True)
    variance = jnp.mean(centered * centered, axis=-1, keepdims=True)
    heads_normalised = (
        centered
        * lax.rsqrt(variance + GROUP_EPS)
        * head_norm_gain.reshape(head_number, head_extent)
    )
    self_term = (
        jnp.sum(receptance_rows * blended_rows * self_term_weight, axis=-1, keepdims=True)
        * value_matrix
    )
    mixed_inputs = (
        (heads_normalised + self_term)
        .reshape(sequence_count, head_number * head_extent)
        .astype(jnp.bfloat16)
    )
    return (mixed_inputs, new_state)


def shards(
    tokens,
    previous,
    first_norm_gain,
    token_shift_share,
    receptance_weight,
    key_weight,
    value_weight,
    decay_down_map,
    decay_up_map,
    decay_offset,
    strength_down_map,
    strength_up_map,
    removal_key_scale,
    key_damping,
    self_term_weight,
    head_norm_gain,
    output_weight,
    state,
    second_norm_gain,
    routes,
    chosen_expert_weight,
    expert_gate_weight,
    expert_up_weight,
    expert_down_weight,
):
    present_rows, prior_rows = in_one_piece((tokens, previous), "tp", 1, 0)
    head_columns = receptance_weight.shape[1]
    head_start = lax.axis_index("tp") * head_columns
    decay_own = lax.dynamic_slice_in_dim(decay_up_map, head_start, head_columns, 1)
    alpha_own = lax.dynamic_slice_in_dim(strength_up_map, head_start, head_columns, 1)
    mixed_inputs, new_state = head_combiner(
        present_rows,
        prior_rows,
        first_norm_gain,
        token_shift_share,
        receptance_weight,
        key_weight,
        value_weight,
        decay_down_map,
        decay_own,
        decay_offset,
        strength_down_map,
        alpha_own,
        removal_key_scale,
        key_damping,
        self_term_weight,
        head_norm_gain,
        state,
    )
    head_terms = jnp.dot(mixed_inputs, output_weight, preferred_element_type=jnp.float32)
    own_columns = tokens.shape[1]
    column_start = lax.axis_index("tp") * own_columns
    residual = present_rows.astype(jnp.float32) + of_everyone(
        head_terms.astype(jnp.bfloat16), "tp"
    ).astype(jnp.float32)
    expert_rows = row_rescale(residual, second_norm_gain).astype(jnp.bfloat16)
    residual_own = lax.dynamic_slice_in_dim(residual, column_start, own_columns, 1)
    normed_own = lax.dynamic_slice_in_dim(expert_rows, column_start, own_columns, 1)
    sequences, choices_per = routes.shape
    experts = expert_gate_weight.shape[0] * lax.axis_size("ep")
    capacity = max(2, 3 * sequences * choices_per // (2 * experts))
    flattened = routes.reshape(-1)
    onehot = (flattened[:, None] == jnp.arange(experts, dtype=jnp.int32)[None, :]).astype(jnp.int32)
    ranking = jnp.sum((jnp.cumsum(onehot, axis=0) - onehot) * onehot, axis=1)
    slot_index = flattened * capacity + ranking
    placing = jnp.arange(experts * capacity, dtype=jnp.int32)[:, None] == slot_index[None, :]
    dispatch = jnp.sum(
        placing.reshape(experts * capacity, sequences, choices_per).astype(jnp.int32), axis=2
    ).astype(jnp.bfloat16)
    outgoing = jnp.dot(dispatch, normed_own, preferred_element_type=jnp.float32).astype(
        jnp.bfloat16
    )
    outgoing = outgoing.reshape(experts, capacity, -1)
    arrived = gather_directly(
        lax.all_to_all(outgoing, "ep", split_axis=0, concat_axis=0, tiled=True), "tp", 2
    )
    sources, slot_count, feature_count = arrived.shape
    expert_input = arrived.reshape(sources * slot_count, feature_count)
    gate_pre = jnp.minimum(
        jnp.dot(expert_input, expert_gate_weight[0], preferred_element_type=jnp.float32), GATE_LIMIT
    )
    up_pre = jnp.clip(
        jnp.dot(expert_input, expert_up_weight[0], preferred_element_type=jnp.float32),
        -GATE_LIMIT,
        GATE_LIMIT,
    )
    activation = ((up_pre + 1.0) * gate_pre * jax.nn.sigmoid(GATE_SLOPE * gate_pre)).astype(
        jnp.bfloat16
    )
    down_terms = jnp.dot(activation, expert_down_weight[0], preferred_element_type=jnp.float32)
    down_terms = down_terms.reshape(sources, slot_count, -1)
    shares = summed_on_arrival(down_terms.astype(jnp.bfloat16), "tp", 2).astype(jnp.bfloat16)
    returned = lax.all_to_all(shares, "ep", split_axis=0, concat_axis=0, tiled=True)
    returned_rows = returned.reshape(experts * capacity, -1)
    picked = jnp.take(returned_rows, slot_index, axis=0).astype(jnp.float32)
    weighted = jnp.sum(
        picked.reshape(sequences, choices_per, -1) * chosen_expert_weight[:, :, None], axis=1
    )
    layer_out = (residual_own + weighted).astype(jnp.bfloat16)
    return (layer_out, new_state)


def solution(mesh):
    in_specs = (
        P("ep", "tp"),
        P("ep", "tp"),
        P(),
        P(),
        P(None, "tp"),
        P(None, "tp"),
        P(None, "tp"),
        P(),
        P(),
        P("tp"),
        P(),
        P(),
        P("tp"),
        P("tp"),
        P("tp", None),
        P("tp"),
        P("tp", None),
        P("ep", "tp", None, None),
        P(),
        P("ep", None),
        P("ep", None),
        P("ep", None, "tp"),
        P("ep", None, "tp"),
        P("ep", "tp", None),
    )
    out_specs = (P("ep", "tp"), P("ep", "tp", None, None))
    return jax.shard_map(shards, mesh=mesh, in_specs=in_specs, out_specs=out_specs, check_vma=False)
```

profile of v0, /device:TPU:1, one launch (start us, length us, event | category | flops | bytes accessed | tf_op | source)
XLA Modules:
  0.0 125.7 jit_solution(13619742929195453664)
XLA Ops:
  0.7 0.9 pad_maximum_fusion
  1.6 11.0 %all_gather.3 = bf16[64,2048]{1,0:T(8,128)(2,1)S(1)} all-gather(bf16[64,512]{1,0:T(8,128)(2,1)S(1)} %pad_maximum_fusion), channel_id=1, replica_groups=mesh['ep'=64,'tp'=4] {'tp'}, dimensions={1}, use_global_device_ids=true | all-gather | bytes 327680 | tf_op jit(solution)/shard_map/all_gather | solution.py:16
  12.8 1.1 fusion.98
  13.8 1.6 %fusion.29 = f32[32,256]{1,0:T(8,128)S(1)} fusion(bf16[2048,256]{1,0:T(8,128)(2,1)} %param.28, f32[2048]{0:T(1024)S(1)} %bitcast.67, f32[2048]{0:T(1024)} %param.26, f32[32]{0:T(128)S(1)} %add_rsqrt_fusion.3, bf16[64,2048]{1,0:T(8,128)(2,1)S(1)} %all_gather.3), kind=kOutput, calls=%fused_computation.47 | convolution fusion | flops 34078720 | bytes 1360000 | tf_op jit(solution)/shard_map/dot_general | solution.py:87
  15.6 1.4 %fusion.10 = f32[32,256]{1,0:T(8,128)S(1)} fusion(bf16[2048,128]{1,0:T(8,128)(2,1)} %param.34, f32[2048]{0:T(1024)S(1)} %bitcast.69, f32[2048]{0:T(1024)} %param.26, f32[32]{0:T(128)S(1)} %add_rsqrt_fusion.3, bf16[64,2048]{1,0:T(8,128)(2,1)S(1)} %all_gather.3, bf16[128,1024]{1,0:T(8,128)(2,1)} %param.35, s32[]{:T(128)S(6)} %select_n.34), kind=kOutput, calls=%fused_computation.18 | convolution fusion | flops 19427328 | bytes 901252 | tf_op jit(solution)/shard_map/dot_general | solution.py:87
  17.1 1.6 %fusion.35 = f32[32,256]{1,0:T(8,128)S(1)} fusion(bf16[2048,256]{1,0:T(8,128)(2,1)} %param.29, f32[2048]{0:T(1024)S(1)} %bitcast.66, f32[2048]{0:T(1024)} %param.26, f32[32]{0:T(128)S(1)} %add_rsqrt_fusion.3, bf16[64,2048]{1,0:T(8,128)(2,1)S(1)} %all_gather.3), kind=kOutput, calls=%fused_computation.49 | convolution fusion | flops 34078720 | bytes 1360000 | tf_op jit(solution)/shard_map/dot_general | solution.py:87
  19.1 1.3 %fusion.82 = f32[32,256]{1,0:T(8,128)S(1)} fusion(bf16[128,1024]{1,0:T(8,128)(2,1)} %param.32, s32[]{:T(128)S(6)} %select_n.34, bf16[2048,128]{1,0:T(8,128)(2,1)S(1)} %copy-done.13, f32[2048]{0:T(1024)S(1)} %bitcast.68, f32[2048]{0:T(1024)S(1)} %copy-done.6, f32[32]{0:T(128)S(1)} %add_rsqrt_fusion.3, bf16[64,2048]{1,0:T(8,128)(2,1)S(1)} %all_gather.3, ...), kind=kOutput, calls=%fused_computation.96 | convolution fusion | flops 19492864 | bytes 902276 | tf_op jit(solution)/shard_map/dot_general | solution.py:87
  20.5 0.3 fusion.31
  21.1 3.5 %fusion.99 = f32[32,4,1,64]{3,2,1,0:T(1,128)S(1)} fusion(f32[32,4,64,1]{2,3,1,0:T(1,128)S(1)} %bitcast.64, f32[32,4,64,64]{3,2,1,0:T(8,128)} %param.41), kind=kOutput, calls=%fused_computation.119 | convolution fusion | flops 1048576 | bytes 2162688 | tf_op jit(solution)/shard_map/shij,shj->shi/dot_general | solution.py:103
  24.6 2.8 %multiply_add_fusion = f32[32,4,64,64]{3,2,1,0:T(8,128)S(1)} fusion(f32[32,4,64,64]{3,2,1,0:T(8,128)S(1)} %copy-done.1, f32[32,4,64]{2,1,0:T(4,128)S(1)} %get-tuple-element.8, f32[32,4,64]{2,1,0:T(4,128)S(1)} %mul.306, f32[32,4,64]{2,1,0:T(4,128)S(1)} %get-tuple-element.6, f32[32,4,64]{2,1,0:T(4,128)S(1)} %bitcast.62, f32[32,4,64]{2,1,0:T(4,128)S(1)} %mul.284), kind=kLoop, calls=%fused_computation.2 | loop fusion | flops 2621440 | bytes 4358144 | tf_op jit(solution)/shard_map/add | solution.py:105
  27.5 2.0 %copy-done.2 = f32[32,4,64,64]{3,2,1,0:T(8,128)} copy-done((f32[32,4,64,64]{3,2,1,0:T(8,128)}, f32[32,4,64,64]{3,2,1,0:T(8,128)S(1)}, u32[]{:S(2)}) %copy-start.2) | copy-done | bytes 2097176
  29.4 1.2 fusion.100
  31.1 0.5 fusion.7
  31.7 0.3 convolution_convert_fusion.1
  32.0 0.8 broadcast_in_dim.11
  32.8 3.5 %all-to-all-start = ((bf16[4,32,2048]{2,1,0:T(8,128)(2,1)}), bf16[4,32,2048]{2,1,0:T(8,128)(2,1)S(1)}, u32[]{:S(2)}, u32[]{:S(2)}) async-start(bf16[4,32,2048]{2,1,0:T(8,128)(2,1)} %broadcast_in_dim.11), calls=%async_computation | async-start | bytes 1048576 | tf_op jit(solution)/shard_map/all_to_all | solution.py:22
  37.1 0.8 dynamic-slice
  38.0 5.2 %all-to-all-done = bf16[4,32,2048]{2,1,0:T(8,128)(2,1)S(1)} async-done(((bf16[4,32,2048]{2,1,0:T(8,128)(2,1)}), bf16[4,32,2048]{2,1,0:T(8,128)(2,1)S(1)}, u32[]{:S(2)}, u32[]{:S(2)}) %all-to-all-start) | async-done | bytes 524320 | tf_op jit(solution)/shard_map/all_to_all | solution.py:22
  43.5 0.3 convolution_convert_fusion.2
  43.8 29.1 %all_to_all.25 = bf16[64,3,512]{2,1,0:T(4,128)(2,1)S(1)} all-to-all(bf16[64,3,512]{2,1,0:T(4,128)(2,1)S(1)} %reshape.165), channel_id=1, replica_groups=mesh['ep'=64,'tp'=4] {'ep'}, dimensions={0} | all-to-all | bytes 393216 | tf_op jit(solution)/shard_map/all_to_all | solution.py:204
  73.0 14.7 %all_to_all.26 = bf16[4,64,3,512]{3,1,2,0:T(8,128)(2,1)S(1)} all-to-all(bf16[4,64,3,512]{3,1,2,0:T(8,128)(2,1)S(1)} %broadcast_in_dim.13), channel_id=1, replica_groups=mesh['ep'=64,'tp'=4] {'tp'}, dimensions={0} | all-to-all | bytes 1572864 | tf_op jit(solution)/shard_map/all_to_all | solution.py:22
  87.7 0.6 copy.65
  88.5 0.4 convolution_minimum_fusion
  88.9 0.4 fusion.4
  89.4 0.4 convolution_convert_fusion
  89.8 13.7 %all_to_all.27 = bf16[4,64,3,512]{3,1,2,0:T(8,128)(2,1)S(1)} all-to-all(bf16[4,64,3,512]{3,1,2,0:T(8,128)(2,1)S(1)} %bitcast.55), channel_id=1, replica_groups=mesh['ep'=64,'tp'=4] {'tp'}, dimensions={0} | all-to-all | bytes 1572864 | tf_op jit(solution)/shard_map/all_to_all | solution.py:39
  103.7 0.9 copy.69
  104.5 6.1 %all-to-all-start.4 = ((bf16[64,3,512]{2,1,0:T(4,128)(2,1)}), bf16[64,3,512]{2,1,0:T(4,128)(2,1)S(1)}, u32[]{:S(2)}, u32[]{:S(2)}) async-start(bf16[64,3,512]{2,1,0:T(4,128)(2,1)} %copy.69), calls=%async_computation.4 | async-start | bytes 524288 | tf_op jit(solution)/shard_map/all_to_all | solution.py:222
  111.0 12.7 %all-to-all-done.4 = bf16[64,3,512]{2,1,0:T(4,128)(2,1)S(1)} async-done(((bf16[64,3,512]{2,1,0:T(4,128)(2,1)}), bf16[64,3,512]{2,1,0:T(4,128)(2,1)S(1)}, u32[]{:S(2)}, u32[]{:S(2)}) %all-to-all-start.4) | async-done | bytes 196640 | tf_op jit(solution)/shard_map/all_to_all | solution.py:222
  123.9 0.8 gather_fusion
  124.8 0.3 multiply_reduce_fusion
  125.1 0.6 add_convert_fusion
  (78 shorter events, 4.1 us)
Async XLA Ops:
  0.6 88.7 %copy-start = (bf16[1,256,2048]{2,1,0:T(8,128)(2,1)S(1)}, bf16[1,256,2048]{2,1,0:T(8,128)(2,1)}, u32[]{:S(2)}) copy-start(bf16[1,256,2048]{2,1,0:T(8,128)(2,1)} %param.47) | copy-start | bytes 3145732
  0.6 18.5 %copy-start.6 = (f32[2048]{0:T(1024)S(1)}, f32[2048]{0:T(1024)}, u32[]{:S(2)}) copy-start(f32[2048]{0:T(1024)} %param.26) | copy-start | bytes 24580
  0.7 18.2 %copy-start.9 = (f32[256]{0:T(256)S(1)}, f32[256]{0:T(256)}, u32[]{:S(2)}) copy-start(f32[256]{0:T(256)} %param.36) | copy-start | bytes 3076
  0.7 18.4 %copy-start.10 = (f32[256]{0:T(256)S(1)}, f32[256]{0:T(256)}, u32[]{:S(2)}) copy-start(f32[256]{0:T(256)} %param.37) | copy-start | bytes 3076
  0.7 18.5 %copy-start.13 = (bf16[2048,128]{1,0:T(8,128)(2,1)S(1)}, bf16[2048,128]{1,0:T(8,128)(2,1)}, u32[]{:S(2)}) copy-start(bf16[2048,128]{1,0:T(8,128)(2,1)} %param.31) | copy-start | bytes 1572868
  0.7 18.4 %copy-start.15 = (f32[256]{0:T(256)S(1)}, f32[256]{0:T(256)}, u32[]{:S(2)}) copy-start(f32[256]{0:T(256)} %param.33) | copy-start | bytes 3076
  0.7 19.8 %copy-start.4 = (bf16[2048,256]{1,0:T(8,128)(2,1)S(1)}, bf16[2048,256]{1,0:T(8,128)(2,1)}, u32[]{:S(2)}) copy-start(bf16[2048,256]{1,0:T(8,128)(2,1)} %param.30) | copy-start | bytes 3145732
  21.0 3.6 %copy-start.1 = (f32[32,4,64,64]{3,2,1,0:T(8,128)S(1)}, f32[32,4,64,64]{3,2,1,0:T(8,128)}, u32[]{:S(2)}) copy-start(f32[32,4,64,64]{3,2,1,0:T(8,128)} %param.41) | copy-start | bytes 6291460
  27.4 2.0 %copy-start.2 = (f32[32,4,64,64]{3,2,1,0:T(8,128)}, f32[32,4,64,64]{3,2,1,0:T(8,128)S(1)}, u32[]{:S(2)}) copy-start(f32[32,4,64,64]{3,2,1,0:T(8,128)S(1)} %multiply_add_fusion) | copy-start | bytes 6291460
  27.4 3.5 %copy-start.11 = (f32[256]{0:T(256)S(1)}, f32[256]{0:T(256)}, u32[]{:S(2)}) copy-start(f32[256]{0:T(256)} %param.39) | copy-start | bytes 3076
  27.4 3.6 %copy-start.14 = (f32[4,64]{1,0:T(4,128)S(1)}, f32[4,64]{1,0:T(4,128)}, u32[]{:S(2)}) copy-start(f32[4,64]{1,0:T(4,128)} %param.38) | copy-start | bytes 3076
  27.5 4.2 %copy-start.3 = (bf16[256,2048]{1,0:T(8,128)(2,1)S(1)}, bf16[256,2048]{1,0:T(8,128)(2,1)}, u32[]{:S(2)}) copy-start(bf16[256,2048]{1,0:T(8,128)(2,1)} %param.40) | copy-start | bytes 3145732
  27.5 8.8 %copy-start.7 = (s32[32,4]{0,1:T(4,128)S(1)}, s32[32,4]{0,1:T(4,128)}, u32[]{:S(2)}) copy-start(s32[32,4]{0,1:T(4,128)} %param.43) | copy-start | bytes 1540
  32.8 10.4 %all-to-all-start = ((bf16[4,32,2048]{2,1,0:T(8,128)(2,1)}), bf16[4,32,2048]{2,1,0:T(8,128)(2,1)S(1)}, u32[]{:S(2)}, u32[]{:S(2)}) async-start(bf16[4,32,2048]{2,1,0:T(8,128)(2,1)} %broadcast_in_dim.11), calls=%async_computation | async-start | bytes 1048576 | tf_op jit(solution)/shard_map/all_to_all | solution.py:22
  43.3 45.2 %copy-start.5 = (bf16[1,2048,256]{2,1,0:T(8,128)(2,1)S(1)}, bf16[1,2048,256]{2,1,0:T(8,128)(2,1)}, u32[]{:S(2)}) copy-start(bf16[1,2048,256]{2,1,0:T(8,128)(2,1)} %param.45) | copy-start | bytes 3145732
  72.9 16.0 %copy-start.12 = (bf16[1,2048,256]{2,1,0:T(8,128)(2,1)S(1)}, bf16[1,2048,256]{2,1,0:T(8,128)(2,1)}, u32[]{:S(2)}) copy-start(bf16[1,2048,256]{2,1,0:T(8,128)(2,1)} %param.46) | copy-start | bytes 3145732
  89.3 21.6 %copy-start.8 = (f32[32,4]{0,1:T(4,128)S(1)}, f32[32,4]{0,1:T(4,128)}, u32[]{:S(2)}) copy-start(f32[32,4]{0,1:T(4,128)} %param.44) | copy-start | bytes 1540
  104.5 19.2 %all-to-all-start.4 = ((bf16[64,3,512]{2,1,0:T(4,128)(2,1)}), bf16[64,3,512]{2,1,0:T(4,128)(2,1)S(1)}, u32[]{:S(2)}, u32[]{:S(2)}) async-start(bf16[64,3,512]{2,1,0:T(4,128)(2,1)} %copy.69), calls=%async_computation.4 | async-start | bytes 524288 | tf_op jit(solution)/shard_map/all_to_all | solution.py:222
where the time goes:
time: 126 us
  blocking collectives  68.4 us (54%)
  waiting for transfers between devices  17.9 us (14%)
  matrix products  12.5 us (10%)
  starting transfers between devices  9.55 us (8%)
  local copies, waits for them, and re-layouts  9.45 us (7%)
  other arithmetic  6.78 us (5%)
    all_to_all x1, blocking collectives, shards(): lax.all_to_all(outgoing, 'ep', split_axis=0, concat_axis=0, tiled=True)  29.1 us
    all_to_all x1, blocking collectives, sent_to_all(): lax.all_to_all(jnp.broadcast_to(value[None], (devices, *value.shape)), ax...  14.7 us
    all_to_all x1, blocking collectives, summed_on_arrival(): lax.all_to_all(tiles, axis, split_axis=0, concat_axis=0, tiled=True)  13.7 us
    all_to_all x1, waiting for transfers between devices, shards(): lax.all_to_all(shares, 'ep', split_axis=0, concat_axis=0, tiled=True)  12.7 us
    all_gather x1, blocking collectives, in_one_piece(): result = lax.all_gather(both, axis, axis=dim, tiled=True)  11 us
    dot_general x5, matrix products, project(): return jnp.dot(inputs, weight, preferred_element_type=jnp.float32)  6.18 us
    all_to_all x1, starting transfers between devices, shards(): lax.all_to_all(shares, 'ep', split_axis=0, concat_axis=0, tiled=True)  6.08 us
    all_to_all x1, waiting for transfers between devices, sent_to_all(): lax.all_to_all(jnp.broadcast_to(value[None], (devices, *value.shape)), ax...  5.18 us
  transfers between devices with their start and end apart: 2, of which 2 were waited for; matrix products, arithmetic and copies ran while one was open for 2% of the time, Pallas kernels for 0%

commit v1 on v0

v1 whole, which is shorter than its diff:
```python
import jax
import jax.numpy as jnp
from jax import lax
from jax.experimental import pallas as pl
from jax.experimental.pallas import tpu as pltpu
from jax.sharding import PartitionSpec as P

NORM_EPS = 1e-06
GROUP_EPS = 0.00064
KEY_EPS = 1e-06
GATE_LIMIT = 7.0
GATE_SLOPE = 1.702
CAPACITY = 3


def from_offset(value, offset, axis="tp"):
    devices = lax.axis_size(axis)
    return lax.ppermute(value, axis, [(i, (i - offset) % devices) for i in range(devices)])


def to_offset(value, offset, axis="tp"):
    return from_offset(value, -offset, axis)


def row_rescale(values, gain):
    return values * lax.rsqrt(jnp.mean(values * values, axis=-1, keepdims=True) + NORM_EPS) * gain


def head_combiner(
    present_rows,
    prior_rows,
    first_norm_gain,
    token_shift_share,
    receptance_weight,
    key_weight,
    value_weight,
    decay_down_map,
    decay_up_map,
    decay_offset,
    strength_down_map,
    strength_up_map,
    removal_key_scale,
    key_damping,
    self_term_weight,
    head_norm_gain,
    state,
):
    sequence_count = present_rows.shape[0]
    head_number = state.shape[1]
    head_extent = state.shape[2]
    normed = row_rescale(present_rows.astype(jnp.float32), first_norm_gain)
    before = prior_rows.astype(jnp.float32)

    def shifted(role):
        return (normed + (before - normed) * token_shift_share[role]).astype(jnp.bfloat16)

    def project(inputs, weight):
        return jnp.dot(inputs, weight, preferred_element_type=jnp.float32)

    def by_heads(values):
        return values.reshape(sequence_count, head_number, head_extent)

    receptance_rows = by_heads(project(shifted(0), receptance_weight))
    key_rows = by_heads(project(shifted(1), key_weight))
    value_matrix = by_heads(project(shifted(2), value_weight))
    decay_low = jnp.tanh(project(shifted(3), decay_down_map)).astype(jnp.bfloat16)
    decay_pre = decay_offset + project(decay_low, decay_up_map)
    decay = by_heads(jnp.exp(-jnp.exp(-jax.nn.softplus(-decay_pre) - 0.5)))
    alpha_low = project(shifted(4), strength_down_map).astype(jnp.bfloat16)
    alpha = by_heads(jax.nn.sigmoid(project(alpha_low, strength_up_map)))
    removal = key_rows * removal_key_scale.reshape(head_number, head_extent)
    removal = removal * lax.rsqrt(jnp.sum(removal * removal, axis=-1, keepdims=True) + KEY_EPS)
    blended_rows = key_rows * (1.0 + (alpha - 1.0) * key_damping.reshape(head_number, head_extent))
    along = jnp.einsum("shij,shj->shi", state, removal)
    kept = jnp.einsum("shij,shj->shi", state, decay * receptance_rows)
    readout = (
        kept
        - along * jnp.sum(removal * alpha * receptance_rows, axis=-1, keepdims=True)
        + value_matrix * jnp.sum(blended_rows * receptance_rows, axis=-1, keepdims=True)
    )
    new_state = (
        state * decay[:, :, None, :]
        - along[..., None] * (removal * alpha)[:, :, None, :]
        + value_matrix[..., None] * blended_rows[:, :, None, :]
    )
    centered = readout - jnp.mean(readout, axis=-1, keepdims=True)
    variance = jnp.mean(centered * centered, axis=-1, keepdims=True)
    heads_normalised = (
        centered
        * lax.rsqrt(variance + GROUP_EPS)
        * head_norm_gain.reshape(head_number, head_extent)
    )
    self_term = (
        jnp.sum(receptance_rows * blended_rows * self_term_weight, axis=-1, keepdims=True)
        * value_matrix
    )
    mixed_inputs = (
        (heads_normalised + self_term)
        .reshape(sequence_count, head_number * head_extent)
        .astype(jnp.bfloat16)
    )
    return (mixed_inputs, new_state)


def hidden_kernel(at, x0, x1, x2, x3, gain, gate_weight, up_weight, out):
    pieces = (x0, x1, x2, x3)
    width = x0.shape[1]
    places = [lax.rem(at[0] + k, 4) * width for k in range(4)]
    floats = [x[...].astype(jnp.float32) for x in pieces]
    squares = sum(jnp.sum(f * f, axis=1, keepdims=True) for f in floats)
    scale = lax.rsqrt(squares / (4 * width) + NORM_EPS)
    gate = jnp.zeros(out.shape, jnp.float32)
    up = jnp.zeros(out.shape, jnp.float32)
    for f, place in zip(floats, places):
        rows = pl.ds(pl.multiple_of(place, width), width)
        x = (f * scale * gain[:, rows]).astype(jnp.bfloat16)
        gate = gate + jnp.dot(x, gate_weight[rows, :], preferred_element_type=jnp.float32)
        up = up + jnp.dot(x, up_weight[rows, :], preferred_element_type=jnp.float32)
    gate = jnp.minimum(gate, GATE_LIMIT)
    up = jnp.clip(up, -GATE_LIMIT, GATE_LIMIT)
    out[...] = ((up + 1.0) * gate * jax.nn.sigmoid(GATE_SLOPE * gate)).astype(jnp.bfloat16)


def down_kernel(a0, a1, a2, a3, w0, w1, w2, w3, out):
    total = jnp.zeros(out.shape, jnp.float32)
    for a, w in ((a0, w0), (a1, w1), (a2, w2), (a3, w3)):
        total = total + jnp.dot(a[...], w[...], preferred_element_type=jnp.float32)
    out[...] = total.astype(jnp.bfloat16)


def in_vmem(count):
    return [pl.BlockSpec(memory_space=pltpu.VMEM)] * count


def shards(
    tokens,
    previous,
    first_norm_gain,
    token_shift_share,
    receptance_weight,
    key_weight,
    value_weight,
    decay_down_map,
    decay_up_map,
    decay_offset,
    strength_down_map,
    strength_up_map,
    removal_key_scale,
    key_damping,
    self_term_weight,
    head_norm_gain,
    output_weight,
    state,
    second_norm_gain,
    routes,
    chosen_expert_weight,
    expert_gate_weight,
    expert_up_weight,
    expert_down_weight,
):
    at = lax.axis_index("tp")
    sequences, own_columns = tokens.shape
    both = jnp.concatenate([tokens, previous], axis=0)
    pieces = [both] + [from_offset(both, k) for k in (1, 2, 3)]
    rotated = jnp.concatenate(pieces + pieces[:3], axis=1)
    everyone = lax.dynamic_slice_in_dim(
        rotated, lax.rem(4 - at, 4) * own_columns, 4 * own_columns, 1
    )
    present_rows, prior_rows = everyone[:sequences], everyone[sequences:]

    experts = expert_gate_weight.shape[0] * lax.axis_size("ep")
    ids = jnp.arange(experts, dtype=jnp.int32)
    hits = routes[:, :, None] == ids[None, None, :]
    named = jnp.sum(hits.astype(jnp.float32), axis=1)
    earlier = jnp.tril(jnp.ones((sequences, sequences), jnp.float32), -1)
    ranking = jnp.dot(earlier, named)
    weight_of = jnp.sum(jnp.where(hits, chosen_expert_weight[:, :, None], 0.0), axis=1)
    slots = [(ranking == c) & (named > 0) for c in range(CAPACITY)]
    dispatch = jnp.concatenate([s.astype(jnp.bfloat16) for s in slots], axis=1)
    combine = jnp.concatenate([jnp.where(s, weight_of, 0.0) for s in slots], axis=1)

    head_columns = receptance_weight.shape[1]
    decay_own = lax.dynamic_slice_in_dim(decay_up_map, at * head_columns, head_columns, 1)
    alpha_own = lax.dynamic_slice_in_dim(strength_up_map, at * head_columns, head_columns, 1)
    mixed_inputs, new_state = head_combiner(
        present_rows,
        prior_rows,
        first_norm_gain,
        token_shift_share,
        receptance_weight,
        key_weight,
        value_weight,
        decay_down_map,
        decay_own,
        decay_offset,
        strength_down_map,
        alpha_own,
        removal_key_scale,
        key_damping,
        self_term_weight,
        head_norm_gain,
        state,
    )
    head_terms = jnp.dot(
        mixed_inputs, output_weight, preferred_element_type=jnp.float32
    ).astype(jnp.bfloat16)
    down_weight = expert_down_weight[0]

    def columns_of(value, k):
        return lax.dynamic_slice_in_dim(value, lax.rem(at + k, 4) * own_columns, own_columns, 1)

    arrived = [columns_of(head_terms, 0)] + [
        to_offset(columns_of(head_terms, k), k) for k in (1, 2, 3)
    ]
    residual = tokens.astype(jnp.float32) + sum(a.astype(jnp.float32) for a in arrived)
    down_tied, head_tied = lax.optimization_barrier((down_weight, head_terms))
    down_pieces = [columns_of(down_weight, 0)] + [
        to_offset(columns_of(down_tied, k), k) for k in (1, 2, 3)
    ]

    outgoing = lax.dot_general(
        dispatch,
        residual.astype(jnp.bfloat16),
        (((0,), (0,)), ((), ())),
        preferred_element_type=jnp.float32,
    ).astype(jnp.bfloat16)
    outgoing = outgoing.reshape(CAPACITY, experts, own_columns)
    came = lax.all_to_all(outgoing, "ep", split_axis=1, concat_axis=1, tiled=True)
    own_rows = came.reshape(CAPACITY * experts, own_columns)
    row_pieces = [own_rows] + [from_offset(own_rows, k) for k in (1, 2, 3)]
    hidden_columns = expert_gate_weight.shape[2]
    activation = pl.pallas_call(
        hidden_kernel,
        out_shape=jax.ShapeDtypeStruct((own_rows.shape[0], hidden_columns), jnp.bfloat16),
        in_specs=[pl.BlockSpec(memory_space=pltpu.SMEM)] + in_vmem(7),
        out_specs=pl.BlockSpec(memory_space=pltpu.VMEM),
        name="hidden",
    )(
        at[None],
        *row_pieces,
        second_norm_gain[None, :],
        expert_gate_weight[0],
        expert_up_weight[0],
    )
    act_pieces = [activation] + [to_offset(activation, k) for k in (1, 2, 3)]
    shares = pl.pallas_call(
        down_kernel,
        out_shape=jax.ShapeDtypeStruct((own_rows.shape[0], own_columns), jnp.bfloat16),
        in_specs=in_vmem(8),
        out_specs=pl.BlockSpec(memory_space=pltpu.VMEM),
        name="down",
    )(*act_pieces, *down_pieces)
    shares = shares.reshape(CAPACITY, experts, own_columns)
    returned = lax.all_to_all(shares, "ep", split_axis=1, concat_axis=1, tiled=True)
    returned = returned.reshape(CAPACITY * experts, own_columns)
    high = combine.astype(jnp.bfloat16)
    low = (combine - high.astype(jnp.float32)).astype(jnp.bfloat16)
    weighted = jnp.dot(
        jnp.concatenate([high, low], axis=0), returned, preferred_element_type=jnp.float32
    )
    layer_out = (residual + weighted[:sequences] + weighted[sequences:]).astype(jnp.bfloat16)
    return (layer_out, new_state)


def solution(mesh):
    in_specs = (
        P("ep", "tp"),
        P("ep", "tp"),
        P(),
        P(),
        P(None, "tp"),
        P(None, "tp"),
        P(None, "tp"),
        P(),
        P(),
        P("tp"),
        P(),
        P(),
        P("tp"),
        P("tp"),
        P("tp", None),
        P("tp"),
        P("tp", None),
        P("ep", "tp", None, None),
        P(),
        P("ep", None),
        P("ep", None),
        P("ep", None, "tp"),
        P("ep", None, "tp"),
        P("ep", "tp", None),
    )
    out_specs = (P("ep", "tp"), P("ep", "tp", None, None))
    return jax.shard_map(shards, mesh=mesh, in_specs=in_specs, out_specs=out_specs, check_vma=False)
```

time: 126 us -> 127 us (level)
  blocking collectives: 68.4 us -> 27.7 us
  starting transfers between devices: 9.55 us -> 26.4 us
  waiting for transfers between devices: 17.9 us -> 29.6 us
  Pallas kernels: 0 us -> 5.75 us
  other arithmetic: 6.78 us -> 10.4 us
  local copies, waits for them, and re-layouts: 9.45 us -> 12.4 us
    all_to_all x3 -> x1, blocking collectives: 57.4 us -> 27.7 us  [shards(): lax.all_to_all(outgoing, 'ep', split_axis=1, concat_axis=1, tiled=True)]
    ppermute x0 -> x15, waiting for transfers between devices: none -> 22.5 us  [from_offset(): lax.ppermute(value, axis, [(i, (i - offset) % devices) for i in range(dev...]
    ppermute x0 -> x15, starting transfers between devices: none -> 19.3 us  [from_offset(): lax.ppermute(value, axis, [(i, (i - offset) % devices) for i in range(dev...]
    all_gather x1 -> x0, blocking collectives: 11 us -> none  [in_one_piece(): result = lax.all_gather(both, axis, axis=dim, tiled=True)]
    all_to_all x2 -> x1, waiting for transfers between devices: 17.9 us -> 7.15 us  [shards(): lax.all_to_all(shares, 'ep', split_axis=1, concat_axis=1, tiled=True)]
    pallas_call x0 -> x2, Pallas kernels: none -> 5.75 us  [the longest x1 3.33 us: shards(): pl.pallas_call(hidden_kernel, out_shape=jax.ShapeDtypeStruct((own_rows.sh...]
    add x1, other arithmetic: 2.81 us -> 5.9 us  [head_combiner(): state * decay[:, :, None, :]]
    all_to_all x2 -> x1, starting transfers between devices: 9.55 us -> 7.05 us  [shards(): lax.all_to_all(shares, 'ep', split_axis=1, concat_axis=1, tiled=True)]
  transfers between devices with their start and end apart: 2 -> 16, of which waited for: 2 -> 9; matrix products, arithmetic and copies ran while one was open for 2% -> 11% of each run, Pallas kernels for 0% -> 3%
where the time goes in v1:
time: 127 us; the launch traced here: 126 us
  waiting for transfers between devices  29.6 us (23%)
  blocking collectives  27.7 us (22%)
  starting transfers between devices  26.4 us (21%)
  local copies, waits for them, and re-layouts  12.4 us (10%)
  matrix products  12.4 us (10%)
  other arithmetic  10.4 us (8%)
  Pallas kernels  5.75 us (5%)
    all_to_all x1, blocking collectives, shards(): lax.all_to_all(outgoing, 'ep', split_axis=1, concat_axis=1, tiled=True)  27.7 us
    ppermute x15, waiting for transfers between devices, from_offset(): lax.ppermute(value, axis, [(i, (i - offset) % devices) for i in range(dev...  22.5 us
    ppermute x15, starting transfers between devices, from_offset(): lax.ppermute(value, axis, [(i, (i - offset) % devices) for i in range(dev...  19.3 us
    all_to_all x1, waiting for transfers between devices, shards(): lax.all_to_all(shares, 'ep', split_axis=1, concat_axis=1, tiled=True)  7.15 us
    all_to_all x1, starting transfers between devices, shards(): lax.all_to_all(shares, 'ep', split_axis=1, concat_axis=1, tiled=True)  7.05 us
    dot_general x5, matrix products, project(): return jnp.dot(inputs, weight, preferred_element_type=jnp.float32)  6.19 us
    add x1, other arithmetic, head_combiner(): state * decay[:, :, None, :]  5.9 us
    unnamed x55, local copies, waits for them, and re-layouts  3.97 us
  transfers between devices with their start and end apart: 16, of which 9 were waited for; matrix products, arithmetic and copies ran while one was open for 11% of the time, Pallas kernels for 3%

profile of v1, /device:TPU:1, one launch (start us, length us, event | category | flops | bytes accessed | tf_op | source)
XLA Modules:
  0.0 125.8 jit_solution(15608057627209165387)
XLA Ops:
  0.7 0.9 constant_dynamic-update-slice_fusion.1
  2.4 2.0 %collective-permute-start.2 = (bf16[64,512]{1,0:T(8,128)(2,1)S(1)}, bf16[64,512]{1,0:T(8,128)(2,1)S(1)}, u32[]{:S(2)}, u32[]{:S(2)}) collective-permute-start(bf16[64,512]{1,0:T(8,128)(2,1)S(1)} %get-tuple-element.33), channel_id=1, source_target_pairs={{0,1},{1,2},{2,3},{3,0},{4,5},{5,6},{6,7},{7,4},{8,9},{9,10},{10,1... | collective-permute-start | bytes 196616 | tf_op jit(solution)/shard_map/ppermute | solution.py:18
  4.4 2.5 %collective-permute-start.1 = (bf16[64,512]{1,0:T(8,128)(2,1)S(1)}, bf16[64,512]{1,0:T(8,128)(2,1)S(1)}, u32[]{:S(2)}, u32[]{:S(2)}) collective-permute-start(bf16[64,512]{1,0:T(8,128)(2,1)S(1)} %get-tuple-element.33), channel_id=1, source_target_pairs={{0,2},{1,3},{2,0},{3,1},{4,6},{5,7},{6,4},{7,5},{8,10},{9,11},{10,... | collective-permute-start | bytes 196616 | tf_op jit(solution)/shard_map/ppermute | solution.py:18
  6.8 1.2 collective-permute-start
  8.0 1.1 fusion.117
  9.1 0.8 select_reduce_fusion
  9.9 0.8 broadcast_select_fusion.2
  14.7 1.6 %fusion.28 = f32[32,256]{1,0:T(8,128)S(1)} fusion(bf16[2048,256]{1,0:T(8,128)(2,1)} %param.30, f32[2048]{0:T(1024)S(1)} %bitcast.57, f32[2048]{0:T(1024)} %param.26, f32[32]{0:T(128)S(1)} %add_rsqrt_fusion.2, bf16[64,3584]{1,0:T(8,128)(2,1)S(1)} %constant_dynamic-update-slice_fusion.2, s32[]{:T(128)S(6)} %add.185, s32[]{:T(128)S(6)} %select_n.45), kind=kOutput, calls=%fused_computation.38 | convolution fusion | flops 34078720 | bytes 1360392 | tf_op jit(solution)/shard_map/dot_general | solution.py:58
  16.4 1.6 %fusion.34 = f32[32,256]{1,0:T(8,128)S(1)} fusion(bf16[2048,256]{1,0:T(8,128)(2,1)} %param.28, f32[2048]{0:T(1024)S(1)} %bitcast.56, f32[2048]{0:T(1024)} %param.26, f32[32]{0:T(128)S(1)} %add_rsqrt_fusion.2, bf16[64,3584]{1,0:T(8,128)(2,1)S(1)} %constant_dynamic-update-slice_fusion.2, s32[]{:T(128)S(6)} %add.185, s32[]{:T(128)S(6)} %select_n.45), kind=kOutput, calls=%fused_computation.40 | convolution fusion | flops 34078720 | bytes 1360392 | tf_op jit(solution)/shard_map/dot_general | solution.py:58
  18.7 1.3 %fusion.81 = f32[32,256]{1,0:T(8,128)S(1)} fusion(bf16[128,1024]{1,0:T(8,128)(2,1)} %param.32, s32[]{:T(128)S(6)} %select_n.46, bf16[2048,128]{1,0:T(8,128)(2,1)S(1)} %copy-done.21, f32[2048]{0:T(1024)S(1)} %bitcast.60, f32[2048]{0:T(1024)S(1)} %copy-done.20, f32[32]{0:T(128)S(1)} %add_rsqrt_fusion.2, ...), kind=kOutput, calls=%fused_computation.86 | convolution fusion | flops 19492864 | bytes 902668 | tf_op jit(solution)/shard_map/dot_general | solution.py:58
  20.1 1.4 %fusion.12 = f32[32,256]{1,0:T(8,128)S(1)} fusion(bf16[2048,128]{1,0:T(8,128)(2,1)} %param.34, f32[2048]{0:T(1024)S(1)} %bitcast.59, f32[2048]{0:T(1024)S(1)} %copy-done.20, f32[32]{0:T(128)S(1)} %add_rsqrt_fusion.2, bf16[64,3584]{1,0:T(8,128)(2,1)S(1)} %constant_dynamic-update-slice_fusion.2, s32[]{:T(128)S(6)} %add.185, s32[]{:T(128)S(6)} %select_n.45, ...), kind=kOutput, calls=%fused_computation.16 | convolution fusion | flops 19427328 | bytes 901644 | tf_op jit(solution)/shard_map/dot_general | solution.py:58
  21.7 3.5 %fusion.120 = f32[32,4,1,64]{3,2,1,0:T(1,128)S(1)} fusion(f32[32,4,64,1]{2,3,1,0:T(1,128)S(1)} %bitcast.53, f32[32,4,64,64]{3,2,1,0:T(8,128)} %param.41), kind=kOutput, calls=%fused_computation.152 | convolution fusion | flops 1048576 | bytes 2162688 | tf_op jit(solution)/shard_map/shij,shj->shi/dot_general | solution.py:74
  25.3 1.2 fusion.119
  28.4 2.3 %collective-permute-start.5 = (bf16[32,512]{1,0:T(8,128)(2,1)S(1)}, bf16[32,512]{1,0:T(8,128)(2,1)S(1)}, u32[]{:S(2)}, u32[]{:S(2)}) collective-permute-start(bf16[32,512]{1,0:T(8,128)(2,1)S(1)} %get-tuple-element.21), channel_id=1, source_target_pairs={{0,3},{1,0},{2,1},{3,2},{4,7},{5,4},{6,5},{7,6},{8,11},{9,8},{10,9... | collective-permute-start | bytes 98312 | tf_op jit(solution)/shard_map/ppermute | solution.py:18
  30.7 1.3 %collective-permute-done.3 = bf16[32,512]{1,0:T(8,128)(2,1)S(1)} collective-permute-done((bf16[32,512]{1,0:T(8,128)(2,1)S(1)}, bf16[32,512]{1,0:T(8,128)(2,1)S(1)}, u32[]{:S(2)}, u32[]{:S(2)}) %collective-permute-start.3) | collective-permute-done | bytes 32800 | tf_op jit(solution)/shard_map/ppermute | solution.py:18
  32.0 3.0 %collective-permute-done.4 = bf16[32,512]{1,0:T(8,128)(2,1)S(1)} collective-permute-done((bf16[32,512]{1,0:T(8,128)(2,1)S(1)}, bf16[32,512]{1,0:T(8,128)(2,1)S(1)}, u32[]{:S(2)}, u32[]{:S(2)}) %collective-permute-start.4) | collective-permute-done | bytes 32800 | tf_op jit(solution)/shard_map/ppermute | solution.py:18
  35.6 27.7 %all_to_all.10 = bf16[3,64,512]{2,0,1:T(4,128)(2,1)S(1)} all-to-all(bf16[3,64,512]{2,0,1:T(4,128)(2,1)S(1)} %copy.39), channel_id=1, replica_groups=mesh['ep'=64,'tp'=4] {'ep'}, dimensions={1} | all-to-all | bytes 393216 | tf_op jit(solution)/shard_map/all_to_all | solution.py:228
  63.5 0.9 constant_dynamic-slice_fusion
  64.4 2.6 %collective-permute-start.14 = (bf16[256,512]{1,0:T(8,128)(2,1)}, bf16[256,512]{1,0:T(8,128)(2,1)S(1)}, u32[]{:S(2)}, u32[]{:S(2)}) collective-permute-start(bf16[256,512]{1,0:T(8,128)(2,1)} %get-tuple-element.17), channel_id=1, source_target_pairs={{0,3},{1,0},{2,1},{3,2},{4,7},{5,4},{6,5},{7,6},{8,11},{9,8},{10,9... | collective-permute-start | bytes 786440 | tf_op jit(solution)/shard_map/ppermute | solution.py:18
  67.6 2.4 %collective-permute-start.7 = (bf16[192,512]{1,0:T(8,128)(2,1)S(1)}, bf16[192,512]{1,0:T(8,128)(2,1)S(1)}, u32[]{:S(2)}, u32[]{:S(2)}) collective-permute-start(bf16[192,512]{1,0:T(8,128)(2,1)S(1)} %bitcast.44), channel_id=1, source_target_pairs={{0,2},{1,3},{2,0},{3,1},{4,6},{5,7},{6,4},{7,5},{8,10},{9,11},{10,... | collective-permute-start | bytes 589832 | tf_op jit(solution)/shard_map/ppermute | solution.py:18
  70.0 0.8 collective-permute-done.8.x3
  70.9 1.3 collective-permute-start.6
  73.6 12.1 %collective-permute-done.7.x2 = bf16[192,512]{1,0:T(8,128)(2,1)S(1)} collective-permute-done((bf16[192,512]{1,0:T(8,128)(2,1)S(1)}, bf16[192,512]{1,0:T(8,128)(2,1)S(1)}, u32[]{:S(2)}, u32[]{:S(2)}) %collective-permute-start.7) | collective-permute-done | bytes 196640 | tf_op jit(solution)/shard_map/ppermute | solution.py:18
  87.1 3.3 %hidden.1.a0 = bf16[192,256]{1,0:T(8,128)(2,1)} custom-call(s32[1]{0:T(128)} %bitcast.13.at, bf16[192,512]{1,0:T(8,128)(2,1)} %bitcast.46, bf16[192,512]{1,0:T(8,128)(2,1)} %copy-done.10, bf16[192,512]{1,0:T(8,128)(2,1)} %copy-done.9, bf16[192,512]{1,0:T(8,128)(2,1)} %copy-done.8, f32[1,2048]{1,0:T(1,128)} %bitcast.58, bf16[2048,256]{1,0:T(8,128)(2,1)} %bitcast.40, ...), custom_call_target="tpu_custom_call" | custom-call | tf_op jit(solution)/shard_map/hidden/pallas_call | solution.py:232
  90.5 3.4 %collective-permute-start.11 = (bf16[192,256]{1,0:T(8,128)(2,1)}, bf16[192,256]{1,0:T(8,128)(2,1)S(1)}, u32[]{:S(2)}, u32[]{:S(2)}) collective-permute-start(bf16[192,256]{1,0:T(8,128)(2,1)} %hidden.1.a0), channel_id=1, source_target_pairs={{0,3},{1,0},{2,1},{3,2},{4,7},{5,4},{6,5},{7,6},{8,11},{9,8},{10,9... | collective-permute-start | bytes 294920 | tf_op jit(solution)/shard_map/ppermute | solution.py:18
  95.3 1.1 collective-permute-done.11.a3
  96.4 2.8 %collective-permute-done.10.a2 = bf16[192,256]{1,0:T(8,128)(2,1)S(1)} collective-permute-done((bf16[192,256]{1,0:T(8,128)(2,1)}, bf16[192,256]{1,0:T(8,128)(2,1)S(1)}, u32[]{:S(2)}, u32[]{:S(2)}) %collective-permute-start.10) | collective-permute-done | bytes 98336 | tf_op jit(solution)/shard_map/ppermute | solution.py:18
  100.6 2.4 %down.1 = bf16[192,512]{1,0:T(8,128)(2,1)} custom-call(bf16[192,256]{1,0:T(8,128)(2,1)} %hidden.1.a0, bf16[192,256]{1,0:T(8,128)(2,1)} %copy-done.19, bf16[192,256]{1,0:T(8,128)(2,1)} %copy-done.18, bf16[192,256]{1,0:T(8,128)(2,1)} %copy-done.17, bf16[256,512]{1,0:T(8,128)(2,1)} %dynamic-slice_bitcast_fusion.w0, ...), custom_call_target="tpu_custom_call" | custom-call | tf_op jit(solution)/shard_map/down/pallas_call | solution.py:246
  103.0 1.8 %copy.41 = bf16[3,64,512]{2,0,1:T(4,128)(2,1)} copy(bf16[3,64,512]{2,1,0:T(8,128)(2,1)} %bitcast.47) | data formatting | bytes 393216 | tf_op jit(solution)/shard_map/reshape | solution.py:253
  104.8 7.0 %all-to-all-start.1 = ((bf16[3,64,512]{2,0,1:T(4,128)(2,1)}), bf16[3,64,512]{2,0,1:T(4,128)(2,1)S(1)}, u32[]{:S(2)}, u32[]{:S(2)}) async-start(bf16[3,64,512]{2,0,1:T(4,128)(2,1)} %copy.41), calls=%async_computation.1 | async-start | bytes 524288 | tf_op jit(solution)/shard_map/all_to_all | solution.py:254
  111.9 5.9 %multiply_add_fusion = f32[32,4,64,64]{3,2,1,0:T(8,128)} fusion(f32[32,4,64,64]{3,2,1,0:T(8,128)} %param.41, f32[32,4,64]{2,1,0:T(4,128)S(1)} %get-tuple-element.24, f32[32,4,64]{2,1,0:T(4,128)S(1)} %reshape.101, f32[32,4,64]{2,1,0:T(4,128)S(1)} %get-tuple-element.13, f32[32,4,64]{2,1,0:T(4,128)S(1)} %bitcast.51, f32[32,4,64]{2,1,0:T(4,128)S(1)} %reshape.97), kind=kLoop, calls=%fused_computation.3 | loop fusion | flops 2621440 | bytes 4358144 | tf_op jit(solution)/shard_map/add | solution.py:82
  117.8 7.1 %all-to-all-done.1 = bf16[3,64,512]{2,0,1:T(4,128)(2,1)S(1)} async-done(((bf16[3,64,512]{2,0,1:T(4,128)(2,1)}), bf16[3,64,512]{2,0,1:T(4,128)(2,1)S(1)}, u32[]{:S(2)}, u32[]{:S(2)}) %all-to-all-start.1) | async-done | bytes 196640 | tf_op jit(solution)/shard_map/all_to_all | solution.py:254
  (106 shorter events, 15.5 us)
Async XLA Ops:
  0.6 27.0 %copy-start = (bf16[256,2048]{1,0:T(8,128)(2,1)S(1)}, bf16[256,2048]{1,0:T(8,128)(2,1)}, u32[]{:S(2)}) copy-start(bf16[256,2048]{1,0:T(8,128)(2,1)} %param.40) | copy-start | bytes 3145732
  0.6 17.4 %copy-start.20 = (f32[2048]{0:T(1024)S(1)}, f32[2048]{0:T(1024)}, u32[]{:S(2)}) copy-start(f32[2048]{0:T(1024)} %param.26) | copy-start | bytes 24580
  0.7 17.4 %copy-start.3 = (bf16[2048,256]{1,0:T(8,128)(2,1)S(1)}, bf16[2048,256]{1,0:T(8,128)(2,1)}, u32[]{:S(2)}) copy-start(bf16[2048,256]{1,0:T(8,128)(2,1)} %param.29) | copy-start | bytes 3145732
  0.7 18.0 %copy-start.23 = (f32[256]{0:T(256)S(1)}, f32[256]{0:T(256)}, u32[]{:S(2)}) copy-start(f32[256]{0:T(256)} %param.33) | copy-start | bytes 3076
  0.7 18.0 %copy-start.21 = (bf16[2048,128]{1,0:T(8,128)(2,1)S(1)}, bf16[2048,128]{1,0:T(8,128)(2,1)}, u32[]{:S(2)}) copy-start(bf16[2048,128]{1,0:T(8,128)(2,1)} %param.31) | copy-start | bytes 1572868
  2.4 10.6 %collective-permute-start.2 = (bf16[64,512]{1,0:T(8,128)(2,1)S(1)}, bf16[64,512]{1,0:T(8,128)(2,1)S(1)}, u32[]{:S(2)}, u32[]{:S(2)}) collective-permute-start(bf16[64,512]{1,0:T(8,128)(2,1)S(1)} %get-tuple-element.33), channel_id=1, source_target_pairs={{0,1},{1,2},{2,3},{3,0},{4,5},{5,6},{6,7},{7,4},{8,9},{9,10},{10,1... | collective-permute-start | bytes 196616 | tf_op jit(solution)/shard_map/ppermute | solution.py:18
  4.4 8.6 %collective-permute-start.1 = (bf16[64,512]{1,0:T(8,128)(2,1)S(1)}, bf16[64,512]{1,0:T(8,128)(2,1)S(1)}, u32[]{:S(2)}, u32[]{:S(2)}) collective-permute-start(bf16[64,512]{1,0:T(8,128)(2,1)S(1)} %get-tuple-element.33), channel_id=1, source_target_pairs={{0,2},{1,3},{2,0},{3,1},{4,6},{5,7},{6,4},{7,5},{8,10},{9,11},{10,... | collective-permute-start | bytes 196616 | tf_op jit(solution)/shard_map/ppermute | solution.py:18
  6.8 6.1 %collective-permute-start = (bf16[64,512]{1,0:T(8,128)(2,1)S(1)}, bf16[64,512]{1,0:T(8,128)(2,1)S(1)}, u32[]{:S(2)}, u32[]{:S(2)}) collective-permute-start(bf16[64,512]{1,0:T(8,128)(2,1)S(1)} %get-tuple-element.33), channel_id=1, source_target_pairs={{0,3},{1,0},{2,1},{3,2},{4,7},{5,4},{6,5},{7,6},{8,11},{9,8},{10,9... | collective-permute-start | bytes 196616 | tf_op jit(solution)/shard_map/ppermute | solution.py:18
  21.6 3.7 %copy-start.1 = (f32[32,4,64,64]{3,2,1,0:T(8,128)S(1)}, f32[32,4,64,64]{3,2,1,0:T(8,128)}, u32[]{:S(2)}) copy-start(f32[32,4,64,64]{3,2,1,0:T(8,128)} %param.41) | copy-start | bytes 6291460
  21.7 5.3 %copy-start.22 = (f32[4,64]{1,0:T(4,128)S(1)}, f32[4,64]{1,0:T(4,128)}, u32[]{:S(2)}) copy-start(f32[4,64]{1,0:T(4,128)} %param.38) | copy-start | bytes 3076
  25.2 9.7 %copy-start.5 = (bf16[32,512]{1,0:T(8,128)(2,1)S(1)}, bf16[32,512]{1,0:T(8,128)(2,1)}, u32[]{:S(2)}) copy-start(bf16[32,512]{1,0:T(8,128)(2,1)} %param.24) | copy-start | bytes 98308
  25.3 38.2 %copy-start.2 = (bf16[1,256,2048]{2,1,0:T(8,128)(2,1)S(1)}, bf16[1,256,2048]{2,1,0:T(8,128)(2,1)}, u32[]{:S(2)}) copy-start(bf16[1,256,2048]{2,1,0:T(8,128)(2,1)} %param.47) | copy-start | bytes 3145732
  27.9 4.1 %collective-permute-start.3 = (bf16[32,512]{1,0:T(8,128)(2,1)S(1)}, bf16[32,512]{1,0:T(8,128)(2,1)S(1)}, u32[]{:S(2)}, u32[]{:S(2)}) collective-permute-start(bf16[32,512]{1,0:T(8,128)(2,1)S(1)} %get-tuple-element.20), channel_id=1, source_target_pairs={{0,1},{1,2},{2,3},{3,0},{4,5},{5,6},{6,7},{7,4},{8,9},{9,10},{10,1... | collective-permute-start | bytes 98312 | tf_op jit(solution)/shard_map/ppermute | solution.py:18
  28.4 3.7 %collective-permute-start.5 = (bf16[32,512]{1,0:T(8,128)(2,1)S(1)}, bf16[32,512]{1,0:T(8,128)(2,1)S(1)}, u32[]{:S(2)}, u32[]{:S(2)}) collective-permute-start(bf16[32,512]{1,0:T(8,128)(2,1)S(1)} %get-tuple-element.21), channel_id=1, source_target_pairs={{0,3},{1,0},{2,1},{3,2},{4,7},{5,4},{6,5},{7,6},{8,11},{9,8},{10,9... | collective-permute-start | bytes 98312 | tf_op jit(solution)/shard_map/ppermute | solution.py:18
  30.7 4.3 %collective-permute-start.4 = (bf16[32,512]{1,0:T(8,128)(2,1)S(1)}, bf16[32,512]{1,0:T(8,128)(2,1)S(1)}, u32[]{:S(2)}, u32[]{:S(2)}) collective-permute-start(bf16[32,512]{1,0:T(8,128)(2,1)S(1)} %get-tuple-element.22), channel_id=1, source_target_pairs={{0,2},{1,3},{2,0},{3,1},{4,6},{5,7},{6,4},{7,5},{8,10},{9,11},{10,... | collective-permute-start | bytes 98312 | tf_op jit(solution)/shard_map/ppermute | solution.py:18
  63.4 23.8 %copy-start.4 = (bf16[3,64,512]{2,1,0:T(8,128)(2,1)}, bf16[3,64,512]{2,1,0:T(8,128)(2,1)S(1)}, u32[]{:S(2)}) copy-start(bf16[3,64,512]{2,1,0:T(8,128)(2,1)S(1)} %copy.40) | copy-start | bytes 589828
  63.4 7.5 %collective-permute-start.8 = (bf16[192,512]{1,0:T(8,128)(2,1)S(1)}, bf16[192,512]{1,0:T(8,128)(2,1)S(1)}, u32[]{:S(2)}, u32[]{:S(2)}) collective-permute-start(bf16[192,512]{1,0:T(8,128)(2,1)S(1)} %bitcast.43), channel_id=1, source_target_pairs={{0,1},{1,2},{2,3},{3,0},{4,5},{5,6},{6,7},{7,4},{8,9},{9,10},{10,1... | collective-permute-start | bytes 589832 | tf_op jit(solution)/shard_map/ppermute | solution.py:18
  64.4 29.5 %collective-permute-start.14 = (bf16[256,512]{1,0:T(8,128)(2,1)}, bf16[256,512]{1,0:T(8,128)(2,1)S(1)}, u32[]{:S(2)}, u32[]{:S(2)}) collective-permute-start(bf16[256,512]{1,0:T(8,128)(2,1)} %get-tuple-element.17), channel_id=1, source_target_pairs={{0,3},{1,0},{2,1},{3,2},{4,7},{5,4},{6,5},{7,6},{8,11},{9,8},{10,9... | collective-permute-start | bytes 786440 | tf_op jit(solution)/shard_map/ppermute | solution.py:18
  67.1 28.2 %collective-permute-start.13 = (bf16[256,512]{1,0:T(8,128)(2,1)}, bf16[256,512]{1,0:T(8,128)(2,1)S(1)}, u32[]{:S(2)}, u32[]{:S(2)}) collective-permute-start(bf16[256,512]{1,0:T(8,128)(2,1)} %get-tuple-element.18), channel_id=1, source_target_pairs={{0,2},{1,3},{2,0},{3,1},{4,6},{5,7},{6,4},{7,5},{8,10},{9,11},{10,... | collective-permute-start | bytes 786440 | tf_op jit(solution)/shard_map/ppermute | solution.py:18
  67.1 28.2 %collective-permute-start.12 = (bf16[256,512]{1,0:T(8,128)(2,1)}, bf16[256,512]{1,0:T(8,128)(2,1)}, u32[]{:S(2)}, u32[]{:S(2)}) collective-permute-start(bf16[256,512]{1,0:T(8,128)(2,1)} %get-tuple-element.19), channel_id=1, source_target_pairs={{0,1},{1,2},{2,3},{3,0},{4,5},{5,6},{6,7},{7,4},{8,9},{9,10},{10,1... | collective-permute-start | bytes 786440 | tf_op jit(solution)/shard_map/ppermute | solution.py:18
  67.6 18.1 %collective-permute-start.7 = (bf16[192,512]{1,0:T(8,128)(2,1)S(1)}, bf16[192,512]{1,0:T(8,128)(2,1)S(1)}, u32[]{:S(2)}, u32[]{:S(2)}) collective-permute-start(bf16[192,512]{1,0:T(8,128)(2,1)S(1)} %bitcast.44), channel_id=1, source_target_pairs={{0,2},{1,3},{2,0},{3,1},{4,6},{5,7},{6,4},{7,5},{8,10},{9,11},{10,... | collective-permute-start | bytes 589832 | tf_op jit(solution)/shard_map/ppermute | solution.py:18
  70.9 16.3 %copy-start.8 = (bf16[192,512]{1,0:T(8,128)(2,1)}, bf16[192,512]{1,0:T(8,128)(2,1)S(1)}, u32[]{:S(2)}) copy-start(bf16[192,512]{1,0:T(8,128)(2,1)S(1)} %collective-permute-done.8.x3) | copy-start | bytes 589828
  70.9 15.6 %collective-permute-start.6 = (bf16[192,512]{1,0:T(8,128)(2,1)S(1)}, bf16[192,512]{1,0:T(8,128)(2,1)S(1)}, u32[]{:S(2)}, u32[]{:S(2)}) collective-permute-start(bf16[192,512]{1,0:T(8,128)(2,1)S(1)} %bitcast.45), channel_id=1, source_target_pairs={{0,3},{1,0},{2,1},{3,2},{4,7},{5,4},{6,5},{7,6},{8,11},{9,8},{10,9... | collective-permute-start | bytes 589832 | tf_op jit(solution)/shard_map/ppermute | solution.py:18
  90.5 5.9 %collective-permute-start.11 = (bf16[192,256]{1,0:T(8,128)(2,1)}, bf16[192,256]{1,0:T(8,128)(2,1)S(1)}, u32[]{:S(2)}, u32[]{:S(2)}) collective-permute-start(bf16[192,256]{1,0:T(8,128)(2,1)} %hidden.1.a0), channel_id=1, source_target_pairs={{0,3},{1,0},{2,1},{3,2},{4,7},{5,4},{6,5},{7,6},{8,11},{9,8},{10,9... | collective-permute-start | bytes 294920 | tf_op jit(solution)/shard_map/ppermute | solution.py:18
  93.9 5.3 %collective-permute-start.10 = (bf16[192,256]{1,0:T(8,128)(2,1)}, bf16[192,256]{1,0:T(8,128)(2,1)S(1)}, u32[]{:S(2)}, u32[]{:S(2)}) collective-permute-start(bf16[192,256]{1,0:T(8,128)(2,1)} %hidden.1.a0), channel_id=1, source_target_pairs={{0,2},{1,3},{2,0},{3,1},{4,6},{5,7},{6,4},{7,5},{8,10},{9,11},{10,... | collective-permute-start | bytes 294920 | tf_op jit(solution)/shard_map/ppermute | solution.py:18
  93.9 6.0 %copy-start.6 = (bf16[256,512]{1,0:T(8,128)(2,1)}, bf16[256,512]{1,0:T(8,128)(2,1)S(1)}, u32[]{:S(2)}) copy-start(bf16[256,512]{1,0:T(8,128)(2,1)S(1)} %collective-permute-done.14.w3) | copy-start | bytes 786436
  93.9 6.0 %collective-permute-start.9 = (bf16[192,256]{1,0:T(8,128)(2,1)}, bf16[192,256]{1,0:T(8,128)(2,1)S(1)}, u32[]{:S(2)}, u32[]{:S(2)}) collective-permute-start(bf16[192,256]{1,0:T(8,128)(2,1)} %hidden.1.a0), channel_id=1, source_target_pairs={{0,1},{1,2},{2,3},{3,0},{4,5},{5,6},{6,7},{7,4},{8,9},{9,10},{10,1... | collective-permute-start | bytes 294920 | tf_op jit(solution)/shard_map/ppermute | solution.py:18
  95.3 4.6 %copy-start.7 = (bf16[256,512]{1,0:T(8,128)(2,1)}, bf16[256,512]{1,0:T(8,128)(2,1)S(1)}, u32[]{:S(2)}) copy-start(bf16[256,512]{1,0:T(8,128)(2,1)S(1)} %collective-permute-done.13.w2) | copy-start | bytes 786436
  104.8 20.1 %all-to-all-start.1 = ((bf16[3,64,512]{2,0,1:T(4,128)(2,1)}), bf16[3,64,512]{2,0,1:T(4,128)(2,1)S(1)}, u32[]{:S(2)}, u32[]{:S(2)}) async-start(bf16[3,64,512]{2,0,1:T(4,128)(2,1)} %copy.41), calls=%async_computation.1 | async-start | bytes 524288 | tf_op jit(solution)/shard_map/all_to_all | solution.py:254
  111.9 13.3 %copy-start.12 = (bf16[32,512]{1,0:T(8,128)(2,1)S(1)}, bf16[32,512]{1,0:T(8,128)(2,1)}, u32[]{:S(2)}) copy-start(bf16[32,512]{1,0:T(8,128)(2,1)} %copy-done.11) | copy-start | bytes 98308
  111.9 13.3 %copy-start.14 = (bf16[32,512]{1,0:T(8,128)(2,1)S(1)}, bf16[32,512]{1,0:T(8,128)(2,1)}, u32[]{:S(2)}) copy-start(bf16[32,512]{1,0:T(8,128)(2,1)} %copy-done.13) | copy-start | bytes 98308
  111.9 13.3 %copy-start.16 = (bf16[32,512]{1,0:T(8,128)(2,1)S(1)}, bf16[32,512]{1,0:T(8,128)(2,1)}, u32[]{:S(2)}) copy-start(bf16[32,512]{1,0:T(8,128)(2,1)} %copy-done.15) | copy-start | bytes 98308
  (8 other events, 13.9 us)

commit v2 on v1

v2 whole, which is shorter than its diff:
```python
import math

import jax
import jax.numpy as jnp
from jax import lax
from jax.experimental import pallas as pl
from jax.experimental.pallas import tpu as pltpu
from jax.sharding import PartitionSpec as P

NORM_EPS = 1e-06
GROUP_EPS = 0.00064
KEY_EPS = 1e-06
GATE_LIMIT = 7.0
GATE_SLOPE = 1.702
CAPACITY = 3
HALF_DECAY = math.exp(-0.5)
MIB = 1 << 20


def from_offset(value, offset, axis="tp"):
    devices = lax.axis_size(axis)
    return lax.ppermute(value, axis, [(i, (i - offset) % devices) for i in range(devices)])


def to_offset(value, offset, axis="tp"):
    return from_offset(value, -offset, axis)


def head_sums(values, same_head):
    high = values.astype(jnp.bfloat16)
    low = (values - high.astype(jnp.float32)).astype(jnp.bfloat16)
    return jnp.dot(high, same_head, preferred_element_type=jnp.float32) + jnp.dot(
        low, same_head, preferred_element_type=jnp.float32
    )


def attention_kernel(
    at,
    p0,
    p1,
    p2,
    p3,
    first_gain,
    share,
    receptance_weight,
    key_weight,
    value_weight,
    decay_down,
    decay_up,
    decay_offset,
    strength_down,
    strength_up,
    removal_scale,
    damping,
    self_weight,
    head_gain,
    output_weight,
    state,
    o0,
    o1,
    o2,
    o3,
    decay_out,
    removal_out,
    along_out,
    value_out,
    blended_out,
    vectors,
    results,
):
    sequences, columns = decay_out.shape
    heads, width = self_weight.shape
    block = p0.shape[1]
    places = [pl.multiple_of(lax.rem(at[0] + k, 4) * block, block) for k in range(4)]
    present = [p[:sequences, :].astype(jnp.float32) for p in (p0, p1, p2, p3)]
    prior = [p[sequences:, :].astype(jnp.float32) for p in (p0, p1, p2, p3)]
    squares = sum(jnp.sum(x * x, axis=1, keepdims=True) for x in present)
    scale = lax.rsqrt(squares / (4 * block) + NORM_EPS)
    weights = (receptance_weight, key_weight, value_weight, decay_down, strength_down)
    sums = [None] * 5
    for place, x, b in zip(places, present, prior):
        rows = pl.ds(place, block)
        normed = x * scale * first_gain[:, rows]
        change = b - normed
        for m, weight in enumerate(weights):
            moved = (normed + change * share[m : m + 1, rows]).astype(jnp.bfloat16)
            part = jnp.dot(moved, weight[rows, :], preferred_element_type=jnp.float32)
            sums[m] = part if sums[m] is None else sums[m] + part
    receptance, key, value, decay_low, strength_low = sums
    own = pl.ds(pl.multiple_of(at[0] * columns, columns), columns)
    decay_pre = decay_offset[...] + jnp.dot(
        jnp.tanh(decay_low).astype(jnp.bfloat16),
        decay_up[:, own],
        preferred_element_type=jnp.float32,
    )
    decay = jnp.exp(-HALF_DECAY * jax.nn.sigmoid(decay_pre))
    alpha = jax.nn.sigmoid(
        jnp.dot(
            strength_low.astype(jnp.bfloat16),
            strength_up[:, own],
            preferred_element_type=jnp.float32,
        )
    )
    lane = lax.broadcasted_iota(jnp.int32, (columns, columns), 1) // width
    row = lax.broadcasted_iota(jnp.int32, (columns, columns), 0) // width
    same_head = (lane == row).astype(jnp.bfloat16)
    removal = key * removal_scale[...]
    removal = removal * lax.rsqrt(head_sums(removal * removal, same_head) + KEY_EPS)
    blended = key * (1.0 + (alpha - 1.0) * damping[...])
    removed = removal * alpha
    pair = 2 * width
    rows_each = 2 * heads
    for v, vector in enumerate((removal, decay * receptance)):
        for h in range(heads):
            two = vector[:, h // 2 * pair : h // 2 * pair + pair]
            vectors[pl.ds(v * heads + h, sequences, stride=rows_each), :] = (
                pltpu.roll(two, width, 1) if h % 2 else two
            )
    for s in range(sequences):
        rows = pl.ds(s * rows_each, rows_each)
        found = lax.dot_general(
            vectors[rows, :][:, :width].astype(jnp.bfloat16),
            state[s].astype(jnp.bfloat16),
            (((1,), (1,)), ((), ())),
            preferred_element_type=jnp.float32,
        )
        for c in range(heads // 2):
            results[c, rows, :] = found[:, c * pair : (c + 1) * pair]
    first_of_two = lax.broadcasted_iota(jnp.int32, (sequences, pair), 1) < width

    def of_vector(v):
        parts = []
        for c in range(heads // 2):
            one, other = (
                results[c, pl.ds(v * heads + 2 * c + i, sequences, stride=rows_each), :]
                for i in (0, 1)
            )
            parts.append(jnp.where(first_of_two, one, other))
        return jnp.concatenate(parts, axis=1)

    along, kept = of_vector(0), of_vector(1)
    gains = jnp.concatenate([self_weight[h : h + 1, :] for h in range(heads)], axis=1)
    readout = (
        kept
        - along * head_sums(removed * receptance, same_head)
        + value * head_sums(blended * receptance, same_head)
    )
    centered = readout - head_sums(readout, same_head) / width
    variance = head_sums(centered * centered, same_head) / width
    mixed = (
        centered * lax.rsqrt(variance + GROUP_EPS) * head_gain[...]
        + head_sums(receptance * blended * gains, same_head) * value
    ).astype(jnp.bfloat16)
    for place, o in zip(places, (o0, o1, o2, o3)):
        o[...] = jnp.dot(
            mixed, output_weight[:, pl.ds(place, block)], preferred_element_type=jnp.float32
        ).astype(jnp.bfloat16)
    decay_out[...] = decay
    removal_out[...] = removed
    along_out[...] = along
    value_out[...] = value
    blended_out[...] = blended


def stack_kernel(first, second, out, sems):
    height = first.shape[0]
    copies = [
        pltpu.make_async_copy(first, out.at[pl.ds(0, height)], sems.at[0]),
        pltpu.make_async_copy(second, out.at[pl.ds(height, height)], sems.at[1]),
    ]
    for copy in copies:
        copy.start()
    for copy in copies:
        copy.wait()


def fetch_kernel(*refs):
    count = len(refs) // 2
    sems = refs[-1]
    copies = [
        pltpu.make_async_copy(refs[i], refs[count + i], sems.at[i]) for i in range(count)
    ]
    for copy in copies:
        copy.start()
    for copy in copies:
        copy.wait()


def from_hbm(kernel, name, shapes, count, limit):
    call = pl.pallas_call(
        kernel,
        out_shape=shapes,
        in_specs=[pl.BlockSpec(memory_space=pltpu.HBM)] * count,
        out_specs=jax.tree.map(lambda _: pl.BlockSpec(memory_space=pltpu.VMEM), shapes),
        scratch_shapes=[pltpu.SemaphoreType.DMA((count,))],
        compiler_params=pltpu.CompilerParams(vmem_limit_bytes=limit * MIB),
        name=name,
    )
    return lambda *values: call(
        *[pltpu.with_memory_space_constraint(value, pltpu.HBM) for value in values]
    )


def hidden_kernel(at, x0, x1, x2, x3, gain, gate_weight, up_weight, out):
    pieces = (x0, x1, x2, x3)
    width = x0.shape[1]
    places = [lax.rem(at[0] + k, 4) * width for k in range(4)]
    floats = [x[...].astype(jnp.float32) for x in pieces]
    squares = sum(jnp.sum(f * f, axis=1, keepdims=True) for f in floats)
    scale = lax.rsqrt(squares / (4 * width) + NORM_EPS)
    gate = jnp.zeros(out.shape, jnp.float32)
    up = jnp.zeros(out.shape, jnp.float32)
    for f, place in zip(floats, places):
        rows = pl.ds(pl.multiple_of(place, width), width)
        x = (f * scale * gain[:, rows]).astype(jnp.bfloat16)
        gate = gate + jnp.dot(x, gate_weight[rows, :], preferred_element_type=jnp.float32)
        up = up + jnp.dot(x, up_weight[rows, :], preferred_element_type=jnp.float32)
    gate = jnp.minimum(gate, GATE_LIMIT)
    up = jnp.clip(up, -GATE_LIMIT, GATE_LIMIT)
    out[...] = ((up + 1.0) * gate * jax.nn.sigmoid(GATE_SLOPE * gate)).astype(jnp.bfloat16)


def down_kernel(at, activation, down_weight, o0, o1, o2, o3):
    block = o0.shape[1]
    for k, o in enumerate((o0, o1, o2, o3)):
        place = pl.multiple_of(lax.rem(at[0] + k, 4) * block, block)
        o[...] = jnp.dot(
            activation[...],
            down_weight[:, pl.ds(place, block)],
            preferred_element_type=jnp.float32,
        ).astype(jnp.bfloat16)


def local_call(kernel, name, shapes, limit, scratch=()):
    def call(at, *operands):
        in_vmem = pl.BlockSpec(memory_space=pltpu.VMEM)
        return pl.pallas_call(
            kernel,
            out_shape=shapes,
            in_specs=[pl.BlockSpec(memory_space=pltpu.SMEM)] + [in_vmem] * len(operands),
            out_specs=jax.tree.map(lambda _: in_vmem, shapes),
            scratch_shapes=scratch,
            compiler_params=pltpu.CompilerParams(vmem_limit_bytes=limit * MIB),
            name=name,
        )(at, *operands)

    return call


def shards(
    tokens,
    previous,
    first_norm_gain,
    token_shift_share,
    receptance_weight,
    key_weight,
    value_weight,
    decay_down_map,
    decay_up_map,
    decay_offset,
    strength_down_map,
    strength_up_map,
    removal_key_scale,
    key_damping,
    self_term_weight,
    head_norm_gain,
    output_weight,
    state,
    second_norm_gain,
    routes,
    chosen_expert_weight,
    expert_gate_weight,
    expert_up_weight,
    expert_down_weight,
):
    at = lax.axis_index("tp")[None]
    sequences, own_columns = tokens.shape
    head_columns = receptance_weight.shape[1]
    float32 = lambda *shape: jax.ShapeDtypeStruct(shape, jnp.float32)
    bfloat16 = lambda *shape: jax.ShapeDtypeStruct(shape, jnp.bfloat16)
    both = from_hbm(
        stack_kernel, "stack", jax.ShapeDtypeStruct((2 * sequences, own_columns), tokens.dtype), 2, 1
    )(tokens, previous)
    row_pieces = [both] + [from_offset(both, k) for k in (1, 2, 3)]

    vector = lambda value: value[None, :]
    needed = (
        vector(first_norm_gain),
        token_shift_share,
        receptance_weight,
        key_weight,
        value_weight,
        decay_down_map,
        decay_up_map,
        vector(decay_offset),
        strength_down_map,
        strength_up_map,
        vector(removal_key_scale),
        vector(key_damping),
        self_term_weight,
        vector(head_norm_gain),
        output_weight,
        state.reshape(sequences, head_columns, state.shape[3]),
    )
    needed = from_hbm(
        fetch_kernel,
        "fetch",
        [jax.ShapeDtypeStruct(a.shape, a.dtype) for a in needed],
        len(needed),
        16,
    )(*needed)

    experts = expert_gate_weight.shape[0] * lax.axis_size("ep")
    ids = jnp.arange(experts, dtype=jnp.int32)
    hits = routes[:, :, None] == ids[None, None, :]
    named = jnp.sum(hits.astype(jnp.float32), axis=1)
    earlier = jnp.tril(jnp.ones((sequences, sequences), jnp.float32), -1)
    ranking = jnp.dot(earlier, named)
    weight_of = jnp.sum(jnp.where(hits, chosen_expert_weight[:, :, None], 0.0), axis=1)
    slots = [(ranking == c) & (named > 0) for c in range(CAPACITY)]
    dispatch = jnp.concatenate([s.astype(jnp.bfloat16) for s in slots], axis=1)
    combine = jnp.concatenate([jnp.where(s, weight_of, 0.0) for s in slots], axis=1)

    *head_terms, decay, removed, along, value, blended = local_call(
        attention_kernel,
        "attention",
        [bfloat16(sequences, own_columns)] * 4 + [float32(sequences, head_columns)] * 5,
        24,
        [
            pltpu.VMEM((8 * sequences, 128), jnp.float32),
            pltpu.VMEM((2, 8 * sequences, 128), jnp.float32),
        ],
    )(
        at,
        *row_pieces,
        *needed,
    )
    by_heads = lambda value: value.reshape(state.shape[:3])
    new_state = (
        state * by_heads(decay)[:, :, None, :]
        - by_heads(along)[..., None] * by_heads(removed)[:, :, None, :]
        + by_heads(value)[..., None] * by_heads(blended)[:, :, None, :]
    )
    arrived = [head_terms[0]] + [to_offset(head_terms[k], k) for k in (1, 2, 3)]
    residual = tokens.astype(jnp.float32) + sum(a.astype(jnp.float32) for a in arrived)

    outgoing = lax.dot_general(
        dispatch,
        residual.astype(jnp.bfloat16),
        (((0,), (0,)), ((), ())),
        preferred_element_type=jnp.float32,
    ).astype(jnp.bfloat16)
    outgoing = outgoing.reshape(CAPACITY, experts, own_columns)
    came = lax.all_to_all(outgoing, "ep", split_axis=1, concat_axis=1, tiled=True)
    own_rows = came.reshape(CAPACITY * experts, own_columns)
    row_pieces = [own_rows] + [from_offset(own_rows, k) for k in (1, 2, 3)]
    activation = local_call(
        hidden_kernel, "hidden", bfloat16(own_rows.shape[0], expert_gate_weight.shape[2]), 12
    )(
        at,
        *row_pieces,
        vector(second_norm_gain),
        expert_gate_weight[0],
        expert_up_weight[0],
    )
    down_terms = local_call(
        down_kernel, "down", [bfloat16(own_rows.shape[0], own_columns)] * 4, 8
    )(at, activation, expert_down_weight[0])
    arrived = [down_terms[0]] + [to_offset(down_terms[k], k) for k in (1, 2, 3)]
    shares = sum(a.astype(jnp.float32) for a in arrived).astype(jnp.bfloat16)
    shares = shares.reshape(CAPACITY, experts, own_columns)
    returned = lax.all_to_all(shares, "ep", split_axis=1, concat_axis=1, tiled=True)
    returned = returned.reshape(CAPACITY * experts, own_columns)
    high = combine.astype(jnp.bfloat16)
    low = (combine - high.astype(jnp.float32)).astype(jnp.bfloat16)
    weighted = jnp.dot(
        jnp.concatenate([high, low], axis=0), returned, preferred_element_type=jnp.float32
    )
    layer_out = (residual + weighted[:sequences] + weighted[sequences:]).astype(jnp.bfloat16)
    return (layer_out, new_state)


def solution(mesh):
    in_specs = (
        P("ep", "tp"),
        P("ep", "tp"),
        P(),
        P(),
        P(None, "tp"),
        P(None, "tp"),
        P(None, "tp"),
        P(),
        P(),
        P("tp"),
        P(),
        P(),
        P("tp"),
        P("tp"),
        P("tp", None),
        P("tp"),
        P("tp", None),
        P("ep", "tp", None, None),
        P(),
        P("ep", None),
        P("ep", None),
        P("ep", None, "tp"),
        P("ep", None, "tp"),
        P("ep", "tp", None),
    )
    out_specs = (P("ep", "tp"), P("ep", "tp", None, None))
    return jax.shard_map(shards, mesh=mesh, in_specs=in_specs, out_specs=out_specs, check_vma=False)
```

time: 127 us -> 95.8 us (0.75)
  matrix products: 12.4 us -> 0.66 us
  local copies, waits for them, and re-layouts: 12.4 us -> 1.61 us
  starting transfers between devices: 26.4 us -> 17.8 us
  Pallas kernels: 5.75 us -> 8.57 us
  other arithmetic: 10.4 us -> 7.62 us
  waiting for transfers between devices: 29.6 us -> 30.9 us
    dot_general x8 -> x0, matrix products: 11.2 us -> none  [the longest x5 6.19 us: project(): return jnp.dot(inputs, weight, preferred_element_type=jnp.float32)]
    ppermute x15 -> x12, starting transfers between devices: 19.3 us -> 13.1 us  [from_offset(): lax.ppermute(value, axis, [(i, (i - offset) % devices) for i in range(dev...]
    unnamed x55 -> x10, local copies, waits for them, and re-layouts: 3.97 us -> 0.03 us
    pallas_call x2 -> x5, Pallas kernels: 5.75 us -> 8.57 us  [the longest x2 4.94 us: from_hbm(): call(*[pltpu.with_memory_space_constraint(value, pltpu.HBM) for value in...]
    all_to_all x1, starting transfers between devices: 7.05 us -> 4.72 us  [shards(): lax.all_to_all(shares, 'ep', split_axis=1, concat_axis=1, tiled=True)]
    mul x3 -> x5, local copies, waits for them, and re-layouts: 2.28 us -> 0.46 us  [the longest x2 0.18 us: shards(): by_heads(along)[..., None] * by_heads(removed)[:, :, None, :]]
    dynamic_slice x3 -> x0, local copies, waits for them, and re-layouts: 1.67 us -> none  [columns_of(): lax.dynamic_slice_in_dim(value, lax.rem(at + k, 4) * own_columns, own_col...]
    ppermute x15 -> x12, waiting for transfers between devices: 22.5 us -> 23.7 us  [from_offset(): lax.ppermute(value, axis, [(i, (i - offset) % devices) for i in range(dev...]
  transfers between devices with their start and end apart: 16 -> 13, of which waited for: 9 -> 9; matrix products, arithmetic and copies ran while one was open for 11% -> 8% of each run, Pallas kernels for 3% -> 4%
where the time goes in v2:
time: 95.8 us; the launch traced here: 95.4 us
  waiting for transfers between devices  30.9 us (32%)
  blocking collectives  27.5 us (29%)
  starting transfers between devices  17.8 us (19%)
  Pallas kernels  8.57 us (9%)
  other arithmetic  7.62 us (8%)
  local copies, waits for them, and re-layouts  1.61 us (2%)
    all_to_all x1, blocking collectives, shards(): lax.all_to_all(outgoing, 'ep', split_axis=1, concat_axis=1, tiled=True)  27.5 us
    ppermute x12, waiting for transfers between devices, from_offset(): lax.ppermute(value, axis, [(i, (i - offset) % devices) for i in range(dev...  23.7 us
    ppermute x12, starting transfers between devices, from_offset(): lax.ppermute(value, axis, [(i, (i - offset) % devices) for i in range(dev...  13.1 us
    all_to_all x1, waiting for transfers between devices, shards(): lax.all_to_all(shares, 'ep', split_axis=1, concat_axis=1, tiled=True)  7.19 us
    add x1, other arithmetic, shards(): state * by_heads(decay)[:, :, None, :]  5.89 us
    pallas_call x2, Pallas kernels, from_hbm(): call(*[pltpu.with_memory_space_constraint(value, pltpu.HBM) for value in...  4.94 us
    all_to_all x1, starting transfers between devices, shards(): lax.all_to_all(shares, 'ep', split_axis=1, concat_axis=1, tiled=True)  4.72 us
    pallas_call x3, Pallas kernels, call(): pl.pallas_call(kernel, out_shape=shapes, in_specs=[pl.BlockSpec(memory_sp...  3.63 us
  transfers between devices with their start and end apart: 13, of which 9 were waited for; matrix products, arithmetic and copies ran while one was open for 8% of the time, Pallas kernels for 4%

profile of v2, /device:TPU:1, one launch (start us, length us, event | category | flops | bytes accessed | tf_op | source)
XLA Modules:
  0.0 95.4 jit_solution(1621288650394594810)
XLA Ops:
  0.6 0.8 stack.1.p0
  1.4 3.4 %collective-permute-start = (bf16[64,512]{1,0:T(8,128)(2,1)S(1)}, bf16[64,512]{1,0:T(8,128)(2,1)S(1)}, u32[]{:S(2)}, u32[]{:S(2)}) collective-permute-start(bf16[64,512]{1,0:T(8,128)(2,1)S(1)} %stack.1.p0), channel_id=1, source_target_pairs={{0,3},{1,0},{2,1},{3,2},{4,7},{5,4},{6,5},{7,6},{8,11},{9,8},{10,9... | collective-permute-start | bytes 196616 | tf_op jit(solution)/shard_map/ppermute | solution.py:22
  4.8 0.5 collective-permute-start.1
  5.3 0.6 collective-permute-start.2
  5.9 0.8 select_reduce_fusion
  6.7 0.2 broadcast_select_fusion.2
  6.9 4.2 %fetch.1 = (f32[1,2048]{1,0:T(1,128)S(1)}, f32[5,2048]{1,0:T(8,128)S(1)}, bf16[2048,256]{1,0:T(8,128)(2,1)S(1)}, bf16[2048,256]{1,0:T(8,128)(2,1)S(1)}, bf16[204...) custom-call(f32[1,2048]{1,0:T(1,128)} %bitcast.29, ...), custom_call_target="tpu_custom_call" | custom-call | tf_op jit(solution)/shard_map/fetch/pallas_call | solution.py:199
  11.2 2.5 %attention.1 = (bf16[32,512]{1,0:T(8,128)(2,1)S(1)}, bf16[32,512]{1,0:T(8,128)(2,1)S(1)}, bf16[32,512]{1,0:T(8,128)(2,1)S(1)}, bf16[32,512]{1,0:T(8,128)(2,1)S(1...) custom-call(s32[1]{0:T(128)} %bitcast.at, ...), custom_call_target="tpu_custom_call" | custom-call | tf_op jit(solution)/shard_map/attention/pallas_call | solution.py:237
  13.6 1.6 %collective-permute-start.3 = (bf16[32,512]{1,0:T(8,128)(2,1)S(1)}, bf16[32,512]{1,0:T(8,128)(2,1)S(1)}, u32[]{:S(2)}, u32[]{:S(2)}) collective-permute-start(bf16[32,512]{1,0:T(8,128)(2,1)S(1)} %get-tuple-element.48), channel_id=1, source_target_pairs={{0,1},{1,2},{2,3},{3,0},{4,5},{5,6},{6,7},{7,4},{8,9},{9,10},{10,1... | collective-permute-start | bytes 98312 | tf_op jit(solution)/shard_map/ppermute | solution.py:22
  15.2 1.7 %collective-permute-start.4 = (bf16[32,512]{1,0:T(8,128)(2,1)S(1)}, bf16[32,512]{1,0:T(8,128)(2,1)S(1)}, u32[]{:S(2)}, u32[]{:S(2)}) collective-permute-start(bf16[32,512]{1,0:T(8,128)(2,1)S(1)} %get-tuple-element.49), channel_id=1, source_target_pairs={{0,2},{1,3},{2,0},{3,1},{4,6},{5,7},{6,4},{7,5},{8,10},{9,11},{10,... | collective-permute-start | bytes 98312 | tf_op jit(solution)/shard_map/ppermute | solution.py:22
  17.0 0.8 collective-permute-start.5
  17.8 1.8 %collective-permute-done.4 = bf16[32,512]{1,0:T(8,128)(2,1)S(1)} collective-permute-done((bf16[32,512]{1,0:T(8,128)(2,1)S(1)}, bf16[32,512]{1,0:T(8,128)(2,1)S(1)}, u32[]{:S(2)}, u32[]{:S(2)}) %collective-permute-start.4) | collective-permute-done | bytes 32800 | tf_op jit(solution)/shard_map/ppermute | solution.py:22
  19.5 0.5 collective-permute-done.5
  20.0 0.3 convolution_convert_fusion
  20.5 27.5 %all_to_all.10 = bf16[3,64,512]{2,0,1:T(4,128)(2,1)S(1)} all-to-all(bf16[3,64,512]{2,0,1:T(4,128)(2,1)S(1)} %copy.39), channel_id=1, replica_groups=mesh['ep'=64,'tp'=4] {'ep'}, dimensions={1} | all-to-all | bytes 393216 | tf_op jit(solution)/shard_map/all_to_all | solution.py:354
  48.0 1.8 %collective-permute-start.6 = (bf16[192,512]{1,0:T(8,128)(2,1)S(1)}, bf16[192,512]{1,0:T(8,128)(2,1)S(1)}, u32[]{:S(2)}, u32[]{:S(2)}) collective-permute-start(bf16[192,512]{1,0:T(8,128)(2,1)S(1)} %bitcast.20), channel_id=1, source_target_pairs={{0,3},{1,0},{2,1},{3,2},{4,7},{5,4},{6,5},{7,6},{8,11},{9,8},{10,9... | collective-permute-start | bytes 589832 | tf_op jit(solution)/shard_map/ppermute | solution.py:22
  49.9 0.6 collective-permute-start.8
  50.5 3.8 %collective-permute-done.6.x1 = bf16[192,512]{1,0:T(8,128)(2,1)S(1)} collective-permute-done((bf16[192,512]{1,0:T(8,128)(2,1)S(1)}, bf16[192,512]{1,0:T(8,128)(2,1)S(1)}, u32[]{:S(2)}, u32[]{:S(2)}) %collective-permute-start.6) | collective-permute-done | bytes 196640 | tf_op jit(solution)/shard_map/ppermute | solution.py:22
  54.3 3.0 %collective-permute-done.7.x2 = bf16[192,512]{1,0:T(8,128)(2,1)S(1)} collective-permute-done((bf16[192,512]{1,0:T(8,128)(2,1)S(1)}, bf16[192,512]{1,0:T(8,128)(2,1)S(1)}, u32[]{:S(2)}, u32[]{:S(2)}) %collective-permute-start.7) | collective-permute-done | bytes 196640 | tf_op jit(solution)/shard_map/ppermute | solution.py:22
  57.3 4.6 %collective-permute-done.8.x3 = bf16[192,512]{1,0:T(8,128)(2,1)S(1)} collective-permute-done((bf16[192,512]{1,0:T(8,128)(2,1)S(1)}, bf16[192,512]{1,0:T(8,128)(2,1)S(1)}, u32[]{:S(2)}, u32[]{:S(2)}) %collective-permute-start.8) | collective-permute-done | bytes 196640 | tf_op jit(solution)/shard_map/ppermute | solution.py:22
  62.0 0.8 hidden.1.activation
  62.8 0.4 down.1
  63.2 0.6 collective-permute-start.10
  63.8 1.4 %collective-permute-start.9 = (bf16[192,512]{1,0:T(8,128)(2,1)S(1)}, bf16[192,512]{1,0:T(8,128)(2,1)S(1)}, u32[]{:S(2)}, u32[]{:S(2)}) collective-permute-start(bf16[192,512]{1,0:T(8,128)(2,1)S(1)} %get-tuple-element.52), channel_id=1, source_target_pairs={{0,1},{1,2},{2,3},{3,0},{4,5},{5,6},{6,7},{7,4},{8,9},{9,10},{10,1... | collective-permute-start | bytes 589832 | tf_op jit(solution)/shard_map/ppermute | solution.py:22
  65.8 4.7 %collective-permute-done.10 = bf16[192,512]{1,0:T(8,128)(2,1)S(1)} collective-permute-done((bf16[192,512]{1,0:T(8,128)(2,1)S(1)}, bf16[192,512]{1,0:T(8,128)(2,1)S(1)}, u32[]{:S(2)}, u32[]{:S(2)}) %collective-permute-start.10) | collective-permute-done | bytes 196640 | tf_op jit(solution)/shard_map/ppermute | solution.py:22
  70.6 1.7 %collective-permute-done.11 = bf16[192,512]{1,0:T(8,128)(2,1)S(1)} collective-permute-done((bf16[192,512]{1,0:T(8,128)(2,1)S(1)}, bf16[192,512]{1,0:T(8,128)(2,1)S(1)}, u32[]{:S(2)}, u32[]{:S(2)}) %collective-permute-start.11) | collective-permute-done | bytes 196640 | tf_op jit(solution)/shard_map/ppermute | solution.py:22
  72.2 3.5 %collective-permute-done.9 = bf16[192,512]{1,0:T(8,128)(2,1)S(1)} collective-permute-done((bf16[192,512]{1,0:T(8,128)(2,1)S(1)}, bf16[192,512]{1,0:T(8,128)(2,1)S(1)}, u32[]{:S(2)}, u32[]{:S(2)}) %collective-permute-start.9) | collective-permute-done | bytes 196640 | tf_op jit(solution)/shard_map/ppermute | solution.py:22
  75.9 0.9 copy.41
  76.8 4.7 %all-to-all-start.1 = ((bf16[3,64,512]{2,0,1:T(4,128)(2,1)}), bf16[3,64,512]{2,0,1:T(4,128)(2,1)S(1)}, u32[]{:S(2)}, u32[]{:S(2)}) async-start(bf16[3,64,512]{2,0,1:T(4,128)(2,1)} %copy.41), calls=%async_computation.1 | async-start | bytes 524288 | tf_op jit(solution)/shard_map/all_to_all | solution.py:372
  81.5 5.9 %multiply_add_fusion = f32[32,4,64,64]{3,2,1,0:T(8,128)} fusion(f32[32,4,64,64]{3,2,1,0:T(8,128)} %param.41, f32[32,4,64]{2,1,0:T(4,128)S(1)} %mul.54, f32[32,4,64]{2,1,0:T(4,128)S(1)} %mul.52, f32[32,4,64]{2,1,0:T(4,128)S(1)} %mul.49, f32[32,4,64]{2,1,0:T(4,128)S(1)} %mul.47, f32[32,4,64]{2,1,0:T(4,128)S(1)} %mul.44), kind=kLoop, calls=%fused_computation | loop fusion | flops 2621440 | bytes 4358144 | tf_op jit(solution)/shard_map/add | solution.py:340
  87.4 7.2 %all-to-all-done.1 = bf16[3,64,512]{2,0,1:T(4,128)(2,1)S(1)} async-done(((bf16[3,64,512]{2,0,1:T(4,128)(2,1)}), bf16[3,64,512]{2,0,1:T(4,128)(2,1)S(1)}, u32[]{:S(2)}, u32[]{:S(2)}) %all-to-all-start.1) | async-done | bytes 196640 | tf_op jit(solution)/shard_map/all_to_all | solution.py:372
  94.8 0.7 fusion
  (30 shorter events, 1.3 us)
Async XLA Ops:
  1.4 9.7 %collective-permute-start = (bf16[64,512]{1,0:T(8,128)(2,1)S(1)}, bf16[64,512]{1,0:T(8,128)(2,1)S(1)}, u32[]{:S(2)}, u32[]{:S(2)}) collective-permute-start(bf16[64,512]{1,0:T(8,128)(2,1)S(1)} %stack.1.p0), channel_id=1, source_target_pairs={{0,3},{1,0},{2,1},{3,2},{4,7},{5,4},{6,5},{7,6},{8,11},{9,8},{10,9... | collective-permute-start | bytes 196616 | tf_op jit(solution)/shard_map/ppermute | solution.py:22
  4.8 6.3 %collective-permute-start.1 = (bf16[64,512]{1,0:T(8,128)(2,1)S(1)}, bf16[64,512]{1,0:T(8,128)(2,1)S(1)}, u32[]{:S(2)}, u32[]{:S(2)}) collective-permute-start(bf16[64,512]{1,0:T(8,128)(2,1)S(1)} %stack.1.p0), channel_id=1, source_target_pairs={{0,2},{1,3},{2,0},{3,1},{4,6},{5,7},{6,4},{7,5},{8,10},{9,11},{10,... | collective-permute-start | bytes 196616 | tf_op jit(solution)/shard_map/ppermute | solution.py:22
  5.3 5.8 %collective-permute-start.2 = (bf16[64,512]{1,0:T(8,128)(2,1)S(1)}, bf16[64,512]{1,0:T(8,128)(2,1)S(1)}, u32[]{:S(2)}, u32[]{:S(2)}) collective-permute-start(bf16[64,512]{1,0:T(8,128)(2,1)S(1)} %stack.1.p0), channel_id=1, source_target_pairs={{0,1},{1,2},{2,3},{3,0},{4,5},{5,6},{6,7},{7,4},{8,9},{9,10},{10,1... | collective-permute-start | bytes 196616 | tf_op jit(solution)/shard_map/ppermute | solution.py:22
  11.1 8.9 %copy-start.4 = (bf16[32,512]{1,0:T(8,128)(2,1)S(1)}, bf16[32,512]{1,0:T(8,128)(2,1)}, u32[]{:S(2)}) copy-start(bf16[32,512]{1,0:T(8,128)(2,1)} %first.1) | copy-start | bytes 98308
  11.1 50.8 %copy-start = (bf16[1,2048,256]{2,1,0:T(8,128)(2,1)S(1)}, bf16[1,2048,256]{2,1,0:T(8,128)(2,1)}, u32[]{:S(2)}) copy-start(bf16[1,2048,256]{2,1,0:T(8,128)(2,1)} %param.45) | copy-start | bytes 3145732
  11.2 50.8 %copy-start.1 = (bf16[1,2048,256]{2,1,0:T(8,128)(2,1)S(1)}, bf16[1,2048,256]{2,1,0:T(8,128)(2,1)}, u32[]{:S(2)}) copy-start(bf16[1,2048,256]{2,1,0:T(8,128)(2,1)} %param.46) | copy-start | bytes 3145732
  11.2 50.8 %copy-start.3 = (f32[2048]{0:T(1024)S(1)}, f32[2048]{0:T(1024)}, u32[]{:S(2)}) copy-start(f32[2048]{0:T(1024)} %param.42) | copy-start | bytes 24580
  13.6 49.1 %copy-start.2 = (bf16[1,256,2048]{2,1,0:T(8,128)(2,1)S(1)}, bf16[1,256,2048]{2,1,0:T(8,128)(2,1)}, u32[]{:S(2)}) copy-start(bf16[1,256,2048]{2,1,0:T(8,128)(2,1)} %param.47) | copy-start | bytes 3145732
  13.6 4.1 %collective-permute-start.3 = (bf16[32,512]{1,0:T(8,128)(2,1)S(1)}, bf16[32,512]{1,0:T(8,128)(2,1)S(1)}, u32[]{:S(2)}, u32[]{:S(2)}) collective-permute-start(bf16[32,512]{1,0:T(8,128)(2,1)S(1)} %get-tuple-element.48), channel_id=1, source_target_pairs={{0,1},{1,2},{2,3},{3,0},{4,5},{5,6},{6,7},{7,4},{8,9},{9,10},{10,1... | collective-permute-start | bytes 98312 | tf_op jit(solution)/shard_map/ppermute | solution.py:22
  15.2 4.3 %collective-permute-start.4 = (bf16[32,512]{1,0:T(8,128)(2,1)S(1)}, bf16[32,512]{1,0:T(8,128)(2,1)S(1)}, u32[]{:S(2)}, u32[]{:S(2)}) collective-permute-start(bf16[32,512]{1,0:T(8,128)(2,1)S(1)} %get-tuple-element.49), channel_id=1, source_target_pairs={{0,2},{1,3},{2,0},{3,1},{4,6},{5,7},{6,4},{7,5},{8,10},{9,11},{10,... | collective-permute-start | bytes 98312 | tf_op jit(solution)/shard_map/ppermute | solution.py:22
  17.0 3.1 %collective-permute-start.5 = (bf16[32,512]{1,0:T(8,128)(2,1)S(1)}, bf16[32,512]{1,0:T(8,128)(2,1)S(1)}, u32[]{:S(2)}, u32[]{:S(2)}) collective-permute-start(bf16[32,512]{1,0:T(8,128)(2,1)S(1)} %get-tuple-element.50), channel_id=1, source_target_pairs={{0,3},{1,0},{2,1},{3,2},{4,7},{5,4},{6,5},{7,6},{8,11},{9,8},{10,9... | collective-permute-start | bytes 98312 | tf_op jit(solution)/shard_map/ppermute | solution.py:22
  48.0 6.3 %collective-permute-start.6 = (bf16[192,512]{1,0:T(8,128)(2,1)S(1)}, bf16[192,512]{1,0:T(8,128)(2,1)S(1)}, u32[]{:S(2)}, u32[]{:S(2)}) collective-permute-start(bf16[192,512]{1,0:T(8,128)(2,1)S(1)} %bitcast.20), channel_id=1, source_target_pairs={{0,3},{1,0},{2,1},{3,2},{4,7},{5,4},{6,5},{7,6},{8,11},{9,8},{10,9... | collective-permute-start | bytes 589832 | tf_op jit(solution)/shard_map/ppermute | solution.py:22
  49.8 7.5 %collective-permute-start.7 = (bf16[192,512]{1,0:T(8,128)(2,1)S(1)}, bf16[192,512]{1,0:T(8,128)(2,1)S(1)}, u32[]{:S(2)}, u32[]{:S(2)}) collective-permute-start(bf16[192,512]{1,0:T(8,128)(2,1)S(1)} %bitcast.21), channel_id=1, source_target_pairs={{0,2},{1,3},{2,0},{3,1},{4,6},{5,7},{6,4},{7,5},{8,10},{9,11},{10,... | collective-permute-start | bytes 589832 | tf_op jit(solution)/shard_map/ppermute | solution.py:22
  49.9 12.0 %collective-permute-start.8 = (bf16[192,512]{1,0:T(8,128)(2,1)S(1)}, bf16[192,512]{1,0:T(8,128)(2,1)S(1)}, u32[]{:S(2)}, u32[]{:S(2)}) collective-permute-start(bf16[192,512]{1,0:T(8,128)(2,1)S(1)} %bitcast.22), channel_id=1, source_target_pairs={{0,1},{1,2},{2,3},{3,0},{4,5},{5,6},{6,7},{7,4},{8,9},{9,10},{10,1... | collective-permute-start | bytes 589832 | tf_op jit(solution)/shard_map/ppermute | solution.py:22
  63.2 7.4 %collective-permute-start.10 = (bf16[192,512]{1,0:T(8,128)(2,1)S(1)}, bf16[192,512]{1,0:T(8,128)(2,1)S(1)}, u32[]{:S(2)}, u32[]{:S(2)}) collective-permute-start(bf16[192,512]{1,0:T(8,128)(2,1)S(1)} %get-tuple-element.53), channel_id=1, source_target_pairs={{0,2},{1,3},{2,0},{3,1},{4,6},{5,7},{6,4},{7,5},{8,10},{9,11},{10,... | collective-permute-start | bytes 589832 | tf_op jit(solution)/shard_map/ppermute | solution.py:22
  63.7 8.5 %collective-permute-start.11 = (bf16[192,512]{1,0:T(8,128)(2,1)S(1)}, bf16[192,512]{1,0:T(8,128)(2,1)S(1)}, u32[]{:S(2)}, u32[]{:S(2)}) collective-permute-start(bf16[192,512]{1,0:T(8,128)(2,1)S(1)} %get-tuple-element.54), channel_id=1, source_target_pairs={{0,3},{1,0},{2,1},{3,2},{4,7},{5,4},{6,5},{7,6},{8,11},{9,8},{10,9... | collective-permute-start | bytes 589832 | tf_op jit(solution)/shard_map/ppermute | solution.py:22
  63.8 12.0 %collective-permute-start.9 = (bf16[192,512]{1,0:T(8,128)(2,1)S(1)}, bf16[192,512]{1,0:T(8,128)(2,1)S(1)}, u32[]{:S(2)}, u32[]{:S(2)}) collective-permute-start(bf16[192,512]{1,0:T(8,128)(2,1)S(1)} %get-tuple-element.52), channel_id=1, source_target_pairs={{0,1},{1,2},{2,3},{3,0},{4,5},{5,6},{6,7},{7,4},{8,9},{9,10},{10,1... | collective-permute-start | bytes 589832 | tf_op jit(solution)/shard_map/ppermute | solution.py:22
  76.8 17.8 %all-to-all-start.1 = ((bf16[3,64,512]{2,0,1:T(4,128)(2,1)}), bf16[3,64,512]{2,0,1:T(4,128)(2,1)S(1)}, u32[]{:S(2)}, u32[]{:S(2)}) async-start(bf16[3,64,512]{2,0,1:T(4,128)(2,1)} %copy.41), calls=%async_computation.1 | async-start | bytes 524288 | tf_op jit(solution)/shard_map/all_to_all | solution.py:372

commit v3 on v2

--- a/solution.py
+++ b/solution.py
@@ -24,6 +24,16 @@
 
 def to_offset(value, offset, axis="tp"):
     return from_offset(value, -offset, axis)
+
+
+def gathered(value):
+    pieces = {k: from_offset(value, k) for k in (1, 3, 2)}
+    return [value, pieces[1], pieces[2], pieces[3]]
+
+
+def scattered(values):
+    pieces = {k: to_offset(values[k], k) for k in (1, 3, 2)}
+    return [values[0], pieces[1], pieces[2], pieces[3]]
 
 
 def head_sums(values, same_head):
@@ -54,8 +64,8 @@
     damping,
     self_weight,
     head_gain,
-    output_weight,
-    state,
+    output_weight_hbm,
+    state_hbm,
     o0,
     o1,
     o2,
@@ -67,7 +77,14 @@
     blended_out,
     vectors,
     results,
+    output_weight,
+    state,
+    sems,
 ):
+    state_copy = pltpu.make_async_copy(state_hbm, state, sems.at[0])
+    state_copy.start()
+    weight_copy = pltpu.make_async_copy(output_weight_hbm, output_weight, sems.at[1])
+    weight_copy.start()
     sequences, columns = decay_out.shape
     heads, width = self_weight.shape
     block = p0.shape[1]
@@ -116,6 +133,7 @@
             vectors[pl.ds(v * heads + h, sequences, stride=rows_each), :] = (
                 pltpu.roll(two, width, 1) if h % 2 else two
             )
+    state_copy.wait()
     for s in range(sequences):
         rows = pl.ds(s * rows_each, rows_each)
         found = lax.dot_general(
@@ -151,6 +169,7 @@
         centered * lax.rsqrt(variance + GROUP_EPS) * head_gain[...]
         + head_sums(receptance * blended * gains, same_head) * value
     ).astype(jnp.bfloat16)
+    weight_copy.wait()
     for place, o in zip(places, (o0, o1, o2, o3)):
         o[...] = jnp.dot(
             mixed, output_weight[:, pl.ds(place, block)], preferred_element_type=jnp.float32
@@ -231,13 +250,19 @@
         ).astype(jnp.bfloat16)
 
 
-def local_call(kernel, name, shapes, limit, scratch=()):
+def local_call(kernel, name, shapes, limit, scratch=(), left=0):
     def call(at, *operands):
         in_vmem = pl.BlockSpec(memory_space=pltpu.VMEM)
+        count = len(operands) - left
+        operands = operands[:count] + tuple(
+            pltpu.with_memory_space_constraint(value, pltpu.HBM) for value in operands[count:]
+        )
         return pl.pallas_call(
             kernel,
             out_shape=shapes,
-            in_specs=[pl.BlockSpec(memory_space=pltpu.SMEM)] + [in_vmem] * len(operands),
+            in_specs=[pl.BlockSpec(memory_space=pltpu.SMEM)]
+            + [in_vmem] * count
+            + [pl.BlockSpec(memory_space=pltpu.HBM)] * left,
             out_specs=jax.tree.map(lambda _: in_vmem, shapes),
             scratch_shapes=scratch,
             compiler_params=pltpu.CompilerParams(vmem_limit_bytes=limit * MIB),
@@ -281,7 +306,7 @@
     both = from_hbm(
         stack_kernel, "stack", jax.ShapeDtypeStruct((2 * sequences, own_columns), tokens.dtype), 2, 1
     )(tokens, previous)
-    row_pieces = [both] + [from_offset(both, k) for k in (1, 2, 3)]
+    row_pieces = gathered(both)
 
     vector = lambda value: value[None, :]
     needed = (
@@ -299,15 +324,13 @@
         vector(key_damping),
         self_term_weight,
         vector(head_norm_gain),
-        output_weight,
-        state.reshape(sequences, head_columns, state.shape[3]),
     )
     needed = from_hbm(
         fetch_kernel,
         "fetch",
         [jax.ShapeDtypeStruct(a.shape, a.dtype) for a in needed],
         len(needed),
-        16,
+        12,
     )(*needed)
 
     experts = expert_gate_weight.shape[0] * lax.axis_size("ep")
@@ -321,27 +344,22 @@
     dispatch = jnp.concatenate([s.astype(jnp.bfloat16) for s in slots], axis=1)
     combine = jnp.concatenate([jnp.where(s, weight_of, 0.0) for s in slots], axis=1)
 
+    flat_state = state.reshape(sequences, head_columns, state.shape[3])
     *head_terms, decay, removed, along, value, blended = local_call(
         attention_kernel,
         "attention",
         [bfloat16(sequences, own_columns)] * 4 + [float32(sequences, head_columns)] * 5,
-        24,
+        16,
         [
             pltpu.VMEM((8 * sequences, 128), jnp.float32),
             pltpu.VMEM((2, 8 * sequences, 128), jnp.float32),
+            pltpu.VMEM(output_weight.shape, output_weight.dtype),
+            pltpu.VMEM(flat_state.shape, flat_state.dtype),
+            pltpu.SemaphoreType.DMA((2,)),
         ],
-    )(
-        at,
-        *row_pieces,
-        *needed,
-    )
-    by_heads = lambda value: value.reshape(state.shape[:3])
-    new_state = (
-        state * by_heads(decay)[:, :, None, :]
-        - by_heads(along)[..., None] * by_heads(removed)[:, :, None, :]
-        + by_heads(value)[..., None] * by_heads(blended)[:, :, None, :]
-    )
-    arrived = [head_terms[0]] + [to_offset(head_terms[k], k) for k in (1, 2, 3)]
+        left=2,
+    )(at, *row_pieces, *needed, output_weight, flat_state)
+    arrived = scattered(head_terms)
     residual = tokens.astype(jnp.float32) + sum(a.astype(jnp.float32) for a in arrived)
 
     outgoing = lax.dot_general(
@@ -351,9 +369,22 @@
         preferred_element_type=jnp.float32,
     ).astype(jnp.bfloat16)
     outgoing = outgoing.reshape(CAPACITY, experts, own_columns)
+    high = combine.astype(jnp.bfloat16)
+    low = (combine - high.astype(jnp.float32)).astype(jnp.bfloat16)
+    outgoing, high, low = lax.optimization_barrier((outgoing, high, low))
     came = lax.all_to_all(outgoing, "ep", split_axis=1, concat_axis=1, tiled=True)
+    came, decay, removed, along, value, blended = lax.optimization_barrier(
+        (came, decay, removed, along, value, blended)
+    )
     own_rows = came.reshape(CAPACITY * experts, own_columns)
-    row_pieces = [own_rows] + [from_offset(own_rows, k) for k in (1, 2, 3)]
+    row_pieces = gathered(own_rows)
+    by_heads = lambda value: value.reshape(state.shape[:3])
+    new_state = (
+        state * by_heads(decay)[:, :, None, :]
+        - by_heads(along)[..., None] * by_heads(removed)[:, :, None, :]
+        + by_heads(value)[..., None] * by_heads(blended)[:, :, None, :]
+    )
+    new_state, *row_pieces = lax.optimization_barrier((new_state, *row_pieces))
     activation = local_call(
         hidden_kernel, "hidden", bfloat16(own_rows.shape[0], expert_gate_weight.shape[2]), 12
     )(
@@ -366,13 +397,11 @@
     down_terms = local_call(
         down_kernel, "down", [bfloat16(own_rows.shape[0], own_columns)] * 4, 8
     )(at, activation, expert_down_weight[0])
-    arrived = [down_terms[0]] + [to_offset(down_terms[k], k) for k in (1, 2, 3)]
+    arrived = scattered(down_terms)
     shares = sum(a.astype(jnp.float32) for a in arrived).astype(jnp.bfloat16)
     shares = shares.reshape(CAPACITY, experts, own_columns)
     returned = lax.all_to_all(shares, "ep", split_axis=1, concat_axis=1, tiled=True)
     returned = returned.reshape(CAPACITY * experts, own_columns)
-    high = combine.astype(jnp.bfloat16)
-    low = (combine - high.astype(jnp.float32)).astype(jnp.bfloat16)
     weighted = jnp.dot(
         jnp.concatenate([high, low], axis=0), returned, preferred_element_type=jnp.float32
     )

time: 95.8 us -> 96.1 us (level)
  blocking collectives: 27.5 us -> 45.4 us
  waiting for transfers between devices: 30.9 us -> 18 us
  starting transfers between devices: 17.8 us -> 13.4 us
    all_to_all x0 -> x1, blocking collectives: none -> 17.6 us  [shards(): lax.all_to_all(shares, 'ep', split_axis=1, concat_axis=1, tiled=True)]
    all_to_all x1 -> x0, waiting for transfers between devices: 7.19 us -> none  [shards(): lax.all_to_all(shares, 'ep', split_axis=1, concat_axis=1, tiled=True)]
    ppermute x12, waiting for transfers between devices: 23.7 us -> 18 us  [from_offset(): lax.ppermute(value, axis, [(i, (i - offset) % devices) for i in range(dev...]
    all_to_all x1 -> x0, starting transfers between devices: 4.72 us -> none  [shards(): lax.all_to_all(shares, 'ep', split_axis=1, concat_axis=1, tiled=True)]
    pallas_call x3, Pallas kernels: 3.63 us -> 5.51 us  [call(): pl.pallas_call(kernel, out_shape=shapes, in_specs=[pl.BlockSpec(memory_sp...]
    pallas_call x2, Pallas kernels: 4.94 us -> 3.31 us  [from_hbm(): call(*[pltpu.with_memory_space_constraint(value, pltpu.HBM) for value in...]
  transfers between devices with their start and end apart: 13 -> 12, of which waited for: 9 -> 9; matrix products, arithmetic and copies ran while one was open for 8% -> 8% of each run, Pallas kernels for 4% -> 3%
where the time goes in v3:
time: 96.1 us; the launch traced here: 95.8 us
  blocking collectives  45.4 us (47%)
  waiting for transfers between devices  18 us (19%)
  starting transfers between devices  13.4 us (14%)
  Pallas kernels  8.82 us (9%)
  other arithmetic  7.77 us (8%)
    all_to_all x1, blocking collectives, shards(): lax.all_to_all(outgoing, 'ep', split_axis=1, concat_axis=1, tiled=True)  27.7 us
    ppermute x12, waiting for transfers between devices, from_offset(): lax.ppermute(value, axis, [(i, (i - offset) % devices) for i in range(dev...  18 us
    all_to_all x1, blocking collectives, shards(): lax.all_to_all(shares, 'ep', split_axis=1, concat_axis=1, tiled=True)  17.6 us
    ppermute x12, starting transfers between devices, from_offset(): lax.ppermute(value, axis, [(i, (i - offset) % devices) for i in range(dev...  13.4 us
    add x1, other arithmetic, shards(): state * by_heads(decay)[:, :, None, :]  6.04 us
    pallas_call x3, Pallas kernels, call(): pl.pallas_call(kernel, out_shape=shapes, in_specs=[pl.BlockSpec(memory_sp...  5.51 us
    pallas_call x2, Pallas kernels, from_hbm(): call(*[pltpu.with_memory_space_constraint(value, pltpu.HBM) for value in...  3.31 us
  transfers between devices with their start and end apart: 12, of which 9 were waited for; matrix products, arithmetic and copies ran while one was open for 8% of the time, Pallas kernels for 3%

profile of v3, /device:TPU:1, one launch (start us, length us, event | category | flops | bytes accessed | tf_op | source)
XLA Modules:
  0.0 95.8 jit_solution(14929622482493965905)
XLA Ops:
  0.6 0.8 stack.1.p0
  1.4 3.4 %collective-permute-start = (bf16[64,512]{1,0:T(8,128)(2,1)S(1)}, bf16[64,512]{1,0:T(8,128)(2,1)S(1)}, u32[]{:S(2)}, u32[]{:S(2)}) collective-permute-start(bf16[64,512]{1,0:T(8,128)(2,1)S(1)} %stack.1.p0), channel_id=1, source_target_pairs={{0,3},{1,0},{2,1},{3,2},{4,7},{5,4},{6,5},{7,6},{8,11},{9,8},{10,9... | collective-permute-start | bytes 196616 | tf_op jit(solution)/shard_map/ppermute | solution.py:22
  4.8 0.5 collective-permute-start.1
  5.3 0.6 collective-permute-start.2
  5.9 0.8 select_reduce_fusion
  6.7 0.2 broadcast_select_fusion.2
  7.0 2.5 %fetch.1 = (f32[1,2048]{1,0:T(1,128)S(1)}, f32[5,2048]{1,0:T(8,128)S(1)}, bf16[2048,256]{1,0:T(8,128)(2,1)S(1)}, bf16[2048,256]{1,0:T(8,128)(2,1)S(1)}, bf16[204...) custom-call(f32[1,2048]{1,0:T(1,128)} %bitcast.29, ...), custom_call_target="tpu_custom_call" | custom-call | tf_op jit(solution)/shard_map/fetch/pallas_call | solution.py:218
  9.6 0.6 collective-permute-done.2.p3
  10.1 4.3 %attention.1 = (bf16[32,512]{1,0:T(8,128)(2,1)S(1)}, bf16[32,512]{1,0:T(8,128)(2,1)S(1)}, bf16[32,512]{1,0:T(8,128)(2,1)S(1)}, bf16[32,512]{1,0:T(8,128)(2,1)S(1...) custom-call(s32[1]{0:T(128)} %bitcast.at, ...), custom_call_target="tpu_custom_call" | custom-call | tf_op jit(solution)/shard_map/attention/pallas_call | solution.py:260
  14.5 1.1 %collective-permute-start.3 = (bf16[32,512]{1,0:T(8,128)(2,1)S(1)}, bf16[32,512]{1,0:T(8,128)(2,1)S(1)}, u32[]{:S(2)}, u32[]{:S(2)}) collective-permute-start(bf16[32,512]{1,0:T(8,128)(2,1)S(1)} %get-tuple-element.58), channel_id=1, source_target_pairs={{0,1},{1,2},{2,3},{3,0},{4,5},{5,6},{6,7},{7,4},{8,9},{9,10},{10,1... | collective-permute-start | bytes 98312 | tf_op jit(solution)/shard_map/ppermute | solution.py:22
  15.5 1.7 %collective-permute-start.4 = (bf16[32,512]{1,0:T(8,128)(2,1)S(1)}, bf16[32,512]{1,0:T(8,128)(2,1)S(1)}, u32[]{:S(2)}, u32[]{:S(2)}) collective-permute-start(bf16[32,512]{1,0:T(8,128)(2,1)S(1)} %get-tuple-element.59), channel_id=1, source_target_pairs={{0,2},{1,3},{2,0},{3,1},{4,6},{5,7},{6,4},{7,5},{8,10},{9,11},{10,... | collective-permute-start | bytes 98312 | tf_op jit(solution)/shard_map/ppermute | solution.py:22
  17.3 0.9 collective-permute-start.5
  18.2 0.3 collective-permute-done.3
  18.5 1.3 %collective-permute-done.4 = bf16[32,512]{1,0:T(8,128)(2,1)S(1)} collective-permute-done((bf16[32,512]{1,0:T(8,128)(2,1)S(1)}, bf16[32,512]{1,0:T(8,128)(2,1)S(1)}, u32[]{:S(2)}, u32[]{:S(2)}) %collective-permute-start.4) | collective-permute-done | bytes 32800 | tf_op jit(solution)/shard_map/ppermute | solution.py:22
  19.8 0.2 collective-permute-done.5
  20.0 0.3 convolution_convert_fusion
  20.5 27.7 %all_to_all.10 = bf16[3,64,512]{2,0,1:T(4,128)(2,1)S(1)} all-to-all(bf16[3,64,512]{2,0,1:T(4,128)(2,1)S(1)} %copy.39), channel_id=1, replica_groups=mesh['ep'=64,'tp'=4] {'ep'}, dimensions={1} | all-to-all | bytes 393216 | tf_op jit(solution)/shard_map/all_to_all | solution.py:375
  48.3 2.3 %collective-permute-start.6 = (bf16[192,512]{1,0:T(8,128)(2,1)S(1)}, bf16[192,512]{1,0:T(8,128)(2,1)S(1)}, u32[]{:S(2)}, u32[]{:S(2)}) collective-permute-start(bf16[192,512]{1,0:T(8,128)(2,1)S(1)} %bitcast.20), channel_id=1, source_target_pairs={{0,3},{1,0},{2,1},{3,2},{4,7},{5,4},{6,5},{7,6},{8,11},{9,8},{10,9... | collective-permute-start | bytes 589832 | tf_op jit(solution)/shard_map/ppermute | solution.py:22
  50.6 0.7 collective-permute-start.7
  51.8 6.0 %multiply_add_fusion = f32[32,4,64,64]{3,2,1,0:T(8,128)} fusion(f32[32,4,64,64]{3,2,1,0:T(8,128)} %param.41, f32[32,4,64]{2,1,0:T(4,128)S(1)} %mul.54, f32[32,4,64]{2,1,0:T(4,128)S(1)} %mul.52, f32[32,4,64]{2,1,0:T(4,128)S(1)} %mul.49, f32[32,4,64]{2,1,0:T(4,128)S(1)} %mul.47, f32[32,4,64]{2,1,0:T(4,128)S(1)} %mul.44), kind=kLoop, calls=%fused_computation | loop fusion | flops 2621440 | bytes 4358144 | tf_op jit(solution)/shard_map/add | solution.py:383
  57.9 0.2 collective-permute-done.7.x2
  58.1 5.1 %collective-permute-done.8.x3 = bf16[192,512]{1,0:T(8,128)(2,1)S(1)} collective-permute-done((bf16[192,512]{1,0:T(8,128)(2,1)S(1)}, bf16[192,512]{1,0:T(8,128)(2,1)S(1)}, u32[]{:S(2)}, u32[]{:S(2)}) %collective-permute-start.8) | collective-permute-done | bytes 196640 | tf_op jit(solution)/shard_map/ppermute | solution.py:22
  63.2 0.8 hidden.1.activation
  64.0 0.4 down.1
  64.4 0.8 collective-permute-start.10
  65.2 1.4 %collective-permute-start.9 = (bf16[192,512]{1,0:T(8,128)(2,1)S(1)}, bf16[192,512]{1,0:T(8,128)(2,1)S(1)}, u32[]{:S(2)}, u32[]{:S(2)}) collective-permute-start(bf16[192,512]{1,0:T(8,128)(2,1)S(1)} %get-tuple-element.80), channel_id=1, source_target_pairs={{0,1},{1,2},{2,3},{3,0},{4,5},{5,6},{6,7},{7,4},{8,9},{9,10},{10,1... | collective-permute-start | bytes 589832 | tf_op jit(solution)/shard_map/ppermute | solution.py:22
  66.6 5.3 %collective-permute-done.10 = bf16[192,512]{1,0:T(8,128)(2,1)S(1)} collective-permute-done((bf16[192,512]{1,0:T(8,128)(2,1)S(1)}, bf16[192,512]{1,0:T(8,128)(2,1)S(1)}, u32[]{:S(2)}, u32[]{:S(2)}) %collective-permute-start.10) | collective-permute-done | bytes 196640 | tf_op jit(solution)/shard_map/ppermute | solution.py:22
  72.0 0.7 collective-permute-done.11
  72.7 4.3 %collective-permute-done.9 = bf16[192,512]{1,0:T(8,128)(2,1)S(1)} collective-permute-done((bf16[192,512]{1,0:T(8,128)(2,1)S(1)}, bf16[192,512]{1,0:T(8,128)(2,1)S(1)}, u32[]{:S(2)}, u32[]{:S(2)}) %collective-permute-start.9) | collective-permute-done | bytes 196640 | tf_op jit(solution)/shard_map/ppermute | solution.py:22
  77.1 0.2 copy.41
  77.3 17.6 %all_to_all.11 = bf16[3,64,512]{2,0,1:T(4,128)(2,1)S(1)} all-to-all(bf16[3,64,512]{2,0,1:T(4,128)(2,1)S(1)} %copy.41), channel_id=1, replica_groups=mesh['ep'=64,'tp'=4] {'ep'}, dimensions={1} | all-to-all | bytes 393216 | tf_op jit(solution)/shard_map/all_to_all | solution.py:403
  95.1 0.7 fusion
  (29 shorter events, 1.2 us)
Async XLA Ops:
  1.4 8.1 %collective-permute-start = (bf16[64,512]{1,0:T(8,128)(2,1)S(1)}, bf16[64,512]{1,0:T(8,128)(2,1)S(1)}, u32[]{:S(2)}, u32[]{:S(2)}) collective-permute-start(bf16[64,512]{1,0:T(8,128)(2,1)S(1)} %stack.1.p0), channel_id=1, source_target_pairs={{0,3},{1,0},{2,1},{3,2},{4,7},{5,4},{6,5},{7,6},{8,11},{9,8},{10,9... | collective-permute-start | bytes 196616 | tf_op jit(solution)/shard_map/ppermute | solution.py:22
  4.8 4.8 %collective-permute-start.1 = (bf16[64,512]{1,0:T(8,128)(2,1)S(1)}, bf16[64,512]{1,0:T(8,128)(2,1)S(1)}, u32[]{:S(2)}, u32[]{:S(2)}) collective-permute-start(bf16[64,512]{1,0:T(8,128)(2,1)S(1)} %stack.1.p0), channel_id=1, source_target_pairs={{0,2},{1,3},{2,0},{3,1},{4,6},{5,7},{6,4},{7,5},{8,10},{9,11},{10,... | collective-permute-start | bytes 196616 | tf_op jit(solution)/shard_map/ppermute | solution.py:22
  5.3 4.8 %collective-permute-start.2 = (bf16[64,512]{1,0:T(8,128)(2,1)S(1)}, bf16[64,512]{1,0:T(8,128)(2,1)S(1)}, u32[]{:S(2)}, u32[]{:S(2)}) collective-permute-start(bf16[64,512]{1,0:T(8,128)(2,1)S(1)} %stack.1.p0), channel_id=1, source_target_pairs={{0,1},{1,2},{2,3},{3,0},{4,5},{5,6},{6,7},{7,4},{8,9},{9,10},{10,1... | collective-permute-start | bytes 196616 | tf_op jit(solution)/shard_map/ppermute | solution.py:22
  10.1 9.9 %copy-start.4 = (bf16[32,512]{1,0:T(8,128)(2,1)S(1)}, bf16[32,512]{1,0:T(8,128)(2,1)}, u32[]{:S(2)}) copy-start(bf16[32,512]{1,0:T(8,128)(2,1)} %first.1) | copy-start | bytes 98308
  14.5 4.1 %collective-permute-start.3 = (bf16[32,512]{1,0:T(8,128)(2,1)S(1)}, bf16[32,512]{1,0:T(8,128)(2,1)S(1)}, u32[]{:S(2)}, u32[]{:S(2)}) collective-permute-start(bf16[32,512]{1,0:T(8,128)(2,1)S(1)} %get-tuple-element.58), channel_id=1, source_target_pairs={{0,1},{1,2},{2,3},{3,0},{4,5},{5,6},{6,7},{7,4},{8,9},{9,10},{10,1... | collective-permute-start | bytes 98312 | tf_op jit(solution)/shard_map/ppermute | solution.py:22
  15.5 4.3 %collective-permute-start.4 = (bf16[32,512]{1,0:T(8,128)(2,1)S(1)}, bf16[32,512]{1,0:T(8,128)(2,1)S(1)}, u32[]{:S(2)}, u32[]{:S(2)}) collective-permute-start(bf16[32,512]{1,0:T(8,128)(2,1)S(1)} %get-tuple-element.59), channel_id=1, source_target_pairs={{0,2},{1,3},{2,0},{3,1},{4,6},{5,7},{6,4},{7,5},{8,10},{9,11},{10,... | collective-permute-start | bytes 98312 | tf_op jit(solution)/shard_map/ppermute | solution.py:22
  17.3 2.8 %collective-permute-start.5 = (bf16[32,512]{1,0:T(8,128)(2,1)S(1)}, bf16[32,512]{1,0:T(8,128)(2,1)S(1)}, u32[]{:S(2)}, u32[]{:S(2)}) collective-permute-start(bf16[32,512]{1,0:T(8,128)(2,1)S(1)} %get-tuple-element.60), channel_id=1, source_target_pairs={{0,3},{1,0},{2,1},{3,2},{4,7},{5,4},{6,5},{7,6},{8,11},{9,8},{10,9... | collective-permute-start | bytes 98312 | tf_op jit(solution)/shard_map/ppermute | solution.py:22
  48.3 9.5 %collective-permute-start.6 = (bf16[192,512]{1,0:T(8,128)(2,1)S(1)}, bf16[192,512]{1,0:T(8,128)(2,1)S(1)}, u32[]{:S(2)}, u32[]{:S(2)}) collective-permute-start(bf16[192,512]{1,0:T(8,128)(2,1)S(1)} %bitcast.20), channel_id=1, source_target_pairs={{0,3},{1,0},{2,1},{3,2},{4,7},{5,4},{6,5},{7,6},{8,11},{9,8},{10,9... | collective-permute-start | bytes 589832 | tf_op jit(solution)/shard_map/ppermute | solution.py:22
  50.6 7.5 %collective-permute-start.7 = (bf16[192,512]{1,0:T(8,128)(2,1)S(1)}, bf16[192,512]{1,0:T(8,128)(2,1)S(1)}, u32[]{:S(2)}, u32[]{:S(2)}) collective-permute-start(bf16[192,512]{1,0:T(8,128)(2,1)S(1)} %bitcast.21), channel_id=1, source_target_pairs={{0,2},{1,3},{2,0},{3,1},{4,6},{5,7},{6,4},{7,5},{8,10},{9,11},{10,... | collective-permute-start | bytes 589832 | tf_op jit(solution)/shard_map/ppermute | solution.py:22
  51.3 11.8 %collective-permute-start.8 = (bf16[192,512]{1,0:T(8,128)(2,1)S(1)}, bf16[192,512]{1,0:T(8,128)(2,1)S(1)}, u32[]{:S(2)}, u32[]{:S(2)}) collective-permute-start(bf16[192,512]{1,0:T(8,128)(2,1)S(1)} %bitcast.22), channel_id=1, source_target_pairs={{0,1},{1,2},{2,3},{3,0},{4,5},{5,6},{6,7},{7,4},{8,9},{9,10},{10,1... | collective-permute-start | bytes 589832 | tf_op jit(solution)/shard_map/ppermute | solution.py:22
  51.8 11.3 %copy-start = (bf16[1,2048,256]{2,1,0:T(8,128)(2,1)S(1)}, bf16[1,2048,256]{2,1,0:T(8,128)(2,1)}, u32[]{:S(2)}) copy-start(bf16[1,2048,256]{2,1,0:T(8,128)(2,1)} %param.45) | copy-start | bytes 3145732
  51.8 11.3 %copy-start.1 = (bf16[1,2048,256]{2,1,0:T(8,128)(2,1)S(1)}, bf16[1,2048,256]{2,1,0:T(8,128)(2,1)}, u32[]{:S(2)}) copy-start(bf16[1,2048,256]{2,1,0:T(8,128)(2,1)} %param.46) | copy-start | bytes 3145732
  51.8 11.3 %copy-start.3 = (f32[2048]{0:T(1024)S(1)}, f32[2048]{0:T(1024)}, u32[]{:S(2)}) copy-start(f32[2048]{0:T(1024)} %param.42) | copy-start | bytes 24580
  51.8 12.1 %copy-start.2 = (bf16[1,256,2048]{2,1,0:T(8,128)(2,1)S(1)}, bf16[1,256,2048]{2,1,0:T(8,128)(2,1)}, u32[]{:S(2)}) copy-start(bf16[1,256,2048]{2,1,0:T(8,128)(2,1)} %param.47) | copy-start | bytes 3145732
  64.4 7.6 %collective-permute-start.10 = (bf16[192,512]{1,0:T(8,128)(2,1)S(1)}, bf16[192,512]{1,0:T(8,128)(2,1)S(1)}, u32[]{:S(2)}, u32[]{:S(2)}) collective-permute-start(bf16[192,512]{1,0:T(8,128)(2,1)S(1)} %get-tuple-element.81), channel_id=1, source_target_pairs={{0,2},{1,3},{2,0},{3,1},{4,6},{5,7},{6,4},{7,5},{8,10},{9,11},{10,... | collective-permute-start | bytes 589832 | tf_op jit(solution)/shard_map/ppermute | solution.py:22
  65.2 7.5 %collective-permute-start.11 = (bf16[192,512]{1,0:T(8,128)(2,1)S(1)}, bf16[192,512]{1,0:T(8,128)(2,1)S(1)}, u32[]{:S(2)}, u32[]{:S(2)}) collective-permute-start(bf16[192,512]{1,0:T(8,128)(2,1)S(1)} %get-tuple-element.82), channel_id=1, source_target_pairs={{0,3},{1,0},{2,1},{3,2},{4,7},{5,4},{6,5},{7,6},{8,11},{9,8},{10,9... | collective-permute-start | bytes 589832 | tf_op jit(solution)/shard_map/ppermute | solution.py:22
  65.2 11.8 %collective-permute-start.9 = (bf16[192,512]{1,0:T(8,128)(2,1)S(1)}, bf16[192,512]{1,0:T(8,128)(2,1)S(1)}, u32[]{:S(2)}, u32[]{:S(2)}) collective-permute-start(bf16[192,512]{1,0:T(8,128)(2,1)S(1)} %get-tuple-element.80), channel_id=1, source_target_pairs={{0,1},{1,2},{2,3},{3,0},{4,5},{5,6},{6,7},{7,4},{8,9},{9,10},{10,1... | collective-permute-start | bytes 589832 | tf_op jit(solution)/shard_map/ppermute | solution.py:22

commit v4 on v3

--- a/solution.py
+++ b/solution.py
@@ -6,6 +6,7 @@
 from jax.experimental import pallas as pl
 from jax.experimental.pallas import tpu as pltpu
 from jax.sharding import PartitionSpec as P
+
 
 NORM_EPS = 1e-06
 GROUP_EPS = 0.00064
@@ -17,22 +18,18 @@
 MIB = 1 << 20
 
 
-def from_offset(value, offset, axis="tp"):
-    devices = lax.axis_size(axis)
-    return lax.ppermute(value, axis, [(i, (i - offset) % devices) for i in range(devices)])
-
-
-def to_offset(value, offset, axis="tp"):
-    return from_offset(value, -offset, axis)
+def from_offset(value, offset):
+    devices = lax.axis_size("tp")
+    return lax.ppermute(value, "tp", [(i, (i - offset) % devices) for i in range(devices)])
 
 
 def gathered(value):
-    pieces = {k: from_offset(value, k) for k in (1, 3, 2)}
+    pieces = {k: from_offset(value, k) for k in (2, 3, 1)}
     return [value, pieces[1], pieces[2], pieces[3]]
 
 
 def scattered(values):
-    pieces = {k: to_offset(values[k], k) for k in (1, 3, 2)}
+    pieces = {k: from_offset(values[k], -k) for k in (2, 1, 3)}
     return [values[0], pieces[1], pieces[2], pieces[3]]
 
 
@@ -64,6 +61,7 @@
     damping,
     self_weight,
     head_gain,
+    state_head,
     output_weight_hbm,
     state_hbm,
     o0,
@@ -71,21 +69,22 @@
     o2,
     o3,
     decay_out,
-    removal_out,
     along_out,
     value_out,
+    removal_out,
     blended_out,
     vectors,
     results,
     output_weight,
-    state,
+    state_tail,
     sems,
 ):
-    state_copy = pltpu.make_async_copy(state_hbm, state, sems.at[0])
+    half = state_tail.shape[0]
+    state_copy = pltpu.make_async_copy(state_hbm.at[pl.ds(half, half)], state_tail, sems.at[0])
     state_copy.start()
     weight_copy = pltpu.make_async_copy(output_weight_hbm, output_weight, sems.at[1])
     weight_copy.start()
-    sequences, columns = decay_out.shape
+    sequences, columns = along_out.shape
     heads, width = self_weight.shape
     block = p0.shape[1]
     places = [pl.multiple_of(lax.rem(at[0] + k, 4) * block, block) for k in range(4)]
@@ -127,18 +126,22 @@
     removed = removal * alpha
     pair = 2 * width
     rows_each = 2 * heads
+
+    def of_head(vector, h):
+        two = vector[:, h // 2 * pair : h // 2 * pair + pair]
+        return pltpu.roll(two, width, 1) if h % 2 else two
+
     for v, vector in enumerate((removal, decay * receptance)):
         for h in range(heads):
-            two = vector[:, h // 2 * pair : h // 2 * pair + pair]
-            vectors[pl.ds(v * heads + h, sequences, stride=rows_each), :] = (
-                pltpu.roll(two, width, 1) if h % 2 else two
-            )
-    state_copy.wait()
+            vectors[pl.ds(v * heads + h, sequences, stride=rows_each), :] = of_head(vector, h)
     for s in range(sequences):
+        if s == half:
+            state_copy.wait()
+        state = state_head if s < half else state_tail
         rows = pl.ds(s * rows_each, rows_each)
         found = lax.dot_general(
             vectors[rows, :][:, :width].astype(jnp.bfloat16),
-            state[s].astype(jnp.bfloat16),
+            state[s % half].astype(jnp.bfloat16),
             (((1,), (1,)), ((), ())),
             preferred_element_type=jnp.float32,
         )
@@ -174,11 +177,46 @@
         o[...] = jnp.dot(
             mixed, output_weight[:, pl.ds(place, block)], preferred_element_type=jnp.float32
         ).astype(jnp.bfloat16)
-    decay_out[...] = decay
-    removal_out[...] = removed
     along_out[...] = along
     value_out[...] = value
-    blended_out[...] = blended
+    for out, vector in ((decay_out, decay), (removal_out, removed), (blended_out, blended)):
+        for h in range(heads):
+            out[pl.ds(h, sequences, stride=heads), :] = of_head(vector, h)
+
+
+def renew_kernel(
+    decay, removed, blended, along, value, state_hbm, new_state_hbm, state, new_state, sems
+):
+    sequences, columns, width = state.shape
+    heads = columns // width
+    groups = sems.shape[1]
+    each = sequences // groups
+
+    def copies_of(g):
+        part = pl.ds(g * each, each)
+        return (
+            pltpu.make_async_copy(state_hbm.at[part], state.at[part], sems.at[0, g]),
+            pltpu.make_async_copy(new_state.at[part], new_state_hbm.at[part], sems.at[1, g]),
+        )
+
+    copies = [copies_of(g) for g in range(groups)]
+    for arriving, _ in copies:
+        arriving.start()
+    along_columns, value_columns = along[...].T, value[...].T
+    for g, (arriving, leaving) in enumerate(copies):
+        arriving.wait()
+        for s in range(g * each, (g + 1) * each):
+            for h in range(heads):
+                rows = slice(h * width, (h + 1) * width)
+                at = slice(s * heads + h, s * heads + h + 1)
+                new_state[s, rows, :] = (
+                    state[s, rows, :] * decay[at, :width]
+                    - along_columns[rows, s : s + 1] * removed[at, :width]
+                    + value_columns[rows, s : s + 1] * blended[at, :width]
+                )
+        leaving.start()
+    for _, leaving in copies:
+        leaving.wait()
 
 
 def stack_kernel(first, second, out, sems):
@@ -193,38 +231,35 @@
         copy.wait()
 
 
-def fetch_kernel(*refs):
-    count = len(refs) // 2
+def fetch_kernel(at, *refs):
     sems = refs[-1]
+    count = len(sems) - 3
+    *sources, down_weight = refs[: count + 1]
+    wholes, columns = refs[count + 1 : 2 * count + 1], refs[2 * count + 1 : -1]
+    sources[-1] = sources[-1].at[pl.ds(0, wholes[-1].shape[0])]
     copies = [
-        pltpu.make_async_copy(refs[i], refs[count + i], sems.at[i]) for i in range(count)
+        pltpu.make_async_copy(source, whole, sems.at[i])
+        for i, (source, whole) in enumerate(zip(sources, wholes))
     ]
+    for k, piece in enumerate(columns, 1):
+        block = piece.shape[1]
+        place = pl.multiple_of(lax.rem(at[0] + k, 4) * block, block)
+        copies.append(
+            pltpu.make_async_copy(
+                down_weight.at[:, pl.ds(place, block)], piece, sems.at[count + k - 1]
+            )
+        )
     for copy in copies:
         copy.start()
     for copy in copies:
         copy.wait()
 
 
-def from_hbm(kernel, name, shapes, count, limit):
-    call = pl.pallas_call(
-        kernel,
-        out_shape=shapes,
-        in_specs=[pl.BlockSpec(memory_space=pltpu.HBM)] * count,
-        out_specs=jax.tree.map(lambda _: pl.BlockSpec(memory_space=pltpu.VMEM), shapes),
-        scratch_shapes=[pltpu.SemaphoreType.DMA((count,))],
-        compiler_params=pltpu.CompilerParams(vmem_limit_bytes=limit * MIB),
-        name=name,
-    )
-    return lambda *values: call(
-        *[pltpu.with_memory_space_constraint(value, pltpu.HBM) for value in values]
-    )
-
-
-def hidden_kernel(at, x0, x1, x2, x3, gain, gate_weight, up_weight, out):
-    pieces = (x0, x1, x2, x3)
+def hidden_kernel(at, x0, x1, x2, x2_rest, x3, gain, gate_weight, up_weight, out):
+    pieces = (x0[...], x1[...], jnp.concatenate([x2[...], x2_rest[...]], axis=0), x3[...])
     width = x0.shape[1]
     places = [lax.rem(at[0] + k, 4) * width for k in range(4)]
-    floats = [x[...].astype(jnp.float32) for x in pieces]
+    floats = [x.astype(jnp.float32) for x in pieces]
     squares = sum(jnp.sum(f * f, axis=1, keepdims=True) for f in floats)
     scale = lax.rsqrt(squares / (4 * width) + NORM_EPS)
     gate = jnp.zeros(out.shape, jnp.float32)
@@ -239,19 +274,17 @@
     out[...] = ((up + 1.0) * gate * jax.nn.sigmoid(GATE_SLOPE * gate)).astype(jnp.bfloat16)
 
 
-def down_kernel(at, activation, down_weight, o0, o1, o2, o3):
-    block = o0.shape[1]
-    for k, o in enumerate((o0, o1, o2, o3)):
-        place = pl.multiple_of(lax.rem(at[0] + k, 4) * block, block)
-        o[...] = jnp.dot(
-            activation[...],
-            down_weight[:, pl.ds(place, block)],
-            preferred_element_type=jnp.float32,
-        ).astype(jnp.bfloat16)
-
-
-def local_call(kernel, name, shapes, limit, scratch=(), left=0):
-    def call(at, *operands):
+def down_kernel(at, a0, a1, a2, a3, w1, w2, w3, down_weight, out):
+    block = out.shape[1]
+    own = pl.ds(pl.multiple_of(at[0] * block, block), block)
+    total = jnp.dot(a0[...], down_weight[:, own], preferred_element_type=jnp.float32)
+    for a, w in ((a1, w1), (a2, w2), (a3, w3)):
+        total = total + jnp.dot(a[...], w[...], preferred_element_type=jnp.float32)
+    out[...] = total.astype(jnp.bfloat16)
+
+
+def local_call(kernel, shapes, limit, scratch=(), scalars=0, left=0):
+    def call(*operands):
         in_vmem = pl.BlockSpec(memory_space=pltpu.VMEM)
         count = len(operands) - left
         operands = operands[:count] + tuple(
@@ -260,14 +293,13 @@
         return pl.pallas_call(
             kernel,
             out_shape=shapes,
-            in_specs=[pl.BlockSpec(memory_space=pltpu.SMEM)]
-            + [in_vmem] * count
+            in_specs=[pl.BlockSpec(memory_space=pltpu.SMEM)] * scalars
+            + [in_vmem] * (count - scalars)
             + [pl.BlockSpec(memory_space=pltpu.HBM)] * left,
             out_specs=jax.tree.map(lambda _: in_vmem, shapes),
             scratch_shapes=scratch,
             compiler_params=pltpu.CompilerParams(vmem_limit_bytes=limit * MIB),
-            name=name,
-        )(at, *operands)
+        )(*operands)
 
     return call
 
@@ -303,8 +335,12 @@
     head_columns = receptance_weight.shape[1]
     float32 = lambda *shape: jax.ShapeDtypeStruct(shape, jnp.float32)
     bfloat16 = lambda *shape: jax.ShapeDtypeStruct(shape, jnp.bfloat16)
-    both = from_hbm(
-        stack_kernel, "stack", jax.ShapeDtypeStruct((2 * sequences, own_columns), tokens.dtype), 2, 1
+    both = local_call(
+        stack_kernel,
+        jax.ShapeDtypeStruct((2 * sequences, own_columns), tokens.dtype),
+        1,
+        [pltpu.SemaphoreType.DMA((2,))],
+        left=2,
     )(tokens, previous)
     row_pieces = gathered(both)
 
@@ -325,13 +361,17 @@
         self_term_weight,
         vector(head_norm_gain),
     )
-    needed = from_hbm(
+    flat_state = state.reshape(sequences, head_columns, state.shape[3])
+    shapes = [jax.ShapeDtypeStruct(a.shape, a.dtype) for a in needed]
+    shapes.append(float32(sequences // 2, *flat_state.shape[1:]))
+    *needed, down_1, down_2, down_3 = local_call(
         fetch_kernel,
-        "fetch",
-        [jax.ShapeDtypeStruct(a.shape, a.dtype) for a in needed],
-        len(needed),
-        12,
-    )(*needed)
+        shapes + [bfloat16(expert_down_weight.shape[1], own_columns)] * 3,
+        14,
+        [pltpu.SemaphoreType.DMA((len(shapes) + 3,))],
+        scalars=1,
+        left=len(shapes) + 1,
+    )(at, *needed, flat_state, expert_down_weight[0])
 
     experts = expert_gate_weight.shape[0] * lax.axis_size("ep")
     ids = jnp.arange(experts, dtype=jnp.int32)
@@ -344,22 +384,25 @@
     dispatch = jnp.concatenate([s.astype(jnp.bfloat16) for s in slots], axis=1)
     combine = jnp.concatenate([jnp.where(s, weight_of, 0.0) for s in slots], axis=1)
 
-    flat_state = state.reshape(sequences, head_columns, state.shape[3])
-    *head_terms, decay, removed, along, value, blended = local_call(
+    *head_terms, decay, along, value, removed, blended = local_call(
         attention_kernel,
-        "attention",
-        [bfloat16(sequences, own_columns)] * 4 + [float32(sequences, head_columns)] * 5,
+        [bfloat16(sequences, own_columns)] * 4
+        + [float32(sequences * state.shape[1], 128)]
+        + [float32(sequences, head_columns)] * 2
+        + [float32(sequences * state.shape[1], 128)] * 2,
         16,
         [
             pltpu.VMEM((8 * sequences, 128), jnp.float32),
             pltpu.VMEM((2, 8 * sequences, 128), jnp.float32),
             pltpu.VMEM(output_weight.shape, output_weight.dtype),
-            pltpu.VMEM(flat_state.shape, flat_state.dtype),
+            pltpu.VMEM((sequences // 2, *flat_state.shape[1:]), jnp.float32),
             pltpu.SemaphoreType.DMA((2,)),
         ],
+        scalars=1,
         left=2,
     )(at, *row_pieces, *needed, output_weight, flat_state)
     arrived = scattered(head_terms)
+    down_pieces = scattered([None, down_1, down_2, down_3])[1:]
     residual = tokens.astype(jnp.float32) + sum(a.astype(jnp.float32) for a in arrived)
 
     outgoing = lax.dot_general(
@@ -373,32 +416,48 @@
     low = (combine - high.astype(jnp.float32)).astype(jnp.bfloat16)
     outgoing, high, low = lax.optimization_barrier((outgoing, high, low))
     came = lax.all_to_all(outgoing, "ep", split_axis=1, concat_axis=1, tiled=True)
-    came, decay, removed, along, value, blended = lax.optimization_barrier(
-        (came, decay, removed, along, value, blended)
-    )
     own_rows = came.reshape(CAPACITY * experts, own_columns)
-    row_pieces = gathered(own_rows)
-    by_heads = lambda value: value.reshape(state.shape[:3])
-    new_state = (
-        state * by_heads(decay)[:, :, None, :]
-        - by_heads(along)[..., None] * by_heads(removed)[:, :, None, :]
-        + by_heads(value)[..., None] * by_heads(blended)[:, :, None, :]
-    )
-    new_state, *row_pieces = lax.optimization_barrier((new_state, *row_pieces))
+    half = own_rows.shape[0] // 2
+    second = from_offset(own_rows[:half], 2)
+    first = from_offset(own_rows, 1)
+    third = from_offset(own_rows, 3)
+    second_rest = from_offset(first[half:], 1)
     activation = local_call(
-        hidden_kernel, "hidden", bfloat16(own_rows.shape[0], expert_gate_weight.shape[2]), 12
+        hidden_kernel, bfloat16(own_rows.shape[0], expert_gate_weight.shape[2]), 12, scalars=1
     )(
         at,
-        *row_pieces,
+        own_rows,
+        first,
+        second,
+        second_rest,
+        third,
         vector(second_norm_gain),
         expert_gate_weight[0],
         expert_up_weight[0],
     )
-    down_terms = local_call(
-        down_kernel, "down", [bfloat16(own_rows.shape[0], own_columns)] * 4, 8
-    )(at, activation, expert_down_weight[0])
-    arrived = scattered(down_terms)
-    shares = sum(a.astype(jnp.float32) for a in arrived).astype(jnp.bfloat16)
+    activation, *renewing = lax.optimization_barrier(
+        (activation, decay, removed, blended, along, value)
+    )
+    act_pieces = scattered([activation] * 4)
+    new_state = pl.pallas_call(
+        renew_kernel,
+        out_shape=float32(*flat_state.shape),
+        in_specs=[pl.BlockSpec(memory_space=pltpu.VMEM)] * 5
+        + [pl.BlockSpec(memory_space=pltpu.HBM)],
+        out_specs=pl.BlockSpec(memory_space=pltpu.HBM),
+        scratch_shapes=[
+            pltpu.VMEM(flat_state.shape, jnp.float32),
+            pltpu.VMEM(flat_state.shape, jnp.float32),
+            pltpu.SemaphoreType.DMA((2, 8)),
+        ],
+        compiler_params=pltpu.CompilerParams(vmem_limit_bytes=12 * MIB),
+        name="renew",
+    )(*renewing, pltpu.with_memory_space_constraint(flat_state, pltpu.HBM))
+    new_state, *act_pieces = lax.optimization_barrier((new_state, *act_pieces))
+    new_state = new_state.reshape(state.shape)
+    shares = local_call(
+        down_kernel, bfloat16(own_rows.shape[0], own_columns), 8, scalars=1
+    )(at, *act_pieces, *down_pieces, expert_down_weight[0])
     shares = shares.reshape(CAPACITY, experts, own_columns)
     returned = lax.all_to_all(shares, "ep", split_axis=1, concat_axis=1, tiled=True)
     returned = returned.reshape(CAPACITY * experts, own_columns)
@@ -437,4 +496,5 @@
         P("ep", "tp", None),
     )
     out_specs = (P("ep", "tp"), P("ep", "tp", None, None))
+
     return jax.shard_map(shards, mesh=mesh, in_specs=in_specs, out_specs=out_specs, check_vma=False)

time: 96.1 us -> 101 us (1.051)
  starting transfers between devices: 13.4 us -> 21 us
  other arithmetic: 7.77 us -> 1.63 us
  Pallas kernels: 8.82 us -> 13.5 us
  waiting for transfers between devices: 18 us -> 14.7 us
  blocking collectives: 45.4 us -> 48 us
    ppermute x12 -> x16, starting transfers between devices: 13.4 us -> 21 us  [from_offset(): lax.ppermute(value, 'tp', [(i, (i - offset) % devices) for i in range(dev...]
    add x1 -> x0, other arithmetic: 6.04 us -> none  [shards(): state * by_heads(decay)[:, :, None, :]]
    pallas_call x3 -> x5, Pallas kernels: 5.51 us -> 8.82 us  [call(): pl.pallas_call(kernel, out_shape=shapes, in_specs=[pl.BlockSpec(memory_sp...]
    ppermute x12 -> x16, waiting for transfers between devices: 18 us -> 14.7 us  [from_offset(): lax.ppermute(value, 'tp', [(i, (i - offset) % devices) for i in range(dev...]
    all_to_all x1, blocking collectives: 17.6 us -> 20.6 us  [shards(): lax.all_to_all(shares, 'ep', split_axis=1, concat_axis=1, tiled=True)]
    pallas_call x2 -> x1, Pallas kernels: 3.31 us -> 4.72 us  [shards(): pl.pallas_call(renew_kernel, out_shape=float32(*flat_state.shape), in_spe...]
  transfers between devices with their start and end apart: 12 -> 16, of which waited for: 9 -> 4; matrix products, arithmetic and copies ran while one was open for 8% -> 1% of each run, Pallas kernels for 3% -> 9%
where the time goes in v4:
time: 101 us
  blocking collectives  48 us (48%)
  starting transfers between devices  21 us (21%)
  waiting for transfers between devices  14.7 us (15%)
  Pallas kernels  13.5 us (13%)
  other arithmetic  1.63 us (2%)
    all_to_all x1, blocking collectives, shards(): lax.all_to_all(outgoing, 'ep', split_axis=1, concat_axis=1, tiled=True)  27.5 us
    ppermute x16, starting transfers between devices, from_offset(): lax.ppermute(value, 'tp', [(i, (i - offset) % devices) for i in range(dev...  21 us
    all_to_all x1, blocking collectives, shards(): lax.all_to_all(shares, 'ep', split_axis=1, concat_axis=1, tiled=True)  20.6 us
    ppermute x16, waiting for transfers between devices, from_offset(): lax.ppermute(value, 'tp', [(i, (i - offset) % devices) for i in range(dev...  14.7 us
    pallas_call x5, Pallas kernels, call(): pl.pallas_call(kernel, out_shape=shapes, in_specs=[pl.BlockSpec(memory_sp...  8.82 us
    pallas_call x1, Pallas kernels, shards(): pl.pallas_call(renew_kernel, out_shape=float32(*flat_state.shape), in_spe...  4.72 us
  transfers between devices with their start and end apart: 16, of which 4 were waited for; matrix products, arithmetic and copies ran while one was open for 1% of the time, Pallas kernels for 9%

profile of v4, /device:TPU:1, one launch (start us, length us, event | category | flops | bytes accessed | tf_op | source)
XLA Modules:
  0.0 100.9 jit_solution(2954295168445353482)
XLA Ops:
  0.6 0.8 shard_map.239.p0
  1.4 3.4 %collective-permute-start = (bf16[64,512]{1,0:T(8,128)(2,1)S(1)}, bf16[64,512]{1,0:T(8,128)(2,1)S(1)}, u32[]{:S(2)}, u32[]{:S(2)}) collective-permute-start(bf16[64,512]{1,0:T(8,128)(2,1)S(1)} %shard_map.239.p0), channel_id=1, source_target_pairs={{0,3},{1,0},{2,1},{3,2},{4,7},{5,4},{6,5},{7,6},{8,11},{9,8},{10,9... | collective-permute-start | bytes 196616 | tf_op jit(solution)/shard_map/ppermute | solution.py:23
  4.8 0.5 collective-permute-start.1
  5.3 0.6 collective-permute-start.2
  5.9 0.8 select_reduce_fusion
  6.7 0.2 broadcast_select_fusion.2
  7.0 3.4 %shard_map.240 = (f32[1,2048]{1,0:T(1,128)S(1)}, f32[5,2048]{1,0:T(8,128)S(1)}, bf16[2048,256]{1,0:T(8,128)(2,1)S(1)}, bf16[2048,256]{1,0:T(8,128)(2,1)S(1)}, bf...) custom-call(s32[1]{0:T(128)} %bitcast.at, ...), custom_call_target="tpu_custom_call" | custom-call | tf_op jit(solution)/shard_map/pallas_call | solution.py:293
  10.5 3.5 %shard_map.241 = (bf16[32,512]{1,0:T(8,128)(2,1)S(1)}, bf16[32,512]{1,0:T(8,128)(2,1)S(1)}, bf16[32,512]{1,0:T(8,128)(2,1)S(1)}, bf16[32,512]{1,0:T(8,128)(2,1)S...) custom-call(s32[1]{0:T(128)} %bitcast.at, ...), custom_call_target="tpu_custom_call" | custom-call | tf_op jit(solution)/shard_map/pallas_call | solution.py:293
  14.0 1.6 %collective-permute-start.3 = (bf16[32,512]{1,0:T(8,128)(2,1)S(1)}, bf16[32,512]{1,0:T(8,128)(2,1)S(1)}, u32[]{:S(2)}, u32[]{:S(2)}) collective-permute-start(bf16[32,512]{1,0:T(8,128)(2,1)S(1)} %get-tuple-element.59), channel_id=1, source_target_pairs={{0,1},{1,2},{2,3},{3,0},{4,5},{5,6},{6,7},{7,4},{8,9},{9,10},{10,1... | collective-permute-start | bytes 98312 | tf_op jit(solution)/shard_map/ppermute | solution.py:23
  15.6 1.7 %collective-permute-start.4 = (bf16[32,512]{1,0:T(8,128)(2,1)S(1)}, bf16[32,512]{1,0:T(8,128)(2,1)S(1)}, u32[]{:S(2)}, u32[]{:S(2)}) collective-permute-start(bf16[32,512]{1,0:T(8,128)(2,1)S(1)} %get-tuple-element.60), channel_id=1, source_target_pairs={{0,2},{1,3},{2,0},{3,1},{4,6},{5,7},{6,4},{7,5},{8,10},{9,11},{10,... | collective-permute-start | bytes 98312 | tf_op jit(solution)/shard_map/ppermute | solution.py:23
  17.4 0.8 collective-permute-start.5
  18.2 1.7 %collective-permute-done.4 = bf16[32,512]{1,0:T(8,128)(2,1)S(1)} collective-permute-done((bf16[32,512]{1,0:T(8,128)(2,1)S(1)}, bf16[32,512]{1,0:T(8,128)(2,1)S(1)}, u32[]{:S(2)}, u32[]{:S(2)}) %collective-permute-start.4) | collective-permute-done | bytes 32800 | tf_op jit(solution)/shard_map/ppermute | solution.py:23
  19.9 0.5 collective-permute-done.5
  20.4 0.3 convolution_convert_fusion
  20.7 0.2 copy.39
  20.9 27.5 %all_to_all.10 = bf16[3,64,512]{2,0,1:T(4,128)(2,1)S(1)} all-to-all(bf16[3,64,512]{2,0,1:T(4,128)(2,1)S(1)} %copy.39), channel_id=1, replica_groups=mesh['ep'=64,'tp'=4] {'ep'}, dimensions={1} | all-to-all | bytes 393216 | tf_op jit(solution)/shard_map/all_to_all | solution.py:418
  48.4 1.8 %collective-permute-start.6 = (bf16[192,512]{1,0:T(8,128)(2,1)S(1)}, bf16[192,512]{1,0:T(8,128)(2,1)S(1)}, u32[]{:S(2)}, u32[]{:S(2)}) collective-permute-start(bf16[192,512]{1,0:T(8,128)(2,1)S(1)} %bitcast.20), channel_id=1, source_target_pairs={{0,3},{1,0},{2,1},{3,2},{4,7},{5,4},{6,5},{7,6},{8,11},{9,8},{10,9... | collective-permute-start | bytes 589832 | tf_op jit(solution)/shard_map/ppermute | solution.py:23
  50.2 1.4 %collective-permute-start.7 = (bf16[96,512]{1,0:T(8,128)(2,1)S(1)}, bf16[96,512]{1,0:T(8,128)(2,1)S(1)}, u32[]{:S(2)}, u32[]{:S(2)}) collective-permute-start(bf16[96,512]{1,0:T(8,128)(2,1)S(1)} %slice.16), channel_id=1, source_target_pairs={{0,2},{1,3},{2,0},{3,1},{4,6},{5,7},{6,4},{7,5},{8,10},{9,11},{10,... | collective-permute-start | bytes 294920 | tf_op jit(solution)/shard_map/ppermute | solution.py:23
  51.6 3.1 %collective-permute-done.6.x1 = bf16[192,512]{1,0:T(8,128)(2,1)S(1)} collective-permute-done((bf16[192,512]{1,0:T(8,128)(2,1)S(1)}, bf16[192,512]{1,0:T(8,128)(2,1)S(1)}, u32[]{:S(2)}, u32[]{:S(2)}) %collective-permute-start.6) | collective-permute-done | bytes 196640 | tf_op jit(solution)/shard_map/ppermute | solution.py:23
  54.7 3.4 %collective-permute-start.8 = (bf16[96,512]{1,0:T(8,128)(2,1)S(1)}, bf16[96,512]{1,0:T(8,128)(2,1)S(1)}, u32[]{:S(2)}, u32[]{:S(2)}) collective-permute-start(bf16[96,512]{1,0:T(8,128)(2,1)S(1)} %slice.17), channel_id=1, source_target_pairs={{0,3},{1,0},{2,1},{3,2},{4,7},{5,4},{6,5},{7,6},{8,11},{9,8},{10,9... | collective-permute-start | bytes 294920 | tf_op jit(solution)/shard_map/ppermute | solution.py:23
  58.1 1.3 %collective-permute-start.14 = (bf16[256,512]{1,0:T(8,128)(2,1)S(1)}, bf16[256,512]{1,0:T(8,128)(2,1)S(1)}, u32[]{:S(2)}, u32[]{:S(2)}) collective-permute-start(bf16[256,512]{1,0:T(8,128)(2,1)S(1)} %get-tuple-element.81), channel_id=1, source_target_pairs={{0,2},{1,3},{2,0},{3,1},{4,6},{5,7},{6,4},{7,5},{8,10},{9,11},{10,... | collective-permute-start | bytes 786440 | tf_op jit(solution)/shard_map/ppermute | solution.py:23
  59.4 1.4 %collective-permute-start.15 = (bf16[256,512]{1,0:T(8,128)(2,1)S(1)}, bf16[256,512]{1,0:T(8,128)(2,1)S(1)}, u32[]{:S(2)}, u32[]{:S(2)}) collective-permute-start(bf16[256,512]{1,0:T(8,128)(2,1)S(1)} %get-tuple-element.82), channel_id=1, source_target_pairs={{0,3},{1,0},{2,1},{3,2},{4,7},{5,4},{6,5},{7,6},{8,11},{9,8},{10,9... | collective-permute-start | bytes 786440 | tf_op jit(solution)/shard_map/ppermute | solution.py:23
  60.8 0.8 shard_map.242.a0
  61.6 0.7 collective-permute-start.10
  62.3 2.6 %collective-permute-start.11 = (bf16[192,256]{1,0:T(8,128)(2,1)S(1)}, bf16[192,256]{1,0:T(8,128)(2,1)S(1)}, u32[]{:S(2)}, u32[]{:S(2)}) collective-permute-start(bf16[192,256]{1,0:T(8,128)(2,1)S(1)} %shard_map.242.a0), channel_id=1, source_target_pairs={{0,2},{1,3},{2,0},{3,1},{4,6},{5,7},{6,4},{7,5},{8,10},{9,11},{10,... | collective-permute-start | bytes 294920 | tf_op jit(solution)/shard_map/ppermute | solution.py:23
  64.8 9.3 %collective-permute-done.10.a1 = bf16[192,256]{1,0:T(8,128)(2,1)S(1)} collective-permute-done((bf16[192,256]{1,0:T(8,128)(2,1)S(1)}, bf16[192,256]{1,0:T(8,128)(2,1)S(1)}, u32[]{:S(2)}, u32[]{:S(2)}) %collective-permute-start.10) | collective-permute-done | bytes 98336 | tf_op jit(solution)/shard_map/ppermute | solution.py:23
  74.2 4.7 %renew.1 = f32[32,256,64]{2,1,0:T(8,128)} custom-call(f32[128,128]{1,0:T(8,128)S(1)} %get-tuple-element.70.decay, f32[128,128]{1,0:T(8,128)S(1)} %get-tuple-element.71.removed, f32[128,128]{1,0:T(8,128)S(1)} %get-tuple-element.72.blended, f32[32,256]{1,0:T(8,128)S(1)} %get-tuple-element.73.along, f32[32,256]{1,0:T(8,128)S(1)} %get-tuple-element.74.value, ...), custom_call_target="tpu_custom_call" | custom-call | tf_op jit(solution)/shard_map/renew/pallas_call | solution.py:442
  79.0 0.4 shard_map.243
  79.3 0.2 copy.41
  79.5 20.6 %all_to_all.11 = bf16[3,64,512]{2,0,1:T(4,128)(2,1)S(1)} all-to-all(bf16[3,64,512]{2,0,1:T(4,128)(2,1)S(1)} %copy.41), channel_id=1, replica_groups=mesh['ep'=64,'tp'=4] {'ep'}, dimensions={1} | all-to-all | bytes 393216 | tf_op jit(solution)/shard_map/all_to_all | solution.py:462
  100.1 0.1 fusion.1
  100.3 0.7 fusion
  (33 shorter events, 0.3 us)
Async XLA Ops:
  1.4 9.1 %collective-permute-start = (bf16[64,512]{1,0:T(8,128)(2,1)S(1)}, bf16[64,512]{1,0:T(8,128)(2,1)S(1)}, u32[]{:S(2)}, u32[]{:S(2)}) collective-permute-start(bf16[64,512]{1,0:T(8,128)(2,1)S(1)} %shard_map.239.p0), channel_id=1, source_target_pairs={{0,3},{1,0},{2,1},{3,2},{4,7},{5,4},{6,5},{7,6},{8,11},{9,8},{10,9... | collective-permute-start | bytes 196616 | tf_op jit(solution)/shard_map/ppermute | solution.py:23
  4.8 5.7 %collective-permute-start.1 = (bf16[64,512]{1,0:T(8,128)(2,1)S(1)}, bf16[64,512]{1,0:T(8,128)(2,1)S(1)}, u32[]{:S(2)}, u32[]{:S(2)}) collective-permute-start(bf16[64,512]{1,0:T(8,128)(2,1)S(1)} %shard_map.239.p0), channel_id=1, source_target_pairs={{0,2},{1,3},{2,0},{3,1},{4,6},{5,7},{6,4},{7,5},{8,10},{9,11},{10,... | collective-permute-start | bytes 196616 | tf_op jit(solution)/shard_map/ppermute | solution.py:23
  5.3 5.2 %collective-permute-start.2 = (bf16[64,512]{1,0:T(8,128)(2,1)S(1)}, bf16[64,512]{1,0:T(8,128)(2,1)S(1)}, u32[]{:S(2)}, u32[]{:S(2)}) collective-permute-start(bf16[64,512]{1,0:T(8,128)(2,1)S(1)} %shard_map.239.p0), channel_id=1, source_target_pairs={{0,1},{1,2},{2,3},{3,0},{4,5},{5,6},{6,7},{7,4},{8,9},{9,10},{10,1... | collective-permute-start | bytes 196616 | tf_op jit(solution)/shard_map/ppermute | solution.py:23
  10.5 9.9 %copy-start.4 = (bf16[32,512]{1,0:T(8,128)(2,1)S(1)}, bf16[32,512]{1,0:T(8,128)(2,1)}, u32[]{:S(2)}) copy-start(bf16[32,512]{1,0:T(8,128)(2,1)} %first.1) | copy-start | bytes 98308
  10.5 50.3 %copy-start.1 = (bf16[1,2048,256]{2,1,0:T(8,128)(2,1)S(1)}, bf16[1,2048,256]{2,1,0:T(8,128)(2,1)}, u32[]{:S(2)}) copy-start(bf16[1,2048,256]{2,1,0:T(8,128)(2,1)} %param.45) | copy-start | bytes 3145732
  10.5 50.3 %copy-start.2 = (bf16[1,2048,256]{2,1,0:T(8,128)(2,1)S(1)}, bf16[1,2048,256]{2,1,0:T(8,128)(2,1)}, u32[]{:S(2)}) copy-start(bf16[1,2048,256]{2,1,0:T(8,128)(2,1)} %param.46) | copy-start | bytes 3145732
  10.5 50.3 %copy-start.3 = (f32[2048]{0:T(1024)S(1)}, f32[2048]{0:T(1024)}, u32[]{:S(2)}) copy-start(f32[2048]{0:T(1024)} %param.42) | copy-start | bytes 24580
  14.0 4.2 %collective-permute-start.3 = (bf16[32,512]{1,0:T(8,128)(2,1)S(1)}, bf16[32,512]{1,0:T(8,128)(2,1)S(1)}, u32[]{:S(2)}, u32[]{:S(2)}) collective-permute-start(bf16[32,512]{1,0:T(8,128)(2,1)S(1)} %get-tuple-element.59), channel_id=1, source_target_pairs={{0,1},{1,2},{2,3},{3,0},{4,5},{5,6},{6,7},{7,4},{8,9},{9,10},{10,1... | collective-permute-start | bytes 98312 | tf_op jit(solution)/shard_map/ppermute | solution.py:23
  15.6 4.3 %collective-permute-start.4 = (bf16[32,512]{1,0:T(8,128)(2,1)S(1)}, bf16[32,512]{1,0:T(8,128)(2,1)S(1)}, u32[]{:S(2)}, u32[]{:S(2)}) collective-permute-start(bf16[32,512]{1,0:T(8,128)(2,1)S(1)} %get-tuple-element.60), channel_id=1, source_target_pairs={{0,2},{1,3},{2,0},{3,1},{4,6},{5,7},{6,4},{7,5},{8,10},{9,11},{10,... | collective-permute-start | bytes 98312 | tf_op jit(solution)/shard_map/ppermute | solution.py:23
  17.4 3.1 %collective-permute-start.5 = (bf16[32,512]{1,0:T(8,128)(2,1)S(1)}, bf16[32,512]{1,0:T(8,128)(2,1)S(1)}, u32[]{:S(2)}, u32[]{:S(2)}) collective-permute-start(bf16[32,512]{1,0:T(8,128)(2,1)S(1)} %get-tuple-element.61), channel_id=1, source_target_pairs={{0,3},{1,0},{2,1},{3,2},{4,7},{5,4},{6,5},{7,6},{8,11},{9,8},{10,9... | collective-permute-start | bytes 98312 | tf_op jit(solution)/shard_map/ppermute | solution.py:23
  48.4 6.3 %collective-permute-start.6 = (bf16[192,512]{1,0:T(8,128)(2,1)S(1)}, bf16[192,512]{1,0:T(8,128)(2,1)S(1)}, u32[]{:S(2)}, u32[]{:S(2)}) collective-permute-start(bf16[192,512]{1,0:T(8,128)(2,1)S(1)} %bitcast.20), channel_id=1, source_target_pairs={{0,3},{1,0},{2,1},{3,2},{4,7},{5,4},{6,5},{7,6},{8,11},{9,8},{10,9... | collective-permute-start | bytes 589832 | tf_op jit(solution)/shard_map/ppermute | solution.py:23
  50.2 10.6 %collective-permute-start.9 = (bf16[192,512]{1,0:T(8,128)(2,1)S(1)}, bf16[192,512]{1,0:T(8,128)(2,1)S(1)}, u32[]{:S(2)}, u32[]{:S(2)}) collective-permute-start(bf16[192,512]{1,0:T(8,128)(2,1)S(1)} %bitcast.21), channel_id=1, source_target_pairs={{0,1},{1,2},{2,3},{3,0},{4,5},{5,6},{6,7},{7,4},{8,9},{9,10},{10,1... | collective-permute-start | bytes 589832 | tf_op jit(solution)/shard_map/ppermute | solution.py:23
  50.2 9.2 %collective-permute-start.7 = (bf16[96,512]{1,0:T(8,128)(2,1)S(1)}, bf16[96,512]{1,0:T(8,128)(2,1)S(1)}, u32[]{:S(2)}, u32[]{:S(2)}) collective-permute-start(bf16[96,512]{1,0:T(8,128)(2,1)S(1)} %slice.16), channel_id=1, source_target_pairs={{0,2},{1,3},{2,0},{3,1},{4,6},{5,7},{6,4},{7,5},{8,10},{9,11},{10,... | collective-permute-start | bytes 294920 | tf_op jit(solution)/shard_map/ppermute | solution.py:23
  54.7 6.1 %collective-permute-start.8 = (bf16[96,512]{1,0:T(8,128)(2,1)S(1)}, bf16[96,512]{1,0:T(8,128)(2,1)S(1)}, u32[]{:S(2)}, u32[]{:S(2)}) collective-permute-start(bf16[96,512]{1,0:T(8,128)(2,1)S(1)} %slice.17), channel_id=1, source_target_pairs={{0,3},{1,0},{2,1},{3,2},{4,7},{5,4},{6,5},{7,6},{8,11},{9,8},{10,9... | collective-permute-start | bytes 294920 | tf_op jit(solution)/shard_map/ppermute | solution.py:23
  58.1 20.8 %collective-permute-start.13 = (bf16[256,512]{1,0:T(8,128)(2,1)S(1)}, bf16[256,512]{1,0:T(8,128)(2,1)S(1)}, u32[]{:S(2)}, u32[]{:S(2)}) collective-permute-start(bf16[256,512]{1,0:T(8,128)(2,1)S(1)} %get-tuple-element.80), channel_id=1, source_target_pairs={{0,1},{1,2},{2,3},{3,0},{4,5},{5,6},{6,7},{7,4},{8,9},{9,10},{10,1... | collective-permute-start | bytes 786440 | tf_op jit(solution)/shard_map/ppermute | solution.py:23
  58.1 20.8 %collective-permute-start.14 = (bf16[256,512]{1,0:T(8,128)(2,1)S(1)}, bf16[256,512]{1,0:T(8,128)(2,1)S(1)}, u32[]{:S(2)}, u32[]{:S(2)}) collective-permute-start(bf16[256,512]{1,0:T(8,128)(2,1)S(1)} %get-tuple-element.81), channel_id=1, source_target_pairs={{0,2},{1,3},{2,0},{3,1},{4,6},{5,7},{6,4},{7,5},{8,10},{9,11},{10,... | collective-permute-start | bytes 786440 | tf_op jit(solution)/shard_map/ppermute | solution.py:23
  59.4 19.6 %collective-permute-start.15 = (bf16[256,512]{1,0:T(8,128)(2,1)S(1)}, bf16[256,512]{1,0:T(8,128)(2,1)S(1)}, u32[]{:S(2)}, u32[]{:S(2)}) collective-permute-start(bf16[256,512]{1,0:T(8,128)(2,1)S(1)} %get-tuple-element.82), channel_id=1, source_target_pairs={{0,3},{1,0},{2,1},{3,2},{4,7},{5,4},{6,5},{7,6},{8,11},{9,8},{10,9... | collective-permute-start | bytes 786440 | tf_op jit(solution)/shard_map/ppermute | solution.py:23
  61.6 17.4 %copy-start = (bf16[1,256,2048]{2,1,0:T(8,128)(2,1)S(1)}, bf16[1,256,2048]{2,1,0:T(8,128)(2,1)}, u32[]{:S(2)}) copy-start(bf16[1,256,2048]{2,1,0:T(8,128)(2,1)} %param.47) | copy-start | bytes 3145732
  61.6 12.6 %collective-permute-start.10 = (bf16[192,256]{1,0:T(8,128)(2,1)S(1)}, bf16[192,256]{1,0:T(8,128)(2,1)S(1)}, u32[]{:S(2)}, u32[]{:S(2)}) collective-permute-start(bf16[192,256]{1,0:T(8,128)(2,1)S(1)} %shard_map.242.a0), channel_id=1, source_target_pairs={{0,1},{1,2},{2,3},{3,0},{4,5},{5,6},{6,7},{7,4},{8,9},{9,10},{10,1... | collective-permute-start | bytes 294920 | tf_op jit(solution)/shard_map/ppermute | solution.py:23
  62.3 16.6 %collective-permute-start.11 = (bf16[192,256]{1,0:T(8,128)(2,1)S(1)}, bf16[192,256]{1,0:T(8,128)(2,1)S(1)}, u32[]{:S(2)}, u32[]{:S(2)}) collective-permute-start(bf16[192,256]{1,0:T(8,128)(2,1)S(1)} %shard_map.242.a0), channel_id=1, source_target_pairs={{0,2},{1,3},{2,0},{3,1},{4,6},{5,7},{6,4},{7,5},{8,10},{9,11},{10,... | collective-permute-start | bytes 294920 | tf_op jit(solution)/shard_map/ppermute | solution.py:23
  74.2 4.7 %collective-permute-start.12 = (bf16[192,256]{1,0:T(8,128)(2,1)S(1)}, bf16[192,256]{1,0:T(8,128)(2,1)S(1)}, u32[]{:S(2)}, u32[]{:S(2)}) collective-permute-start(bf16[192,256]{1,0:T(8,128)(2,1)S(1)} %shard_map.242.a0), channel_id=1, source_target_pairs={{0,3},{1,0},{2,1},{3,2},{4,7},{5,4},{6,5},{7,6},{8,11},{9,8},{10,9... | collective-permute-start | bytes 294920 | tf_op jit(solution)/shard_map/ppermute | solution.py:23

commit v5 on v4

--- a/solution.py
+++ b/solution.py
@@ -61,9 +61,8 @@
     damping,
     self_weight,
     head_gain,
-    state_head,
-    output_weight_hbm,
-    state_hbm,
+    output_weight,
+    state,
     o0,
     o1,
     o2,
@@ -75,15 +74,7 @@
     blended_out,
     vectors,
     results,
-    output_weight,
-    state_tail,
-    sems,
 ):
-    half = state_tail.shape[0]
-    state_copy = pltpu.make_async_copy(state_hbm.at[pl.ds(half, half)], state_tail, sems.at[0])
-    state_copy.start()
-    weight_copy = pltpu.make_async_copy(output_weight_hbm, output_weight, sems.at[1])
-    weight_copy.start()
     sequences, columns = along_out.shape
     heads, width = self_weight.shape
     block = p0.shape[1]
@@ -135,13 +126,10 @@
         for h in range(heads):
             vectors[pl.ds(v * heads + h, sequences, stride=rows_each), :] = of_head(vector, h)
     for s in range(sequences):
-        if s == half:
-            state_copy.wait()
-        state = state_head if s < half else state_tail
         rows = pl.ds(s * rows_each, rows_each)
         found = lax.dot_general(
             vectors[rows, :][:, :width].astype(jnp.bfloat16),
-            state[s % half].astype(jnp.bfloat16),
+            state[s].astype(jnp.bfloat16),
             (((1,), (1,)), ((), ())),
             preferred_element_type=jnp.float32,
         )
@@ -172,7 +160,6 @@
         centered * lax.rsqrt(variance + GROUP_EPS) * head_gain[...]
         + head_sums(receptance * blended * gains, same_head) * value
     ).astype(jnp.bfloat16)
-    weight_copy.wait()
     for place, o in zip(places, (o0, o1, o2, o3)):
         o[...] = jnp.dot(
             mixed, output_weight[:, pl.ds(place, block)], preferred_element_type=jnp.float32
@@ -231,32 +218,65 @@
         copy.wait()
 
 
-def fetch_kernel(at, *refs):
-    sems = refs[-1]
-    count = len(sems) - 3
-    *sources, down_weight = refs[: count + 1]
-    wholes, columns = refs[count + 1 : 2 * count + 1], refs[2 * count + 1 : -1]
-    sources[-1] = sources[-1].at[pl.ds(0, wholes[-1].shape[0])]
-    copies = [
-        pltpu.make_async_copy(source, whole, sems.at[i])
-        for i, (source, whole) in enumerate(zip(sources, wholes))
+def route_kernel(
+    at,
+    routes_hbm,
+    weights_hbm,
+    down_weight,
+    dispatch,
+    high,
+    low,
+    piece_1,
+    piece_2,
+    piece_3,
+    routes,
+    weights,
+    sems,
+):
+    needed = [
+        pltpu.make_async_copy(routes_hbm, routes, sems.at[3]),
+        pltpu.make_async_copy(weights_hbm, weights, sems.at[4]),
     ]
-    for k, piece in enumerate(columns, 1):
+    for copy in needed:
+        copy.start()
+    copies = []
+    for k, piece in enumerate((piece_1, piece_2, piece_3), 1):
         block = piece.shape[1]
         place = pl.multiple_of(lax.rem(at[0] + k, 4) * block, block)
         copies.append(
-            pltpu.make_async_copy(
-                down_weight.at[:, pl.ds(place, block)], piece, sems.at[count + k - 1]
-            )
+            pltpu.make_async_copy(down_weight.at[:, pl.ds(place, block)], piece, sems.at[k - 1])
         )
     for copy in copies:
         copy.start()
+    for copy in needed:
+        copy.wait()
+    choices, sequences = routes.shape
+    experts = dispatch.shape[0] // CAPACITY
+    ids = lax.broadcasted_iota(jnp.int32, (experts, sequences), 0)
+    named = jnp.zeros((experts, sequences), jnp.float32)
+    weight = jnp.zeros((experts, sequences), jnp.float32)
+    for c in range(choices):
+        hit = ids == routes[c : c + 1, :]
+        named = jnp.where(hit, 1.0, named)
+        weight = jnp.where(hit, weights[c : c + 1, :], weight)
+    row = lax.broadcasted_iota(jnp.int32, (sequences, sequences), 0)
+    column = lax.broadcasted_iota(jnp.int32, (sequences, sequences), 1)
+    earlier = (row < column).astype(jnp.bfloat16)
+    ranking = jnp.dot(named.astype(jnp.bfloat16), earlier, preferred_element_type=jnp.float32)
+    for c in range(CAPACITY):
+        rows = slice(c * experts, (c + 1) * experts)
+        here = jnp.where(ranking == c, named, 0.0)
+        dispatch[rows, :] = here.astype(jnp.bfloat16)
+        share = here * weight
+        first = share.astype(jnp.bfloat16)
+        high[rows, :] = first
+        low[rows, :] = (share - first.astype(jnp.float32)).astype(jnp.bfloat16)
     for copy in copies:
         copy.wait()
 
 
-def hidden_kernel(at, x0, x1, x2, x2_rest, x3, gain, gate_weight, up_weight, out):
-    pieces = (x0[...], x1[...], jnp.concatenate([x2[...], x2_rest[...]], axis=0), x3[...])
+def hidden_kernel(at, x0, x1, x2, x3, gain, gate_weight, up_weight, out):
+    pieces = (x0[...], x1[...], x2[...], x3[...])
     width = x0.shape[1]
     places = [lax.rem(at[0] + k, 4) * width for k in range(4)]
     floats = [x.astype(jnp.float32) for x in pieces]
@@ -283,7 +303,7 @@
     out[...] = total.astype(jnp.bfloat16)
 
 
-def local_call(kernel, shapes, limit, scratch=(), scalars=0, left=0):
+def local_call(kernel, shapes, limit, scratch=(), scalars=0, left=0, cost=None):
     def call(*operands):
         in_vmem = pl.BlockSpec(memory_space=pltpu.VMEM)
         count = len(operands) - left
@@ -299,6 +319,7 @@
             out_specs=jax.tree.map(lambda _: in_vmem, shapes),
             scratch_shapes=scratch,
             compiler_params=pltpu.CompilerParams(vmem_limit_bytes=limit * MIB),
+            cost_estimate=cost,
         )(*operands)
 
     return call
@@ -362,28 +383,25 @@
         vector(head_norm_gain),
     )
     flat_state = state.reshape(sequences, head_columns, state.shape[3])
-    shapes = [jax.ShapeDtypeStruct(a.shape, a.dtype) for a in needed]
-    shapes.append(float32(sequences // 2, *flat_state.shape[1:]))
-    *needed, down_1, down_2, down_3 = local_call(
-        fetch_kernel,
-        shapes + [bfloat16(expert_down_weight.shape[1], own_columns)] * 3,
-        14,
-        [pltpu.SemaphoreType.DMA((len(shapes) + 3,))],
+    experts = expert_gate_weight.shape[0] * lax.axis_size("ep")
+    slots = CAPACITY * experts
+    dispatch, high, low, down_1, down_2, down_3 = local_call(
+        route_kernel,
+        [bfloat16(slots, sequences)] * 3 + [bfloat16(expert_down_weight.shape[1], own_columns)] * 3,
+        4,
+        [
+            pltpu.VMEM(routes.shape[::-1], routes.dtype),
+            pltpu.VMEM(routes.shape[::-1], jnp.float32),
+            pltpu.SemaphoreType.DMA((5,)),
+        ],
         scalars=1,
-        left=len(shapes) + 1,
-    )(at, *needed, flat_state, expert_down_weight[0])
-
-    experts = expert_gate_weight.shape[0] * lax.axis_size("ep")
-    ids = jnp.arange(experts, dtype=jnp.int32)
-    hits = routes[:, :, None] == ids[None, None, :]
-    named = jnp.sum(hits.astype(jnp.float32), axis=1)
-    earlier = jnp.tril(jnp.ones((sequences, sequences), jnp.float32), -1)
-    ranking = jnp.dot(earlier, named)
-    weight_of = jnp.sum(jnp.where(hits, chosen_expert_weight[:, :, None], 0.0), axis=1)
-    slots = [(ranking == c) & (named > 0) for c in range(CAPACITY)]
-    dispatch = jnp.concatenate([s.astype(jnp.bfloat16) for s in slots], axis=1)
-    combine = jnp.concatenate([jnp.where(s, weight_of, 0.0) for s in slots], axis=1)
-
+        left=3,
+        cost=pl.CostEstimate(flops=4_000_000_000, transcendentals=0, bytes_accessed=32_000_000),
+    )(at, routes.T, chosen_expert_weight.T, expert_down_weight[0])
+
+    dispatch, high, low, down_1, down_2, down_3, *row_pieces = lax.optimization_barrier(
+        (dispatch, high, low, down_1, down_2, down_3, *row_pieces)
+    )
     *head_terms, decay, along, value, removed, blended = local_call(
         attention_kernel,
         [bfloat16(sequences, own_columns)] * 4
@@ -394,51 +412,23 @@
         [
             pltpu.VMEM((8 * sequences, 128), jnp.float32),
             pltpu.VMEM((2, 8 * sequences, 128), jnp.float32),
-            pltpu.VMEM(output_weight.shape, output_weight.dtype),
-            pltpu.VMEM((sequences // 2, *flat_state.shape[1:]), jnp.float32),
-            pltpu.SemaphoreType.DMA((2,)),
         ],
         scalars=1,
-        left=2,
     )(at, *row_pieces, *needed, output_weight, flat_state)
     arrived = scattered(head_terms)
     down_pieces = scattered([None, down_1, down_2, down_3])[1:]
     residual = tokens.astype(jnp.float32) + sum(a.astype(jnp.float32) for a in arrived)
 
-    outgoing = lax.dot_general(
-        dispatch,
-        residual.astype(jnp.bfloat16),
-        (((0,), (0,)), ((), ())),
-        preferred_element_type=jnp.float32,
+    outgoing = jnp.dot(
+        dispatch, residual.astype(jnp.bfloat16), preferred_element_type=jnp.float32
     ).astype(jnp.bfloat16)
     outgoing = outgoing.reshape(CAPACITY, experts, own_columns)
-    high = combine.astype(jnp.bfloat16)
-    low = (combine - high.astype(jnp.float32)).astype(jnp.bfloat16)
-    outgoing, high, low = lax.optimization_barrier((outgoing, high, low))
     came = lax.all_to_all(outgoing, "ep", split_axis=1, concat_axis=1, tiled=True)
+    came, decay, removed, blended, along, value = lax.optimization_barrier(
+        (came, decay, removed, blended, along, value)
+    )
     own_rows = came.reshape(CAPACITY * experts, own_columns)
-    half = own_rows.shape[0] // 2
-    second = from_offset(own_rows[:half], 2)
-    first = from_offset(own_rows, 1)
-    third = from_offset(own_rows, 3)
-    second_rest = from_offset(first[half:], 1)
-    activation = local_call(
-        hidden_kernel, bfloat16(own_rows.shape[0], expert_gate_weight.shape[2]), 12, scalars=1
-    )(
-        at,
-        own_rows,
-        first,
-        second,
-        second_rest,
-        third,
-        vector(second_norm_gain),
-        expert_gate_weight[0],
-        expert_up_weight[0],
-    )
-    activation, *renewing = lax.optimization_barrier(
-        (activation, decay, removed, blended, along, value)
-    )
-    act_pieces = scattered([activation] * 4)
+    row_pieces = gathered(own_rows)
     new_state = pl.pallas_call(
         renew_kernel,
         out_shape=float32(*flat_state.shape),
@@ -452,17 +442,30 @@
         ],
         compiler_params=pltpu.CompilerParams(vmem_limit_bytes=12 * MIB),
         name="renew",
-    )(*renewing, pltpu.with_memory_space_constraint(flat_state, pltpu.HBM))
-    new_state, *act_pieces = lax.optimization_barrier((new_state, *act_pieces))
+    )(decay, removed, blended, along, value, pltpu.with_memory_space_constraint(flat_state, pltpu.HBM))
+    new_state, *row_pieces = lax.optimization_barrier((new_state, *row_pieces))
     new_state = new_state.reshape(state.shape)
+    activation = local_call(
+        hidden_kernel, bfloat16(own_rows.shape[0], expert_gate_weight.shape[2]), 12, scalars=1
+    )(
+        at,
+        *row_pieces,
+        vector(second_norm_gain),
+        expert_gate_weight[0],
+        expert_up_weight[0],
+    )
+    act_pieces = scattered([activation] * 4)
     shares = local_call(
         down_kernel, bfloat16(own_rows.shape[0], own_columns), 8, scalars=1
     )(at, *act_pieces, *down_pieces, expert_down_weight[0])
     shares = shares.reshape(CAPACITY, experts, own_columns)
     returned = lax.all_to_all(shares, "ep", split_axis=1, concat_axis=1, tiled=True)
     returned = returned.reshape(CAPACITY * experts, own_columns)
-    weighted = jnp.dot(
-        jnp.concatenate([high, low], axis=0), returned, preferred_element_type=jnp.float32
+    weighted = lax.dot_general(
+        jnp.concatenate([high, low], axis=1),
+        returned,
+        (((0,), (0,)), ((), ())),
+        preferred_element_type=jnp.float32,
     )
     layer_out = (residual + weighted[:sequences] + weighted[sequences:]).astype(jnp.bfloat16)
     return (layer_out, new_state)

time: 101 us -> 102 us (level)
  waiting for transfers between devices: 14.7 us -> 19.9 us
  Pallas kernels: 13.5 us -> 10.5 us
  starting transfers between devices: 21 us -> 19.5 us
    ppermute x16 -> x15, waiting for transfers between devices: 14.7 us -> 19.9 us  [from_offset(): lax.ppermute(value, 'tp', [(i, (i - offset) % devices) for i in range(dev...]
    pallas_call x5, Pallas kernels: 8.82 us -> 5.73 us  [call(): pl.pallas_call(kernel, out_shape=shapes, in_specs=[pl.BlockSpec(memory_sp...]
    ppermute x16 -> x15, starting transfers between devices: 21 us -> 19.5 us  [from_offset(): lax.ppermute(value, 'tp', [(i, (i - offset) % devices) for i in range(dev...]
  transfers between devices with their start and end apart: 16 -> 15, of which waited for: 4 -> 9; matrix products, arithmetic and copies ran while one was open for 1% -> 0% of each run, Pallas kernels for 9% -> 7%
where the time goes in v5:
time: 102 us; the launch traced here: 101 us
  blocking collectives  48.8 us (48%)
  waiting for transfers between devices  19.9 us (20%)
  starting transfers between devices  19.5 us (19%)
  Pallas kernels  10.5 us (10%)
    all_to_all x1, blocking collectives, shards(): lax.all_to_all(outgoing, 'ep', split_axis=1, concat_axis=1, tiled=True)  27.8 us
    all_to_all x1, blocking collectives, shards(): lax.all_to_all(shares, 'ep', split_axis=1, concat_axis=1, tiled=True)  21 us
    ppermute x15, waiting for transfers between devices, from_offset(): lax.ppermute(value, 'tp', [(i, (i - offset) % devices) for i in range(dev...  19.9 us
    ppermute x15, starting transfers between devices, from_offset(): lax.ppermute(value, 'tp', [(i, (i - offset) % devices) for i in range(dev...  19.5 us
    pallas_call x5, Pallas kernels, call(): pl.pallas_call(kernel, out_shape=shapes, in_specs=[pl.BlockSpec(memory_sp...  5.73 us
    pallas_call x1, Pallas kernels, shards(): pl.pallas_call(renew_kernel, out_shape=float32(*flat_state.shape), in_spe...  4.72 us
  transfers between devices with their start and end apart: 15, of which 9 were waited for; matrix products, arithmetic and copies ran while one was open for 0% of the time, Pallas kernels for 7%

profile of v5, /device:TPU:1, one launch (start us, length us, event | category | flops | bytes accessed | tf_op | source)
XLA Modules:
  0.0 101.3 jit_solution(17619281342674140369)
XLA Ops:
  0.6 0.8 shard_map.240.p0
  1.4 3.4 %collective-permute-start = (bf16[64,512]{1,0:T(8,128)(2,1)S(1)}, bf16[64,512]{1,0:T(8,128)(2,1)S(1)}, u32[]{:S(2)}, u32[]{:S(2)}) collective-permute-start(bf16[64,512]{1,0:T(8,128)(2,1)S(1)} %shard_map.240.p0), channel_id=1, source_target_pairs={{0,3},{1,0},{2,1},{3,2},{4,7},{5,4},{6,5},{7,6},{8,11},{9,8},{10,9... | collective-permute-start | bytes 196616 | tf_op jit(solution)/shard_map/ppermute | solution.py:23
  4.8 0.5 collective-permute-start.1
  5.3 0.6 collective-permute-start.2
  6.1 1.3 %shard_map.239 = (bf16[192,32]{1,0:T(8,128)(2,1)S(1)}, bf16[192,32]{1,0:T(8,128)(2,1)S(1)}, bf16[192,32]{1,0:T(8,128)(2,1)S(1)}, bf16[256,512]{1,0:T(8,128)(2,1)...) custom-call(s32[1]{0:T(128)} %bitcast.at, s32[4,32]{1,0:T(4,128)} %bitcast.40, f32[4,32]{1,0:T(4,128)} %bitcast.41, ...), custom_call_target="tpu_custom_call" | custom-call | flops 4000000000 | bytes 32000000 | tf_op jit(solution)/shard_map/pallas_call | solution.py:313
  7.4 2.1 %collective-permute-done.1.p2 = bf16[64,512]{1,0:T(8,128)(2,1)S(1)} collective-permute-done((bf16[64,512]{1,0:T(8,128)(2,1)S(1)}, bf16[64,512]{1,0:T(8,128)(2,1)S(1)}, u32[]{:S(2)}, u32[]{:S(2)}) %collective-permute-start.1) | collective-permute-done | bytes 65568 | tf_op jit(solution)/shard_map/ppermute | solution.py:23
  9.5 0.7 collective-permute-done.2.p3
  10.3 2.5 %shard_map.241 = (bf16[32,512]{1,0:T(8,128)(2,1)S(1)}, bf16[32,512]{1,0:T(8,128)(2,1)S(1)}, bf16[32,512]{1,0:T(8,128)(2,1)S(1)}, bf16[32,512]{1,0:T(8,128)(2,1)S...) custom-call(s32[1]{0:T(128)} %bitcast.at, ...), custom_call_target="tpu_custom_call" | custom-call | tf_op jit(solution)/shard_map/pallas_call | solution.py:313
  12.7 1.3 %collective-permute-start.3 = (bf16[32,512]{1,0:T(8,128)(2,1)S(1)}, bf16[32,512]{1,0:T(8,128)(2,1)S(1)}, u32[]{:S(2)}, u32[]{:S(2)}) collective-permute-start(bf16[32,512]{1,0:T(8,128)(2,1)S(1)} %get-tuple-element.49), channel_id=1, source_target_pairs={{0,1},{1,2},{2,3},{3,0},{4,5},{5,6},{6,7},{7,4},{8,9},{9,10},{10,1... | collective-permute-start | bytes 98312 | tf_op jit(solution)/shard_map/ppermute | solution.py:23
  14.1 1.7 %collective-permute-start.4 = (bf16[32,512]{1,0:T(8,128)(2,1)S(1)}, bf16[32,512]{1,0:T(8,128)(2,1)S(1)}, u32[]{:S(2)}, u32[]{:S(2)}) collective-permute-start(bf16[32,512]{1,0:T(8,128)(2,1)S(1)} %get-tuple-element.50), channel_id=1, source_target_pairs={{0,2},{1,3},{2,0},{3,1},{4,6},{5,7},{6,4},{7,5},{8,10},{9,11},{10,... | collective-permute-start | bytes 98312 | tf_op jit(solution)/shard_map/ppermute | solution.py:23
  15.8 0.8 collective-permute-start.5
  16.6 0.2 collective-permute-done.3
  16.8 1.6 %collective-permute-done.4 = bf16[32,512]{1,0:T(8,128)(2,1)S(1)} collective-permute-done((bf16[32,512]{1,0:T(8,128)(2,1)S(1)}, bf16[32,512]{1,0:T(8,128)(2,1)S(1)}, u32[]{:S(2)}, u32[]{:S(2)}) %collective-permute-start.4) | collective-permute-done | bytes 32800 | tf_op jit(solution)/shard_map/ppermute | solution.py:23
  18.4 0.2 collective-permute-done.5
  18.6 0.2 convolution_convert_fusion
  19.0 27.8 %all_to_all.10 = bf16[3,64,512]{2,0,1:T(4,128)(2,1)S(1)} all-to-all(bf16[3,64,512]{2,0,1:T(4,128)(2,1)S(1)} %copy.29), channel_id=1, replica_groups=mesh['ep'=64,'tp'=4] {'ep'}, dimensions={1} | all-to-all | bytes 393216 | tf_op jit(solution)/shard_map/all_to_all | solution.py:426
  46.8 2.0 %collective-permute-start.6 = (bf16[192,512]{1,0:T(8,128)(2,1)S(1)}, bf16[192,512]{1,0:T(8,128)(2,1)S(1)}, u32[]{:S(2)}, u32[]{:S(2)}) collective-permute-start(bf16[192,512]{1,0:T(8,128)(2,1)S(1)} %bitcast.26), channel_id=1, source_target_pairs={{0,3},{1,0},{2,1},{3,2},{4,7},{5,4},{6,5},{7,6},{8,11},{9,8},{10,9... | collective-permute-start | bytes 589832 | tf_op jit(solution)/shard_map/ppermute | solution.py:23
  48.8 1.3 %collective-permute-start.7 = (bf16[192,512]{1,0:T(8,128)(2,1)S(1)}, bf16[192,512]{1,0:T(8,128)(2,1)S(1)}, u32[]{:S(2)}, u32[]{:S(2)}) collective-permute-start(bf16[192,512]{1,0:T(8,128)(2,1)S(1)} %bitcast.27), channel_id=1, source_target_pairs={{0,2},{1,3},{2,0},{3,1},{4,6},{5,7},{6,4},{7,5},{8,10},{9,11},{10,... | collective-permute-start | bytes 589832 | tf_op jit(solution)/shard_map/ppermute | solution.py:23
  50.1 2.0 %collective-permute-start.8 = (bf16[192,512]{1,0:T(8,128)(2,1)S(1)}, bf16[192,512]{1,0:T(8,128)(2,1)S(1)}, u32[]{:S(2)}, u32[]{:S(2)}) collective-permute-start(bf16[192,512]{1,0:T(8,128)(2,1)S(1)} %bitcast.28), channel_id=1, source_target_pairs={{0,1},{1,2},{2,3},{3,0},{4,5},{5,6},{6,7},{7,4},{8,9},{9,10},{10,1... | collective-permute-start | bytes 589832 | tf_op jit(solution)/shard_map/ppermute | solution.py:23
  52.1 0.7 collective-permute-start.13
  52.8 0.3 collective-permute-done.6.x1
  53.1 3.6 %collective-permute-start.14 = (bf16[256,512]{1,0:T(8,128)(2,1)S(1)}, bf16[256,512]{1,0:T(8,128)(2,1)S(1)}, u32[]{:S(2)}, u32[]{:S(2)}) collective-permute-start(bf16[256,512]{1,0:T(8,128)(2,1)S(1)} %get-tuple-element.72), channel_id=1, source_target_pairs={{0,3},{1,0},{2,1},{3,2},{4,7},{5,4},{6,5},{7,6},{8,11},{9,8},{10,9... | collective-permute-start | bytes 786440 | tf_op jit(solution)/shard_map/ppermute | solution.py:23
  56.7 4.7 %renew.1 = f32[32,256,64]{2,1,0:T(8,128)} custom-call(f32[128,128]{1,0:T(8,128)S(1)} %get-tuple-element.60.decay, f32[128,128]{1,0:T(8,128)S(1)} %get-tuple-element.61.removed, f32[128,128]{1,0:T(8,128)S(1)} %get-tuple-element.62.blended, f32[32,256]{1,0:T(8,128)S(1)} %get-tuple-element.63.along, f32[32,256]{1,0:T(8,128)S(1)} %get-tuple-element.64.value, ...), custom_call_target="tpu_custom_call" | custom-call | tf_op jit(solution)/shard_map/renew/pallas_call | solution.py:432
  61.5 9.9 %collective-permute-done.8.x3 = bf16[192,512]{1,0:T(8,128)(2,1)S(1)} collective-permute-done((bf16[192,512]{1,0:T(8,128)(2,1)S(1)}, bf16[192,512]{1,0:T(8,128)(2,1)S(1)}, u32[]{:S(2)}, u32[]{:S(2)}) %collective-permute-start.8) | collective-permute-done | bytes 196640 | tf_op jit(solution)/shard_map/ppermute | solution.py:23
  71.4 0.8 shard_map.242.a0
  72.4 1.4 %collective-permute-start.9 = (bf16[192,256]{1,0:T(8,128)(2,1)S(1)}, bf16[192,256]{1,0:T(8,128)(2,1)S(1)}, u32[]{:S(2)}, u32[]{:S(2)}) collective-permute-start(bf16[192,256]{1,0:T(8,128)(2,1)S(1)} %shard_map.242.a0), channel_id=1, source_target_pairs={{0,1},{1,2},{2,3},{3,0},{4,5},{5,6},{6,7},{7,4},{8,9},{9,10},{10,1... | collective-permute-start | bytes 294920 | tf_op jit(solution)/shard_map/ppermute | solution.py:23
  73.9 3.5 %collective-permute-done.10.a2 = bf16[192,256]{1,0:T(8,128)(2,1)S(1)} collective-permute-done((bf16[192,256]{1,0:T(8,128)(2,1)S(1)}, bf16[192,256]{1,0:T(8,128)(2,1)S(1)}, u32[]{:S(2)}, u32[]{:S(2)}) %collective-permute-start.10) | collective-permute-done | bytes 98336 | tf_op jit(solution)/shard_map/ppermute | solution.py:23
  77.3 1.4 %collective-permute-done.9.a1 = bf16[192,256]{1,0:T(8,128)(2,1)S(1)} collective-permute-done((bf16[192,256]{1,0:T(8,128)(2,1)S(1)}, bf16[192,256]{1,0:T(8,128)(2,1)S(1)}, u32[]{:S(2)}, u32[]{:S(2)}) %collective-permute-start.9) | collective-permute-done | bytes 98336 | tf_op jit(solution)/shard_map/ppermute | solution.py:23
  78.8 0.4 shard_map.243
  79.3 21.0 %all_to_all.11 = bf16[3,64,512]{2,0,1:T(4,128)(2,1)S(1)} all-to-all(bf16[3,64,512]{2,0,1:T(4,128)(2,1)S(1)} %copy.31), channel_id=1, replica_groups=mesh['ep'=64,'tp'=4] {'ep'}, dimensions={1} | all-to-all | bytes 393216 | tf_op jit(solution)/shard_map/all_to_all | solution.py:462
  100.4 0.3 fusion.1
  100.6 0.7 fusion
  (55 shorter events, 0.7 us)
Async XLA Ops:
  1.4 6.0 %collective-permute-start = (bf16[64,512]{1,0:T(8,128)(2,1)S(1)}, bf16[64,512]{1,0:T(8,128)(2,1)S(1)}, u32[]{:S(2)}, u32[]{:S(2)}) collective-permute-start(bf16[64,512]{1,0:T(8,128)(2,1)S(1)} %shard_map.240.p0), channel_id=1, source_target_pairs={{0,3},{1,0},{2,1},{3,2},{4,7},{5,4},{6,5},{7,6},{8,11},{9,8},{10,9... | collective-permute-start | bytes 196616 | tf_op jit(solution)/shard_map/ppermute | solution.py:23
  4.8 4.7 %collective-permute-start.1 = (bf16[64,512]{1,0:T(8,128)(2,1)S(1)}, bf16[64,512]{1,0:T(8,128)(2,1)S(1)}, u32[]{:S(2)}, u32[]{:S(2)}) collective-permute-start(bf16[64,512]{1,0:T(8,128)(2,1)S(1)} %shard_map.240.p0), channel_id=1, source_target_pairs={{0,2},{1,3},{2,0},{3,1},{4,6},{5,7},{6,4},{7,5},{8,10},{9,11},{10,... | collective-permute-start | bytes 196616 | tf_op jit(solution)/shard_map/ppermute | solution.py:23
  5.3 4.8 %collective-permute-start.2 = (bf16[64,512]{1,0:T(8,128)(2,1)S(1)}, bf16[64,512]{1,0:T(8,128)(2,1)S(1)}, u32[]{:S(2)}, u32[]{:S(2)}) collective-permute-start(bf16[64,512]{1,0:T(8,128)(2,1)S(1)} %shard_map.240.p0), channel_id=1, source_target_pairs={{0,1},{1,2},{2,3},{3,0},{4,5},{5,6},{6,7},{7,4},{8,9},{9,10},{10,1... | collective-permute-start | bytes 196616 | tf_op jit(solution)/shard_map/ppermute | solution.py:23
  5.9 4.2 %copy-start = (f32[32,4,64,64]{3,2,1,0:T(8,128)S(1)}, f32[32,4,64,64]{3,2,1,0:T(8,128)}, u32[]{:S(2)}) copy-start(f32[32,4,64,64]{3,2,1,0:T(8,128)} %param.41) | copy-start | bytes 6291460
  5.9 4.2 %copy-start.1 = (bf16[2048,256]{1,0:T(8,128)(2,1)S(1)}, bf16[2048,256]{1,0:T(8,128)(2,1)}, u32[]{:S(2)}) copy-start(bf16[2048,256]{1,0:T(8,128)(2,1)} %receptance_weight.1) | copy-start | bytes 3145732
  5.9 4.2 %copy-start.2 = (bf16[2048,256]{1,0:T(8,128)(2,1)S(1)}, bf16[2048,256]{1,0:T(8,128)(2,1)}, u32[]{:S(2)}) copy-start(bf16[2048,256]{1,0:T(8,128)(2,1)} %key_weight.1) | copy-start | bytes 3145732
  5.9 4.2 %copy-start.3 = (bf16[2048,256]{1,0:T(8,128)(2,1)S(1)}, bf16[2048,256]{1,0:T(8,128)(2,1)}, u32[]{:S(2)}) copy-start(bf16[2048,256]{1,0:T(8,128)(2,1)} %value_weight.1) | copy-start | bytes 3145732
  5.9 4.2 %copy-start.4 = (bf16[256,2048]{1,0:T(8,128)(2,1)S(1)}, bf16[256,2048]{1,0:T(8,128)(2,1)}, u32[]{:S(2)}) copy-start(bf16[256,2048]{1,0:T(8,128)(2,1)} %output_weight.1) | copy-start | bytes 3145732
  6.0 4.2 %copy-start.8 = (bf16[2048,128]{1,0:T(8,128)(2,1)S(1)}, bf16[2048,128]{1,0:T(8,128)(2,1)}, u32[]{:S(2)}) copy-start(bf16[2048,128]{1,0:T(8,128)(2,1)} %decay_down.1) | copy-start | bytes 1572868
  6.0 4.2 %copy-start.9 = (bf16[2048,128]{1,0:T(8,128)(2,1)S(1)}, bf16[2048,128]{1,0:T(8,128)(2,1)}, u32[]{:S(2)}) copy-start(bf16[2048,128]{1,0:T(8,128)(2,1)} %strength_down.1) | copy-start | bytes 1572868
  6.0 4.2 %copy-start.10 = (bf16[128,1024]{1,0:T(8,128)(2,1)S(1)}, bf16[128,1024]{1,0:T(8,128)(2,1)}, u32[]{:S(2)}) copy-start(bf16[128,1024]{1,0:T(8,128)(2,1)} %decay_up.1) | copy-start | bytes 786436
  6.0 4.2 %copy-start.11 = (bf16[128,1024]{1,0:T(8,128)(2,1)S(1)}, bf16[128,1024]{1,0:T(8,128)(2,1)}, u32[]{:S(2)}) copy-start(bf16[128,1024]{1,0:T(8,128)(2,1)} %strength_up.1) | copy-start | bytes 786436
  6.0 4.2 %copy-start.12 = (f32[5,2048]{1,0:T(8,128)S(1)}, f32[5,2048]{1,0:T(8,128)}, u32[]{:S(2)}) copy-start(f32[5,2048]{1,0:T(8,128)} %share.1) | copy-start | bytes 122884
  6.0 4.2 %copy-start.13 = (f32[2048]{0:T(1024)S(1)}, f32[2048]{0:T(1024)}, u32[]{:S(2)}) copy-start(f32[2048]{0:T(1024)} %param.26) | copy-start | bytes 24580
  6.0 4.2 %copy-start.15 = (f32[4,64]{1,0:T(4,128)S(1)}, f32[4,64]{1,0:T(4,128)}, u32[]{:S(2)}) copy-start(f32[4,64]{1,0:T(4,128)} %self_weight.1) | copy-start | bytes 3076
  10.3 8.3 %copy-start.20 = (bf16[32,512]{1,0:T(8,128)(2,1)S(1)}, bf16[32,512]{1,0:T(8,128)(2,1)}, u32[]{:S(2)}) copy-start(bf16[32,512]{1,0:T(8,128)(2,1)} %first.1) | copy-start | bytes 98308
  12.7 4.0 %collective-permute-start.3 = (bf16[32,512]{1,0:T(8,128)(2,1)S(1)}, bf16[32,512]{1,0:T(8,128)(2,1)S(1)}, u32[]{:S(2)}, u32[]{:S(2)}) collective-permute-start(bf16[32,512]{1,0:T(8,128)(2,1)S(1)} %get-tuple-element.49), channel_id=1, source_target_pairs={{0,1},{1,2},{2,3},{3,0},{4,5},{5,6},{6,7},{7,4},{8,9},{9,10},{10,1... | collective-permute-start | bytes 98312 | tf_op jit(solution)/shard_map/ppermute | solution.py:23
  14.1 4.3 %collective-permute-start.4 = (bf16[32,512]{1,0:T(8,128)(2,1)S(1)}, bf16[32,512]{1,0:T(8,128)(2,1)S(1)}, u32[]{:S(2)}, u32[]{:S(2)}) collective-permute-start(bf16[32,512]{1,0:T(8,128)(2,1)S(1)} %get-tuple-element.50), channel_id=1, source_target_pairs={{0,2},{1,3},{2,0},{3,1},{4,6},{5,7},{6,4},{7,5},{8,10},{9,11},{10,... | collective-permute-start | bytes 98312 | tf_op jit(solution)/shard_map/ppermute | solution.py:23
  15.8 2.8 %collective-permute-start.5 = (bf16[32,512]{1,0:T(8,128)(2,1)S(1)}, bf16[32,512]{1,0:T(8,128)(2,1)S(1)}, u32[]{:S(2)}, u32[]{:S(2)}) collective-permute-start(bf16[32,512]{1,0:T(8,128)(2,1)S(1)} %get-tuple-element.51), channel_id=1, source_target_pairs={{0,3},{1,0},{2,1},{3,2},{4,7},{5,4},{6,5},{7,6},{8,11},{9,8},{10,9... | collective-permute-start | bytes 98312 | tf_op jit(solution)/shard_map/ppermute | solution.py:23
  46.8 24.6 %copy-start.5 = (bf16[1,2048,256]{2,1,0:T(8,128)(2,1)S(1)}, bf16[1,2048,256]{2,1,0:T(8,128)(2,1)}, u32[]{:S(2)}) copy-start(bf16[1,2048,256]{2,1,0:T(8,128)(2,1)} %param.45) | copy-start | bytes 3145732
  46.8 24.6 %copy-start.6 = (bf16[1,2048,256]{2,1,0:T(8,128)(2,1)S(1)}, bf16[1,2048,256]{2,1,0:T(8,128)(2,1)}, u32[]{:S(2)}) copy-start(bf16[1,2048,256]{2,1,0:T(8,128)(2,1)} %param.46) | copy-start | bytes 3145732
  46.8 24.6 %copy-start.14 = (f32[2048]{0:T(1024)S(1)}, f32[2048]{0:T(1024)}, u32[]{:S(2)}) copy-start(f32[2048]{0:T(1024)} %param.42) | copy-start | bytes 24580
  46.8 32.0 %copy-start.7 = (bf16[1,256,2048]{2,1,0:T(8,128)(2,1)S(1)}, bf16[1,256,2048]{2,1,0:T(8,128)(2,1)}, u32[]{:S(2)}) copy-start(bf16[1,256,2048]{2,1,0:T(8,128)(2,1)} %param.47) | copy-start | bytes 3145732
  46.8 6.3 %collective-permute-start.6 = (bf16[192,512]{1,0:T(8,128)(2,1)S(1)}, bf16[192,512]{1,0:T(8,128)(2,1)S(1)}, u32[]{:S(2)}, u32[]{:S(2)}) collective-permute-start(bf16[192,512]{1,0:T(8,128)(2,1)S(1)} %bitcast.26), channel_id=1, source_target_pairs={{0,3},{1,0},{2,1},{3,2},{4,7},{5,4},{6,5},{7,6},{8,11},{9,8},{10,9... | collective-permute-start | bytes 589832 | tf_op jit(solution)/shard_map/ppermute | solution.py:23
  48.8 23.6 %collective-permute-start.12 = (bf16[256,512]{1,0:T(8,128)(2,1)S(1)}, bf16[256,512]{1,0:T(8,128)(2,1)S(1)}, u32[]{:S(2)}, u32[]{:S(2)}) collective-permute-start(bf16[256,512]{1,0:T(8,128)(2,1)S(1)} %get-tuple-element.70), channel_id=1, source_target_pairs={{0,1},{1,2},{2,3},{3,0},{4,5},{5,6},{6,7},{7,4},{8,9},{9,10},{10,1... | collective-permute-start | bytes 786440 | tf_op jit(solution)/shard_map/ppermute | solution.py:23
  48.8 12.6 %collective-permute-start.7 = (bf16[192,512]{1,0:T(8,128)(2,1)S(1)}, bf16[192,512]{1,0:T(8,128)(2,1)S(1)}, u32[]{:S(2)}, u32[]{:S(2)}) collective-permute-start(bf16[192,512]{1,0:T(8,128)(2,1)S(1)} %bitcast.27), channel_id=1, source_target_pairs={{0,2},{1,3},{2,0},{3,1},{4,6},{5,7},{6,4},{7,5},{8,10},{9,11},{10,... | collective-permute-start | bytes 589832 | tf_op jit(solution)/shard_map/ppermute | solution.py:23
  50.1 21.3 %collective-permute-start.8 = (bf16[192,512]{1,0:T(8,128)(2,1)S(1)}, bf16[192,512]{1,0:T(8,128)(2,1)S(1)}, u32[]{:S(2)}, u32[]{:S(2)}) collective-permute-start(bf16[192,512]{1,0:T(8,128)(2,1)S(1)} %bitcast.28), channel_id=1, source_target_pairs={{0,1},{1,2},{2,3},{3,0},{4,5},{5,6},{6,7},{7,4},{8,9},{9,10},{10,1... | collective-permute-start | bytes 589832 | tf_op jit(solution)/shard_map/ppermute | solution.py:23
  52.1 21.8 %collective-permute-start.13 = (bf16[256,512]{1,0:T(8,128)(2,1)S(1)}, bf16[256,512]{1,0:T(8,128)(2,1)S(1)}, u32[]{:S(2)}, u32[]{:S(2)}) collective-permute-start(bf16[256,512]{1,0:T(8,128)(2,1)S(1)} %get-tuple-element.71), channel_id=1, source_target_pairs={{0,2},{1,3},{2,0},{3,1},{4,6},{5,7},{6,4},{7,5},{8,10},{9,11},{10,... | collective-permute-start | bytes 786440 | tf_op jit(solution)/shard_map/ppermute | solution.py:23
  53.1 20.8 %collective-permute-start.14 = (bf16[256,512]{1,0:T(8,128)(2,1)S(1)}, bf16[256,512]{1,0:T(8,128)(2,1)S(1)}, u32[]{:S(2)}, u32[]{:S(2)}) collective-permute-start(bf16[256,512]{1,0:T(8,128)(2,1)S(1)} %get-tuple-element.72), channel_id=1, source_target_pairs={{0,3},{1,0},{2,1},{3,2},{4,7},{5,4},{6,5},{7,6},{8,11},{9,8},{10,9... | collective-permute-start | bytes 786440 | tf_op jit(solution)/shard_map/ppermute | solution.py:23
  72.2 5.1 %collective-permute-start.10 = (bf16[192,256]{1,0:T(8,128)(2,1)S(1)}, bf16[192,256]{1,0:T(8,128)(2,1)S(1)}, u32[]{:S(2)}, u32[]{:S(2)}) collective-permute-start(bf16[192,256]{1,0:T(8,128)(2,1)S(1)} %shard_map.242.a0), channel_id=1, source_target_pairs={{0,2},{1,3},{2,0},{3,1},{4,6},{5,7},{6,4},{7,5},{8,10},{9,11},{10,... | collective-permute-start | bytes 294920 | tf_op jit(solution)/shard_map/ppermute | solution.py:23
  72.3 5.0 %collective-permute-start.11 = (bf16[192,256]{1,0:T(8,128)(2,1)S(1)}, bf16[192,256]{1,0:T(8,128)(2,1)S(1)}, u32[]{:S(2)}, u32[]{:S(2)}) collective-permute-start(bf16[192,256]{1,0:T(8,128)(2,1)S(1)} %shard_map.242.a0), channel_id=1, source_target_pairs={{0,3},{1,0},{2,1},{3,2},{4,7},{5,4},{6,5},{7,6},{8,11},{9,8},{10,9... | collective-permute-start | bytes 294920 | tf_op jit(solution)/shard_map/ppermute | solution.py:23
  72.4 6.4 %collective-permute-start.9 = (bf16[192,256]{1,0:T(8,128)(2,1)S(1)}, bf16[192,256]{1,0:T(8,128)(2,1)S(1)}, u32[]{:S(2)}, u32[]{:S(2)}) collective-permute-start(bf16[192,256]{1,0:T(8,128)(2,1)S(1)} %shard_map.242.a0), channel_id=1, source_target_pairs={{0,1},{1,2},{2,3},{3,0},{4,5},{5,6},{6,7},{7,4},{8,9},{9,10},{10,1... | collective-permute-start | bytes 294920 | tf_op jit(solution)/shard_map/ppermute | solution.py:23
  (4 other events, 16.8 us)

commit v6 on v5

--- a/solution.py
+++ b/solution.py
@@ -160,10 +160,13 @@
         centered * lax.rsqrt(variance + GROUP_EPS) * head_gain[...]
         + head_sums(receptance * blended * gains, same_head) * value
     ).astype(jnp.bfloat16)
-    for place, o in zip(places, (o0, o1, o2, o3)):
-        o[...] = jnp.dot(
+    for k, place in enumerate(places):
+        piece = jnp.dot(
             mixed, output_weight[:, pl.ds(place, block)], preferred_element_type=jnp.float32
         ).astype(jnp.bfloat16)
+        outs = (o0, o1, o2, o3)
+        outs[k][:, :block] = piece
+        outs[(k + 2) % 4][:, block:] = piece
     along_out[...] = along
     value_out[...] = value
     for out, vector in ((decay_out, decay), (removal_out, removed), (blended_out, blended)):
@@ -206,7 +209,8 @@
         leaving.wait()
 
 
-def stack_kernel(first, second, out, sems):
+def stack_kernel(at, first, second, out, sems):
+    del at
     height = first.shape[0]
     copies = [
         pltpu.make_async_copy(first, out.at[pl.ds(0, height)], sems.at[0]),
@@ -216,6 +220,10 @@
         copy.start()
     for copy in copies:
         copy.wait()
+
+
+def gate_kernel(rows, out):
+    out[...] = rows[...]
 
 
 def route_kernel(
@@ -275,9 +283,9 @@
         copy.wait()
 
 
-def hidden_kernel(at, x0, x1, x2, x3, gain, gate_weight, up_weight, out):
-    pieces = (x0[...], x1[...], x2[...], x3[...])
-    width = x0.shape[1]
+def hidden_kernel(at, x02, x1, x3, gain, gate_weight, up_weight, out):
+    width = x1.shape[1]
+    pieces = (x02[:, :width], x1[...], x02[:, width:], x3[...])
     places = [lax.rem(at[0] + k, 4) * width for k in range(4)]
     floats = [x.astype(jnp.float32) for x in pieces]
     squares = sum(jnp.sum(f * f, axis=1, keepdims=True) for f in floats)
@@ -361,8 +369,15 @@
         jax.ShapeDtypeStruct((2 * sequences, own_columns), tokens.dtype),
         1,
         [pltpu.SemaphoreType.DMA((2,))],
+        scalars=1,
         left=2,
-    )(tokens, previous)
+    )(at, tokens, previous)
+    both = local_call(
+        gate_kernel,
+        bfloat16(*both.shape),
+        1,
+        cost=pl.CostEstimate(flops=40_000_000_000, transcendentals=0, bytes_accessed=200_000_000),
+    )(both)
     row_pieces = gathered(both)
 
     vector = lambda value: value[None, :]
@@ -396,7 +411,6 @@
         ],
         scalars=1,
         left=3,
-        cost=pl.CostEstimate(flops=4_000_000_000, transcendentals=0, bytes_accessed=32_000_000),
     )(at, routes.T, chosen_expert_weight.T, expert_down_weight[0])
 
     dispatch, high, low, down_1, down_2, down_3, *row_pieces = lax.optimization_barrier(
@@ -404,7 +418,7 @@
     )
     *head_terms, decay, along, value, removed, blended = local_call(
         attention_kernel,
-        [bfloat16(sequences, own_columns)] * 4
+        [bfloat16(sequences, 2 * own_columns)] * 4
         + [float32(sequences * state.shape[1], 128)]
         + [float32(sequences, head_columns)] * 2
         + [float32(sequences * state.shape[1], 128)] * 2,
@@ -417,18 +431,20 @@
     )(at, *row_pieces, *needed, output_weight, flat_state)
     arrived = scattered(head_terms)
     down_pieces = scattered([None, down_1, down_2, down_3])[1:]
-    residual = tokens.astype(jnp.float32) + sum(a.astype(jnp.float32) for a in arrived)
+    present = jnp.concatenate([row_pieces[0][:sequences], row_pieces[2][:sequences]], axis=1)
+    residual = present.astype(jnp.float32) + sum(a.astype(jnp.float32) for a in arrived)
 
     outgoing = jnp.dot(
         dispatch, residual.astype(jnp.bfloat16), preferred_element_type=jnp.float32
     ).astype(jnp.bfloat16)
-    outgoing = outgoing.reshape(CAPACITY, experts, own_columns)
+    outgoing = outgoing.reshape(CAPACITY, experts, 2 * own_columns)
     came = lax.all_to_all(outgoing, "ep", split_axis=1, concat_axis=1, tiled=True)
     came, decay, removed, blended, along, value = lax.optimization_barrier(
         (came, decay, removed, blended, along, value)
     )
-    own_rows = came.reshape(CAPACITY * experts, own_columns)
-    row_pieces = gathered(own_rows)
+    own_rows = came.reshape(CAPACITY * experts, 2 * own_columns)
+    one_slice = own_rows[:, :own_columns]
+    row_pieces = [own_rows, from_offset(one_slice, 1), from_offset(one_slice, 3)]
     new_state = pl.pallas_call(
         renew_kernel,
         out_shape=float32(*flat_state.shape),
@@ -467,7 +483,7 @@
         (((0,), (0,)), ((), ())),
         preferred_element_type=jnp.float32,
     )
-    layer_out = (residual + weighted[:sequences] + weighted[sequences:]).astype(jnp.bfloat16)
+    layer_out = (residual[:, :own_columns] + weighted[:sequences] + weighted[sequences:]).astype(jnp.bfloat16)
     return (layer_out, new_state)
 
 

time: 102 us -> 100 us (0.980)
  blocking collectives: 48.8 us -> 22 us
  waiting for transfers between devices: 19.9 us -> 32.6 us
  starting transfers between devices: 19.5 us -> 31.2 us
  local copies, waits for them, and re-layouts: 0.55 us -> 1.65 us
    all_to_all x1 -> x0, blocking collectives: 27.8 us -> none  [shards(): lax.all_to_all(outgoing, 'ep', split_axis=1, concat_axis=1, tiled=True)]
    all_to_all x0 -> x1, waiting for transfers between devices: none -> 16.6 us  [shards(): lax.all_to_all(outgoing, 'ep', split_axis=1, concat_axis=1, tiled=True)]
    all_to_all x0 -> x1, starting transfers between devices: none -> 15.2 us  [shards(): lax.all_to_all(outgoing, 'ep', split_axis=1, concat_axis=1, tiled=True)]
    ppermute x15 -> x14, waiting for transfers between devices: 19.9 us -> 16 us  [from_offset(): lax.ppermute(value, 'tp', [(i, (i - offset) % devices) for i in range(dev...]
    ppermute x15 -> x14, starting transfers between devices: 19.5 us -> 16 us  [from_offset(): lax.ppermute(value, 'tp', [(i, (i - offset) % devices) for i in range(dev...]
    all_to_all x1, blocking collectives: 21 us -> 22 us  [shards(): lax.all_to_all(shares, 'ep', split_axis=1, concat_axis=1, tiled=True)]
    pallas_call x5 -> x6, Pallas kernels: 5.73 us -> 5.61 us  [call(): pl.pallas_call(kernel, out_shape=shapes, in_specs=[pl.BlockSpec(memory_sp...]
  transfers between devices with their start and end apart: 15 -> 15, of which waited for: 9 -> 10; matrix products, arithmetic and copies ran while one was open for 0% -> 0% of each run, Pallas kernels for 7% -> 7%
where the time goes in v6:
time: 100 us; the launch traced here: 99.9 us
  waiting for transfers between devices  32.6 us (33%)
  starting transfers between devices  31.2 us (31%)
  blocking collectives  22 us (22%)
  Pallas kernels  10.3 us (10%)
  local copies, waits for them, and re-layouts  1.65 us (2%)
  between operations  1.05 us (1%)
    all_to_all x1, blocking collectives, shards(): lax.all_to_all(shares, 'ep', split_axis=1, concat_axis=1, tiled=True)  22 us
    all_to_all x1, waiting for transfers between devices, shards(): lax.all_to_all(outgoing, 'ep', split_axis=1, concat_axis=1, tiled=True)  16.6 us
    ppermute x14, waiting for transfers between devices, from_offset(): lax.ppermute(value, 'tp', [(i, (i - offset) % devices) for i in range(dev...  16 us
    ppermute x14, starting transfers between devices, from_offset(): lax.ppermute(value, 'tp', [(i, (i - offset) % devices) for i in range(dev...  16 us
    all_to_all x1, starting transfers between devices, shards(): lax.all_to_all(outgoing, 'ep', split_axis=1, concat_axis=1, tiled=True)  15.2 us
    pallas_call x6, Pallas kernels, call(): pl.pallas_call(kernel, out_shape=shapes, in_specs=[pl.BlockSpec(memory_sp...  5.61 us
    pallas_call x1, Pallas kernels, shards(): pl.pallas_call(renew_kernel, out_shape=float32(*flat_state.shape), in_spe...  4.72 us
  transfers between devices with their start and end apart: 15, of which 10 were waited for; matrix products, arithmetic and copies ran while one was open for 0% of the time, Pallas kernels for 7%

profile of v6, /device:TPU:1, one launch (start us, length us, event | category | flops | bytes accessed | tf_op | source)
XLA Modules:
  0.0 99.9 jit_solution(5803424053957785122)
XLA Ops:
  0.6 0.8 shard_map.240.rows
  1.6 3.4 %collective-permute-start = (bf16[64,512]{1,0:T(8,128)(2,1)S(1)}, bf16[64,512]{1,0:T(8,128)(2,1)S(1)}, u32[]{:S(2)}, u32[]{:S(2)}) collective-permute-start(bf16[64,512]{1,0:T(8,128)(2,1)S(1)} %shard_map.241.p0), channel_id=1, source_target_pairs={{0,3},{1,0},{2,1},{3,2},{4,7},{5,4},{6,5},{7,6},{8,11},{9,8},{10,9... | collective-permute-start | bytes 196616 | tf_op jit(solution)/shard_map/ppermute | solution.py:23
  5.0 0.5 collective-permute-start.1
  5.5 0.6 collective-permute-start.2
  6.1 1.2 %shard_map.239 = (bf16[192,32]{1,0:T(8,128)(2,1)S(1)}, bf16[192,32]{1,0:T(8,128)(2,1)S(1)}, bf16[192,32]{1,0:T(8,128)(2,1)S(1)}, bf16[256,512]{1,0:T(8,128)(2,1)...) custom-call(s32[1]{0:T(128)} %bitcast.at, s32[4,32]{1,0:T(4,128)} %bitcast.38, f32[4,32]{1,0:T(4,128)} %bitcast.39, ...), custom_call_target="tpu_custom_call" | custom-call | tf_op jit(solution)/shard_map/pallas_call | solution.py:321
  7.3 2.3 %collective-permute-done.1.p2 = bf16[64,512]{1,0:T(8,128)(2,1)S(1)} collective-permute-done((bf16[64,512]{1,0:T(8,128)(2,1)S(1)}, bf16[64,512]{1,0:T(8,128)(2,1)S(1)}, u32[]{:S(2)}, u32[]{:S(2)}) %collective-permute-start.1) | collective-permute-done | bytes 65568 | tf_op jit(solution)/shard_map/ppermute | solution.py:23
  9.7 0.7 collective-permute-done.2.p3
  10.5 2.5 %shard_map.242 = (bf16[32,1024]{1,0:T(8,128)(2,1)S(1)}, bf16[32,1024]{1,0:T(8,128)(2,1)S(1)}, bf16[32,1024]{1,0:T(8,128)(2,1)S(1)}, bf16[32,1024]{1,0:T(8,128)(2...) custom-call(s32[1]{0:T(128)} %bitcast.at, ...), custom_call_target="tpu_custom_call" | custom-call | tf_op jit(solution)/shard_map/pallas_call | solution.py:321
  13.0 1.7 %collective-permute-start.4 = (bf16[32,1024]{1,0:T(8,128)(2,1)S(1)}, bf16[32,1024]{1,0:T(8,128)(2,1)S(1)}, u32[]{:S(2)}, u32[]{:S(2)}) collective-permute-start(bf16[32,1024]{1,0:T(8,128)(2,1)S(1)} %get-tuple-element.49), channel_id=1, source_target_pairs={{0,2},{1,3},{2,0},{3,1},{4,6},{5,7},{6,4},{7,5},{8,10},{9,11},{10,... | collective-permute-start | bytes 196616 | tf_op jit(solution)/shard_map/ppermute | solution.py:23
  14.8 1.8 %collective-permute-start.5 = (bf16[32,1024]{1,0:T(8,128)(2,1)S(1)}, bf16[32,1024]{1,0:T(8,128)(2,1)S(1)}, u32[]{:S(2)}, u32[]{:S(2)}) collective-permute-start(bf16[32,1024]{1,0:T(8,128)(2,1)S(1)} %get-tuple-element.50), channel_id=1, source_target_pairs={{0,3},{1,0},{2,1},{3,2},{4,7},{5,4},{6,5},{7,6},{8,11},{9,8},{10,9... | collective-permute-start | bytes 196616 | tf_op jit(solution)/shard_map/ppermute | solution.py:23
  16.6 1.4 %collective-permute-done.3 = bf16[32,1024]{1,0:T(8,128)(2,1)S(1)} collective-permute-done((bf16[32,1024]{1,0:T(8,128)(2,1)S(1)}, bf16[32,1024]{1,0:T(8,128)(2,1)S(1)}, u32[]{:S(2)}, u32[]{:S(2)}) %collective-permute-start.3) | collective-permute-done | bytes 65568 | tf_op jit(solution)/shard_map/ppermute | solution.py:23
  18.0 0.6 collective-permute-done.5
  18.7 0.2 convolution_convert_fusion
  18.9 1.1 %copy.29 = bf16[3,64,1024]{2,0,1:T(4,128)(2,1)} copy(bf16[3,64,1024]{2,1,0:T(8,128)(2,1)S(1)} %bitcast.36) | data formatting | bytes 786432 | tf_op jit(solution)/shard_map/reshape | solution.py:440
  20.0 15.2 %all-to-all-start = ((bf16[3,64,1024]{2,0,1:T(4,128)(2,1)}), bf16[3,64,1024]{2,0,1:T(4,128)(2,1)S(1)}, u32[]{:S(2)}, u32[]{:S(2)}) async-start(bf16[3,64,1024]{2,0,1:T(4,128)(2,1)} %copy.29), calls=%async_computation | async-start | bytes 1048576 | tf_op jit(solution)/shard_map/all_to_all | solution.py:441
  35.2 1.1 %collective-permute-start.11 = (bf16[256,512]{1,0:T(8,128)(2,1)S(1)}, bf16[256,512]{1,0:T(8,128)(2,1)S(1)}, u32[]{:S(2)}, u32[]{:S(2)}) collective-permute-start(bf16[256,512]{1,0:T(8,128)(2,1)S(1)} %get-tuple-element.68), channel_id=1, source_target_pairs={{0,1},{1,2},{2,3},{3,0},{4,5},{5,6},{6,7},{7,4},{8,9},{9,10},{10,1... | collective-permute-start | bytes 786440 | tf_op jit(solution)/shard_map/ppermute | solution.py:23
  36.4 16.6 %all-to-all-done = bf16[3,64,1024]{2,0,1:T(4,128)(2,1)S(1)} async-done(((bf16[3,64,1024]{2,0,1:T(4,128)(2,1)}), bf16[3,64,1024]{2,0,1:T(4,128)(2,1)S(1)}, u32[]{:S(2)}, u32[]{:S(2)}) %all-to-all-start) | async-done | bytes 393248 | tf_op jit(solution)/shard_map/all_to_all | solution.py:441
  53.2 2.5 %collective-permute-start.6 = (bf16[192,512]{1,0:T(8,128)(2,1)S(1)}, bf16[192,512]{1,0:T(8,128)(2,1)S(1)}, u32[]{:S(2)}, u32[]{:S(2)}) collective-permute-start(bf16[192,512]{1,0:T(8,128)(2,1)S(1)} %slice.25), channel_id=1, source_target_pairs={{0,3},{1,0},{2,1},{3,2},{4,7},{5,4},{6,5},{7,6},{8,11},{9,8},{10,9... | collective-permute-start | bytes 589832 | tf_op jit(solution)/shard_map/ppermute | solution.py:23
  55.6 1.3 %collective-permute-start.12 = (bf16[256,512]{1,0:T(8,128)(2,1)S(1)}, bf16[256,512]{1,0:T(8,128)(2,1)S(1)}, u32[]{:S(2)}, u32[]{:S(2)}) collective-permute-start(bf16[256,512]{1,0:T(8,128)(2,1)S(1)} %get-tuple-element.69), channel_id=1, source_target_pairs={{0,2},{1,3},{2,0},{3,1},{4,6},{5,7},{6,4},{7,5},{8,10},{9,11},{10,... | collective-permute-start | bytes 786440 | tf_op jit(solution)/shard_map/ppermute | solution.py:23
  56.9 1.4 %collective-permute-start.13 = (bf16[256,512]{1,0:T(8,128)(2,1)S(1)}, bf16[256,512]{1,0:T(8,128)(2,1)S(1)}, u32[]{:S(2)}, u32[]{:S(2)}) collective-permute-start(bf16[256,512]{1,0:T(8,128)(2,1)S(1)} %get-tuple-element.70), channel_id=1, source_target_pairs={{0,3},{1,0},{2,1},{3,2},{4,7},{5,4},{6,5},{7,6},{8,11},{9,8},{10,9... | collective-permute-start | bytes 786440 | tf_op jit(solution)/shard_map/ppermute | solution.py:23
  58.3 4.7 %renew.1 = f32[32,256,64]{2,1,0:T(8,128)} custom-call(f32[128,128]{1,0:T(8,128)S(1)} %get-tuple-element.59.decay, f32[128,128]{1,0:T(8,128)S(1)} %get-tuple-element.60.removed, f32[128,128]{1,0:T(8,128)S(1)} %get-tuple-element.61.blended, f32[32,256]{1,0:T(8,128)S(1)} %get-tuple-element.62.along, f32[32,256]{1,0:T(8,128)S(1)} %get-tuple-element.63.value, ...), custom_call_target="tpu_custom_call" | custom-call | tf_op jit(solution)/shard_map/renew/pallas_call | solution.py:448
  63.0 5.2 %collective-permute-done.7.x3 = bf16[192,512]{1,0:T(8,128)(2,1)S(1)} collective-permute-done((bf16[192,512]{1,0:T(8,128)(2,1)S(1)}, bf16[192,512]{1,0:T(8,128)(2,1)S(1)}, u32[]{:S(2)}, u32[]{:S(2)}) %collective-permute-start.7) | collective-permute-done | bytes 196640 | tf_op jit(solution)/shard_map/ppermute | solution.py:23
  68.3 0.8 shard_map.243.a0
  69.1 1.5 %collective-permute-start.8 = (bf16[192,256]{1,0:T(8,128)(2,1)S(1)}, bf16[192,256]{1,0:T(8,128)(2,1)S(1)}, u32[]{:S(2)}, u32[]{:S(2)}) collective-permute-start(bf16[192,256]{1,0:T(8,128)(2,1)S(1)} %shard_map.243.a0), channel_id=1, source_target_pairs={{0,1},{1,2},{2,3},{3,0},{4,5},{5,6},{6,7},{7,4},{8,9},{9,10},{10,1... | collective-permute-start | bytes 294920 | tf_op jit(solution)/shard_map/ppermute | solution.py:23
  70.7 1.9 %collective-permute-done.10.a3 = bf16[192,256]{1,0:T(8,128)(2,1)S(1)} collective-permute-done((bf16[192,256]{1,0:T(8,128)(2,1)S(1)}, bf16[192,256]{1,0:T(8,128)(2,1)S(1)}, u32[]{:S(2)}, u32[]{:S(2)}) %collective-permute-start.10) | collective-permute-done | bytes 98336 | tf_op jit(solution)/shard_map/ppermute | solution.py:23
  72.6 1.3 %collective-permute-done.8.a1 = bf16[192,256]{1,0:T(8,128)(2,1)S(1)} collective-permute-done((bf16[192,256]{1,0:T(8,128)(2,1)S(1)}, bf16[192,256]{1,0:T(8,128)(2,1)S(1)}, u32[]{:S(2)}, u32[]{:S(2)}) %collective-permute-start.8) | collective-permute-done | bytes 98336 | tf_op jit(solution)/shard_map/ppermute | solution.py:23
  73.9 2.5 %collective-permute-done.9.a2 = bf16[192,256]{1,0:T(8,128)(2,1)S(1)} collective-permute-done((bf16[192,256]{1,0:T(8,128)(2,1)S(1)}, bf16[192,256]{1,0:T(8,128)(2,1)S(1)}, u32[]{:S(2)}, u32[]{:S(2)}) %collective-permute-start.9) | collective-permute-done | bytes 98336 | tf_op jit(solution)/shard_map/ppermute | solution.py:23
  76.4 0.4 shard_map.244
  76.8 0.2 copy.31
  77.0 22.0 %all_to_all.10 = bf16[3,64,512]{2,0,1:T(4,128)(2,1)S(1)} all-to-all(bf16[3,64,512]{2,0,1:T(4,128)(2,1)S(1)} %copy.31), channel_id=1, replica_groups=mesh['ep'=64,'tp'=4] {'ep'}, dimensions={1} | all-to-all | bytes 393216 | tf_op jit(solution)/shard_map/all_to_all | solution.py:478
  99.0 0.3 fusion.2
  99.3 0.6 fusion
  (57 shorter events, 0.7 us)
Async XLA Ops:
  1.4 8.9 %copy-start = (f32[32,4,64,64]{3,2,1,0:T(8,128)S(1)}, f32[32,4,64,64]{3,2,1,0:T(8,128)}, u32[]{:S(2)}) copy-start(f32[32,4,64,64]{3,2,1,0:T(8,128)} %param.41) | copy-start | bytes 6291460
  1.4 8.9 %copy-start.2 = (bf16[2048,256]{1,0:T(8,128)(2,1)S(1)}, bf16[2048,256]{1,0:T(8,128)(2,1)}, u32[]{:S(2)}) copy-start(bf16[2048,256]{1,0:T(8,128)(2,1)} %receptance_weight.1) | copy-start | bytes 3145732
  1.5 8.9 %copy-start.3 = (bf16[2048,256]{1,0:T(8,128)(2,1)S(1)}, bf16[2048,256]{1,0:T(8,128)(2,1)}, u32[]{:S(2)}) copy-start(bf16[2048,256]{1,0:T(8,128)(2,1)} %key_weight.1) | copy-start | bytes 3145732
  1.5 8.9 %copy-start.4 = (bf16[2048,256]{1,0:T(8,128)(2,1)S(1)}, bf16[2048,256]{1,0:T(8,128)(2,1)}, u32[]{:S(2)}) copy-start(bf16[2048,256]{1,0:T(8,128)(2,1)} %value_weight.1) | copy-start | bytes 3145732
  1.5 8.9 %copy-start.5 = (bf16[256,2048]{1,0:T(8,128)(2,1)S(1)}, bf16[256,2048]{1,0:T(8,128)(2,1)}, u32[]{:S(2)}) copy-start(bf16[256,2048]{1,0:T(8,128)(2,1)} %output_weight.1) | copy-start | bytes 3145732
  1.5 8.9 %copy-start.8 = (bf16[2048,128]{1,0:T(8,128)(2,1)S(1)}, bf16[2048,128]{1,0:T(8,128)(2,1)}, u32[]{:S(2)}) copy-start(bf16[2048,128]{1,0:T(8,128)(2,1)} %decay_down.1) | copy-start | bytes 1572868
  1.5 8.9 %copy-start.9 = (bf16[2048,128]{1,0:T(8,128)(2,1)S(1)}, bf16[2048,128]{1,0:T(8,128)(2,1)}, u32[]{:S(2)}) copy-start(bf16[2048,128]{1,0:T(8,128)(2,1)} %strength_down.1) | copy-start | bytes 1572868
  1.5 8.9 %copy-start.10 = (bf16[128,1024]{1,0:T(8,128)(2,1)S(1)}, bf16[128,1024]{1,0:T(8,128)(2,1)}, u32[]{:S(2)}) copy-start(bf16[128,1024]{1,0:T(8,128)(2,1)} %decay_up.1) | copy-start | bytes 786436
  1.5 8.9 %copy-start.11 = (bf16[128,1024]{1,0:T(8,128)(2,1)S(1)}, bf16[128,1024]{1,0:T(8,128)(2,1)}, u32[]{:S(2)}) copy-start(bf16[128,1024]{1,0:T(8,128)(2,1)} %strength_up.1) | copy-start | bytes 786436
  1.5 8.9 %copy-start.12 = (f32[5,2048]{1,0:T(8,128)S(1)}, f32[5,2048]{1,0:T(8,128)}, u32[]{:S(2)}) copy-start(f32[5,2048]{1,0:T(8,128)} %share.1) | copy-start | bytes 122884
  1.6 8.9 %copy-start.13 = (f32[2048]{0:T(1024)S(1)}, f32[2048]{0:T(1024)}, u32[]{:S(2)}) copy-start(f32[2048]{0:T(1024)} %param.26) | copy-start | bytes 24580
  1.6 8.9 %copy-start.15 = (f32[4,64]{1,0:T(4,128)S(1)}, f32[4,64]{1,0:T(4,128)}, u32[]{:S(2)}) copy-start(f32[4,64]{1,0:T(4,128)} %self_weight.1) | copy-start | bytes 3076
  1.6 8.9 %copy-start.16 = (f32[256]{0:T(256)S(1)}, f32[256]{0:T(256)}, u32[]{:S(2)}) copy-start(f32[256]{0:T(256)} %param.33) | copy-start | bytes 3076
  1.6 5.7 %collective-permute-start = (bf16[64,512]{1,0:T(8,128)(2,1)S(1)}, bf16[64,512]{1,0:T(8,128)(2,1)S(1)}, u32[]{:S(2)}, u32[]{:S(2)}) collective-permute-start(bf16[64,512]{1,0:T(8,128)(2,1)S(1)} %shard_map.241.p0), channel_id=1, source_target_pairs={{0,3},{1,0},{2,1},{3,2},{4,7},{5,4},{6,5},{7,6},{8,11},{9,8},{10,9... | collective-permute-start | bytes 196616 | tf_op jit(solution)/shard_map/ppermute | solution.py:23
  5.0 4.7 %collective-permute-start.1 = (bf16[64,512]{1,0:T(8,128)(2,1)S(1)}, bf16[64,512]{1,0:T(8,128)(2,1)S(1)}, u32[]{:S(2)}, u32[]{:S(2)}) collective-permute-start(bf16[64,512]{1,0:T(8,128)(2,1)S(1)} %shard_map.241.p0), channel_id=1, source_target_pairs={{0,2},{1,3},{2,0},{3,1},{4,6},{5,7},{6,4},{7,5},{8,10},{9,11},{10,... | collective-permute-start | bytes 196616 | tf_op jit(solution)/shard_map/ppermute | solution.py:23
  5.5 4.8 %collective-permute-start.2 = (bf16[64,512]{1,0:T(8,128)(2,1)S(1)}, bf16[64,512]{1,0:T(8,128)(2,1)S(1)}, u32[]{:S(2)}, u32[]{:S(2)}) collective-permute-start(bf16[64,512]{1,0:T(8,128)(2,1)S(1)} %shard_map.241.p0), channel_id=1, source_target_pairs={{0,1},{1,2},{2,3},{3,0},{4,5},{5,6},{6,7},{7,4},{8,9},{9,10},{10,1... | collective-permute-start | bytes 196616 | tf_op jit(solution)/shard_map/ppermute | solution.py:23
  13.0 5.1 %collective-permute-start.3 = (bf16[32,1024]{1,0:T(8,128)(2,1)S(1)}, bf16[32,1024]{1,0:T(8,128)(2,1)S(1)}, u32[]{:S(2)}, u32[]{:S(2)}) collective-permute-start(bf16[32,1024]{1,0:T(8,128)(2,1)S(1)} %get-tuple-element.48), channel_id=1, source_target_pairs={{0,1},{1,2},{2,3},{3,0},{4,5},{5,6},{6,7},{7,4},{8,9},{9,10},{10,1... | collective-permute-start | bytes 196616 | tf_op jit(solution)/shard_map/ppermute | solution.py:23
  13.0 5.0 %collective-permute-start.4 = (bf16[32,1024]{1,0:T(8,128)(2,1)S(1)}, bf16[32,1024]{1,0:T(8,128)(2,1)S(1)}, u32[]{:S(2)}, u32[]{:S(2)}) collective-permute-start(bf16[32,1024]{1,0:T(8,128)(2,1)S(1)} %get-tuple-element.49), channel_id=1, source_target_pairs={{0,2},{1,3},{2,0},{3,1},{4,6},{5,7},{6,4},{7,5},{8,10},{9,11},{10,... | collective-permute-start | bytes 196616 | tf_op jit(solution)/shard_map/ppermute | solution.py:23
  14.8 3.8 %collective-permute-start.5 = (bf16[32,1024]{1,0:T(8,128)(2,1)S(1)}, bf16[32,1024]{1,0:T(8,128)(2,1)S(1)}, u32[]{:S(2)}, u32[]{:S(2)}) collective-permute-start(bf16[32,1024]{1,0:T(8,128)(2,1)S(1)} %get-tuple-element.50), channel_id=1, source_target_pairs={{0,3},{1,0},{2,1},{3,2},{4,7},{5,4},{6,5},{7,6},{8,11},{9,8},{10,9... | collective-permute-start | bytes 196616 | tf_op jit(solution)/shard_map/ppermute | solution.py:23
  20.0 32.9 %all-to-all-start = ((bf16[3,64,1024]{2,0,1:T(4,128)(2,1)}), bf16[3,64,1024]{2,0,1:T(4,128)(2,1)S(1)}, u32[]{:S(2)}, u32[]{:S(2)}) async-start(bf16[3,64,1024]{2,0,1:T(4,128)(2,1)} %copy.29), calls=%async_computation | async-start | bytes 1048576 | tf_op jit(solution)/shard_map/all_to_all | solution.py:441
  35.2 35.4 %collective-permute-start.11 = (bf16[256,512]{1,0:T(8,128)(2,1)S(1)}, bf16[256,512]{1,0:T(8,128)(2,1)S(1)}, u32[]{:S(2)}, u32[]{:S(2)}) collective-permute-start(bf16[256,512]{1,0:T(8,128)(2,1)S(1)} %get-tuple-element.68), channel_id=1, source_target_pairs={{0,1},{1,2},{2,3},{3,0},{4,5},{5,6},{6,7},{7,4},{8,9},{9,10},{10,1... | collective-permute-start | bytes 786440 | tf_op jit(solution)/shard_map/ppermute | solution.py:23
  53.1 15.1 %copy-start.6 = (bf16[1,2048,256]{2,1,0:T(8,128)(2,1)S(1)}, bf16[1,2048,256]{2,1,0:T(8,128)(2,1)}, u32[]{:S(2)}) copy-start(bf16[1,2048,256]{2,1,0:T(8,128)(2,1)} %param.45) | copy-start | bytes 3145732
  53.1 15.1 %copy-start.7 = (bf16[1,2048,256]{2,1,0:T(8,128)(2,1)S(1)}, bf16[1,2048,256]{2,1,0:T(8,128)(2,1)}, u32[]{:S(2)}) copy-start(bf16[1,2048,256]{2,1,0:T(8,128)(2,1)} %param.46) | copy-start | bytes 3145732
  53.1 15.1 %copy-start.14 = (f32[2048]{0:T(1024)S(1)}, f32[2048]{0:T(1024)}, u32[]{:S(2)}) copy-start(f32[2048]{0:T(1024)} %param.42) | copy-start | bytes 24580
  53.1 23.3 %copy-start.1 = (bf16[1,256,2048]{2,1,0:T(8,128)(2,1)S(1)}, bf16[1,256,2048]{2,1,0:T(8,128)(2,1)}, u32[]{:S(2)}) copy-start(bf16[1,256,2048]{2,1,0:T(8,128)(2,1)} %param.47) | copy-start | bytes 3145732
  53.2 9.9 %collective-permute-start.6 = (bf16[192,512]{1,0:T(8,128)(2,1)S(1)}, bf16[192,512]{1,0:T(8,128)(2,1)S(1)}, u32[]{:S(2)}, u32[]{:S(2)}) collective-permute-start(bf16[192,512]{1,0:T(8,128)(2,1)S(1)} %slice.25), channel_id=1, source_target_pairs={{0,3},{1,0},{2,1},{3,2},{4,7},{5,4},{6,5},{7,6},{8,11},{9,8},{10,9... | collective-permute-start | bytes 589832 | tf_op jit(solution)/shard_map/ppermute | solution.py:23
  55.6 12.6 %collective-permute-start.7 = (bf16[192,512]{1,0:T(8,128)(2,1)S(1)}, bf16[192,512]{1,0:T(8,128)(2,1)S(1)}, u32[]{:S(2)}, u32[]{:S(2)}) collective-permute-start(bf16[192,512]{1,0:T(8,128)(2,1)S(1)} %slice.25), channel_id=1, source_target_pairs={{0,1},{1,2},{2,3},{3,0},{4,5},{5,6},{6,7},{7,4},{8,9},{9,10},{10,1... | collective-permute-start | bytes 589832 | tf_op jit(solution)/shard_map/ppermute | solution.py:23
  55.6 15.0 %collective-permute-start.12 = (bf16[256,512]{1,0:T(8,128)(2,1)S(1)}, bf16[256,512]{1,0:T(8,128)(2,1)S(1)}, u32[]{:S(2)}, u32[]{:S(2)}) collective-permute-start(bf16[256,512]{1,0:T(8,128)(2,1)S(1)} %get-tuple-element.69), channel_id=1, source_target_pairs={{0,2},{1,3},{2,0},{3,1},{4,6},{5,7},{6,4},{7,5},{8,10},{9,11},{10,... | collective-permute-start | bytes 786440 | tf_op jit(solution)/shard_map/ppermute | solution.py:23
  56.9 13.8 %collective-permute-start.13 = (bf16[256,512]{1,0:T(8,128)(2,1)S(1)}, bf16[256,512]{1,0:T(8,128)(2,1)S(1)}, u32[]{:S(2)}, u32[]{:S(2)}) collective-permute-start(bf16[256,512]{1,0:T(8,128)(2,1)S(1)} %get-tuple-element.70), channel_id=1, source_target_pairs={{0,3},{1,0},{2,1},{3,2},{4,7},{5,4},{6,5},{7,6},{8,11},{9,8},{10,9... | collective-permute-start | bytes 786440 | tf_op jit(solution)/shard_map/ppermute | solution.py:23
  69.0 3.6 %collective-permute-start.10 = (bf16[192,256]{1,0:T(8,128)(2,1)S(1)}, bf16[192,256]{1,0:T(8,128)(2,1)S(1)}, u32[]{:S(2)}, u32[]{:S(2)}) collective-permute-start(bf16[192,256]{1,0:T(8,128)(2,1)S(1)} %shard_map.243.a0), channel_id=1, source_target_pairs={{0,3},{1,0},{2,1},{3,2},{4,7},{5,4},{6,5},{7,6},{8,11},{9,8},{10,9... | collective-permute-start | bytes 294920 | tf_op jit(solution)/shard_map/ppermute | solution.py:23
  69.1 4.8 %collective-permute-start.8 = (bf16[192,256]{1,0:T(8,128)(2,1)S(1)}, bf16[192,256]{1,0:T(8,128)(2,1)S(1)}, u32[]{:S(2)}, u32[]{:S(2)}) collective-permute-start(bf16[192,256]{1,0:T(8,128)(2,1)S(1)} %shard_map.243.a0), channel_id=1, source_target_pairs={{0,1},{1,2},{2,3},{3,0},{4,5},{5,6},{6,7},{7,4},{8,9},{9,10},{10,1... | collective-permute-start | bytes 294920 | tf_op jit(solution)/shard_map/ppermute | solution.py:23
  70.6 5.8 %collective-permute-start.9 = (bf16[192,256]{1,0:T(8,128)(2,1)S(1)}, bf16[192,256]{1,0:T(8,128)(2,1)S(1)}, u32[]{:S(2)}, u32[]{:S(2)}) collective-permute-start(bf16[192,256]{1,0:T(8,128)(2,1)S(1)} %shard_map.243.a0), channel_id=1, source_target_pairs={{0,2},{1,3},{2,0},{3,1},{4,6},{5,7},{6,4},{7,5},{8,10},{9,11},{10,... | collective-permute-start | bytes 294920 | tf_op jit(solution)/shard_map/ppermute | solution.py:23
  (3 other events, 26.6 us)

commit v7 on v6

--- a/solution.py
+++ b/solution.py
@@ -160,13 +160,10 @@
         centered * lax.rsqrt(variance + GROUP_EPS) * head_gain[...]
         + head_sums(receptance * blended * gains, same_head) * value
     ).astype(jnp.bfloat16)
-    for k, place in enumerate(places):
-        piece = jnp.dot(
+    for place, o in zip(places, (o0, o1, o2, o3)):
+        o[...] = jnp.dot(
             mixed, output_weight[:, pl.ds(place, block)], preferred_element_type=jnp.float32
         ).astype(jnp.bfloat16)
-        outs = (o0, o1, o2, o3)
-        outs[k][:, :block] = piece
-        outs[(k + 2) % 4][:, block:] = piece
     along_out[...] = along
     value_out[...] = value
     for out, vector in ((decay_out, decay), (removal_out, removed), (blended_out, blended)):
@@ -232,8 +229,7 @@
     weights_hbm,
     down_weight,
     dispatch,
-    high,
-    low,
+    combine,
     piece_1,
     piece_2,
     piece_3,
@@ -271,21 +267,57 @@
     column = lax.broadcasted_iota(jnp.int32, (sequences, sequences), 1)
     earlier = (row < column).astype(jnp.bfloat16)
     ranking = jnp.dot(named.astype(jnp.bfloat16), earlier, preferred_element_type=jnp.float32)
-    for c in range(CAPACITY):
-        rows = slice(c * experts, (c + 1) * experts)
-        here = jnp.where(ranking == c, named, 0.0)
-        dispatch[rows, :] = here.astype(jnp.bfloat16)
-        share = here * weight
-        first = share.astype(jnp.bfloat16)
-        high[rows, :] = first
-        low[rows, :] = (share - first.astype(jnp.float32)).astype(jnp.bfloat16)
+    here = [jnp.where(ranking == c, named, 0.0) for c in range(CAPACITY)]
+    dispatch[...] = jnp.concatenate(here, axis=0).astype(jnp.bfloat16)
+    share = jnp.concatenate([slot * weight for slot in here], axis=0).T
+    high = share.astype(jnp.bfloat16)
+    combine[:sequences, :] = high
+    combine[sequences:, :] = (share - high.astype(jnp.float32)).astype(jnp.bfloat16)
     for copy in copies:
         copy.wait()
 
 
-def hidden_kernel(at, x02, x1, x3, gain, gate_weight, up_weight, out):
-    width = x1.shape[1]
-    pieces = (x02[:, :width], x1[...], x02[:, width:], x3[...])
+def slots_of(blocks):
+    half = blocks.shape[0] // 2
+    width = blocks.shape[1] // 3 * 2
+    top, bottom = blocks[:half, :], blocks[half:, :]
+    middle = jnp.concatenate([top[:, width:], bottom[:, : width // 2]], axis=1)
+    return jnp.concatenate([top[:, :width], middle, bottom[:, width // 2 :]], axis=0)
+
+
+def put_slots(out, slots):
+    half = out.shape[0] // 2
+    width = out.shape[1] // 3 * 2
+    first, second, third = (slots[c * half : (c + 1) * half, :] for c in range(3))
+    out[:half, :width] = first
+    out[:half, width:] = second[:, : width // 2]
+    out[half:, : width // 2] = second[:, width // 2 :]
+    out[half:, width // 2 :] = third
+
+
+def dispatch_kernel(dispatch, rows, a0, a1, a2, a3, out, residual):
+    total = rows[: residual.shape[0], :].astype(jnp.float32)
+    for a in (a0, a1, a2, a3):
+        total = total + a[...].astype(jnp.float32)
+    residual[...] = total
+    slots = jnp.dot(
+        dispatch[...], total.astype(jnp.bfloat16), preferred_element_type=jnp.float32
+    )
+    put_slots(out, slots.astype(jnp.bfloat16))
+
+
+def finish_kernel(combine, returned, residual, out):
+    sequences = out.shape[0]
+    weighted = jnp.dot(
+        combine[...], slots_of(returned[...]), preferred_element_type=jnp.float32
+    )
+    total = residual[...] + weighted[:sequences] + weighted[sequences:]
+    out[...] = total.astype(jnp.bfloat16)
+
+
+def hidden_kernel(at, x0, x1, x2, x3, gain, gate_weight, up_weight, out):
+    pieces = [slots_of(x[...]) for x in (x0, x1, x2, x3)]
+    width = pieces[0].shape[1]
     places = [lax.rem(at[0] + k, 4) * width for k in range(4)]
     floats = [x.astype(jnp.float32) for x in pieces]
     squares = sum(jnp.sum(f * f, axis=1, keepdims=True) for f in floats)
@@ -303,12 +335,12 @@
 
 
 def down_kernel(at, a0, a1, a2, a3, w1, w2, w3, down_weight, out):
-    block = out.shape[1]
+    block = w1.shape[1]
     own = pl.ds(pl.multiple_of(at[0] * block, block), block)
     total = jnp.dot(a0[...], down_weight[:, own], preferred_element_type=jnp.float32)
     for a, w in ((a1, w1), (a2, w2), (a3, w3)):
         total = total + jnp.dot(a[...], w[...], preferred_element_type=jnp.float32)
-    out[...] = total.astype(jnp.bfloat16)
+    put_slots(out, total.astype(jnp.bfloat16))
 
 
 def local_call(kernel, shapes, limit, scratch=(), scalars=0, left=0, cost=None):
@@ -400,9 +432,10 @@
     flat_state = state.reshape(sequences, head_columns, state.shape[3])
     experts = expert_gate_weight.shape[0] * lax.axis_size("ep")
     slots = CAPACITY * experts
-    dispatch, high, low, down_1, down_2, down_3 = local_call(
+    dispatch, combine, down_1, down_2, down_3 = local_call(
         route_kernel,
-        [bfloat16(slots, sequences)] * 3 + [bfloat16(expert_down_weight.shape[1], own_columns)] * 3,
+        [bfloat16(slots, sequences), bfloat16(2 * sequences, slots)]
+        + [bfloat16(expert_down_weight.shape[1], own_columns)] * 3,
         4,
         [
             pltpu.VMEM(routes.shape[::-1], routes.dtype),
@@ -413,12 +446,12 @@
         left=3,
     )(at, routes.T, chosen_expert_weight.T, expert_down_weight[0])
 
-    dispatch, high, low, down_1, down_2, down_3, *row_pieces = lax.optimization_barrier(
-        (dispatch, high, low, down_1, down_2, down_3, *row_pieces)
+    dispatch, combine, down_1, down_2, down_3, *row_pieces = lax.optimization_barrier(
+        (dispatch, combine, down_1, down_2, down_3, *row_pieces)
     )
     *head_terms, decay, along, value, removed, blended = local_call(
         attention_kernel,
-        [bfloat16(sequences, 2 * own_columns)] * 4
+        [bfloat16(sequences, own_columns)] * 4
         + [float32(sequences * state.shape[1], 128)]
         + [float32(sequences, head_columns)] * 2
         + [float32(sequences * state.shape[1], 128)] * 2,
@@ -431,20 +464,21 @@
     )(at, *row_pieces, *needed, output_weight, flat_state)
     arrived = scattered(head_terms)
     down_pieces = scattered([None, down_1, down_2, down_3])[1:]
-    present = jnp.concatenate([row_pieces[0][:sequences], row_pieces[2][:sequences]], axis=1)
-    residual = present.astype(jnp.float32) + sum(a.astype(jnp.float32) for a in arrived)
-
-    outgoing = jnp.dot(
-        dispatch, residual.astype(jnp.bfloat16), preferred_element_type=jnp.float32
-    ).astype(jnp.bfloat16)
-    outgoing = outgoing.reshape(CAPACITY, experts, 2 * own_columns)
-    came = lax.all_to_all(outgoing, "ep", split_axis=1, concat_axis=1, tiled=True)
+    down_pieces = scattered([None, down_1, down_2, down_3])[1:]
+    residual = tokens.astype(jnp.float32) + sum(a.astype(jnp.float32) for a in arrived)
+
+    blocks = (2 * experts, 3 * own_columns // 2)
+    outgoing, residual = local_call(
+        dispatch_kernel, [bfloat16(*blocks), float32(sequences, own_columns)], 4
+    )(dispatch, both, *arrived)
+    exchanged = lambda value: lax.all_to_all(
+        value.reshape(2, experts, -1), "ep", split_axis=1, concat_axis=1, tiled=True
+    ).reshape(value.shape)
+    came = exchanged(outgoing)
     came, decay, removed, blended, along, value = lax.optimization_barrier(
         (came, decay, removed, blended, along, value)
     )
-    own_rows = came.reshape(CAPACITY * experts, 2 * own_columns)
-    one_slice = own_rows[:, :own_columns]
-    row_pieces = [own_rows, from_offset(one_slice, 1), from_offset(one_slice, 3)]
+    row_pieces = gathered(came)
     new_state = pl.pallas_call(
         renew_kernel,
         out_shape=float32(*flat_state.shape),
@@ -462,7 +496,7 @@
     new_state, *row_pieces = lax.optimization_barrier((new_state, *row_pieces))
     new_state = new_state.reshape(state.shape)
     activation = local_call(
-        hidden_kernel, bfloat16(own_rows.shape[0], expert_gate_weight.shape[2]), 12, scalars=1
+        hidden_kernel, bfloat16(slots, expert_gate_weight.shape[2]), 12, scalars=1
     )(
         at,
         *row_pieces,
@@ -472,18 +506,11 @@
     )
     act_pieces = scattered([activation] * 4)
     shares = local_call(
-        down_kernel, bfloat16(own_rows.shape[0], own_columns), 8, scalars=1
+        down_kernel, bfloat16(*blocks), 8, scalars=1
     )(at, *act_pieces, *down_pieces, expert_down_weight[0])
-    shares = shares.reshape(CAPACITY, experts, own_columns)
-    returned = lax.all_to_all(shares, "ep", split_axis=1, concat_axis=1, tiled=True)
-    returned = returned.reshape(CAPACITY * experts, own_columns)
-    weighted = lax.dot_general(
-        jnp.concatenate([high, low], axis=1),
-        returned,
-        (((0,), (0,)), ((), ())),
-        preferred_element_type=jnp.float32,
-    )
-    layer_out = (residual[:, :own_columns] + weighted[:sequences] + weighted[sequences:]).astype(jnp.bfloat16)
+    layer_out = local_call(
+        finish_kernel, bfloat16(sequences, own_columns), 4
+    )(combine, exchanged(shares), residual)
     return (layer_out, new_state)
 
 

time: 100 us -> 99 us (0.990)
  blocking collectives: 22 us -> 46.7 us
  waiting for transfers between devices: 32.6 us -> 10.8 us
  starting transfers between devices: 31.2 us -> 28.4 us
  local copies, waits for them, and re-layouts: 1.65 us -> 0.58 us
  Pallas kernels: 10.3 us -> 11.3 us
    all_to_all x1 -> x2, blocking collectives: 22 us -> 46.7 us  [shards(): lax.all_to_all(value.reshape(2, experts, -1), 'ep', split_axis=1, concat_...]
    all_to_all x1 -> x0, waiting for transfers between devices: 16.6 us -> none  [shards(): lax.all_to_all(outgoing, 'ep', split_axis=1, concat_axis=1, tiled=True)]
    all_to_all x1 -> x0, starting transfers between devices: 15.2 us -> none  [shards(): lax.all_to_all(outgoing, 'ep', split_axis=1, concat_axis=1, tiled=True)]
    ppermute x14 -> x15, starting transfers between devices: 16 us -> 28.4 us  [from_offset(): lax.ppermute(value, 'tp', [(i, (i - offset) % devices) for i in range(dev...]
    ppermute x14 -> x15, waiting for transfers between devices: 16 us -> 10.8 us  [from_offset(): lax.ppermute(value, 'tp', [(i, (i - offset) % devices) for i in range(dev...]
    pallas_call x6 -> x8, Pallas kernels: 5.61 us -> 6.56 us  [call(): pl.pallas_call(kernel, out_shape=shapes, in_specs=[pl.BlockSpec(memory_sp...]
  transfers between devices with their start and end apart: 15 -> 15, of which waited for: 10 -> 8; matrix products, arithmetic and copies ran while one was open for 0% -> 0% of each run, Pallas kernels for 7% -> 7%
where the time goes in v7:
time: 99 us; the launch traced here: 98.8 us
  blocking collectives  46.7 us (47%)
  starting transfers between devices  28.4 us (29%)
  Pallas kernels  11.3 us (11%)
  waiting for transfers between devices  10.8 us (11%)
  between operations  1.04 us (1%)
    all_to_all x2, blocking collectives, shards(): lax.all_to_all(value.reshape(2, experts, -1), 'ep', split_axis=1, concat_...  46.7 us
    ppermute x15, starting transfers between devices, from_offset(): lax.ppermute(value, 'tp', [(i, (i - offset) % devices) for i in range(dev...  28.4 us
    ppermute x15, waiting for transfers between devices, from_offset(): lax.ppermute(value, 'tp', [(i, (i - offset) % devices) for i in range(dev...  10.8 us
    pallas_call x8, Pallas kernels, call(): pl.pallas_call(kernel, out_shape=shapes, in_specs=[pl.BlockSpec(memory_sp...  6.56 us
    pallas_call x1, Pallas kernels, shards(): pl.pallas_call(renew_kernel, out_shape=float32(*flat_state.shape), in_spe...  4.72 us
  transfers between devices with their start and end apart: 15, of which 8 were waited for; matrix products, arithmetic and copies ran while one was open for 0% of the time, Pallas kernels for 7%

profile of v7, /device:TPU:1, one launch (start us, length us, event | category | flops | bytes accessed | tf_op | source)
XLA Modules:
  0.0 98.8 jit_solution(15411378308598250569)
XLA Ops:
  0.6 0.8 shard_map.240.rows
  1.6 3.4 %collective-permute-start = (bf16[64,512]{1,0:T(8,128)(2,1)S(1)}, bf16[64,512]{1,0:T(8,128)(2,1)S(1)}, u32[]{:S(2)}, u32[]{:S(2)}) collective-permute-start(bf16[64,512]{1,0:T(8,128)(2,1)S(1)} %shard_map.241.p0.rows), channel_id=1, source_target_pairs={{0,3},{1,0},{2,1},{3,2},{4,7},{5,4},{6,5},{7,6},{8,11},{9,8},{10,9... | collective-permute-start | bytes 196616 | tf_op jit(solution)/shard_map/ppermute | solution.py:23
  5.0 0.5 collective-permute-start.1
  5.5 0.6 collective-permute-start.2
  6.1 1.2 %shard_map.239 = (bf16[192,32]{1,0:T(8,128)(2,1)S(1)}, bf16[64,192]{1,0:T(8,128)(2,1)S(1)}, bf16[256,512]{1,0:T(8,128)(2,1)S(1)}, bf16[256,512]{1,0:T(8,128)(2,1)S(1)}, bf16[256,512]{1,0:T(8,128)(2,1)S(1)}) custom-call(s32[1]{0:T(128)} %bitcast.at, s32[4,32]{1,0:T(4,128)} %bitcast.38, f32[4,32]{1,0:T(4,128)} %bitcast.39, bf16[256,2048]{1,0:T(8,128)(2,1)} %bitcast.20), custom_call_target="tpu_custom_call" | custom-call | tf_op jit(solution)/shard_map/pallas_call | solution.py:353
  7.3 2.3 %collective-permute-done.1.p2 = bf16[64,512]{1,0:T(8,128)(2,1)S(1)} collective-permute-done((bf16[64,512]{1,0:T(8,128)(2,1)S(1)}, bf16[64,512]{1,0:T(8,128)(2,1)S(1)}, u32[]{:S(2)}, u32[]{:S(2)}) %collective-permute-start.1) | collective-permute-done | bytes 65568 | tf_op jit(solution)/shard_map/ppermute | solution.py:23
  9.7 0.7 collective-permute-done.2.p3
  10.5 2.5 %shard_map.242 = (bf16[32,512]{1,0:T(8,128)(2,1)S(1)}, bf16[32,512]{1,0:T(8,128)(2,1)S(1)}, bf16[32,512]{1,0:T(8,128)(2,1)S(1)}, bf16[32,512]{1,0:T(8,128)(2,1)S...) custom-call(s32[1]{0:T(128)} %bitcast.at, ...), custom_call_target="tpu_custom_call" | custom-call | tf_op jit(solution)/shard_map/pallas_call | solution.py:353
  13.0 1.7 %collective-permute-start.4 = (bf16[32,512]{1,0:T(8,128)(2,1)S(1)}, bf16[32,512]{1,0:T(8,128)(2,1)S(1)}, u32[]{:S(2)}, u32[]{:S(2)}) collective-permute-start(bf16[32,512]{1,0:T(8,128)(2,1)S(1)} %get-tuple-element.51), channel_id=1, source_target_pairs={{0,2},{1,3},{2,0},{3,1},{4,6},{5,7},{6,4},{7,5},{8,10},{9,11},{10,... | collective-permute-start | bytes 98312 | tf_op jit(solution)/shard_map/ppermute | solution.py:23
  14.8 1.8 %collective-permute-start.5 = (bf16[32,512]{1,0:T(8,128)(2,1)S(1)}, bf16[32,512]{1,0:T(8,128)(2,1)S(1)}, u32[]{:S(2)}, u32[]{:S(2)}) collective-permute-start(bf16[32,512]{1,0:T(8,128)(2,1)S(1)} %get-tuple-element.52), channel_id=1, source_target_pairs={{0,3},{1,0},{2,1},{3,2},{4,7},{5,4},{6,5},{7,6},{8,11},{9,8},{10,9... | collective-permute-start | bytes 98312 | tf_op jit(solution)/shard_map/ppermute | solution.py:23
  16.6 0.4 collective-permute-done.3.a1
  17.0 0.4 collective-permute-done.4.a2
  17.4 0.5 collective-permute-done.5.a3
  17.9 0.2 shard_map.243
  18.1 0.2 copy.26
  18.3 27.0 %all_to_all.10 = bf16[2,64,768]{2,0,1:T(2,128)(2,1)S(1)} all-to-all(bf16[2,64,768]{2,0,1:T(2,128)(2,1)S(1)} %copy.26), channel_id=1, replica_groups=mesh['ep'=64,'tp'=4] {'ep'}, dimensions={1} | all-to-all | bytes 393216 | tf_op jit(solution)/shard_map/all_to_all | solution.py:474
  45.4 2.5 %collective-permute-start.6 = (bf16[128,768]{1,0:T(8,128)(2,1)S(1)}, bf16[128,768]{1,0:T(8,128)(2,1)S(1)}, u32[]{:S(2)}, u32[]{:S(2)}) collective-permute-start(bf16[128,768]{1,0:T(8,128)(2,1)S(1)} %bitcast.24), channel_id=1, source_target_pairs={{0,3},{1,0},{2,1},{3,2},{4,7},{5,4},{6,5},{7,6},{8,11},{9,8},{10,9... | collective-permute-start | bytes 589832 | tf_op jit(solution)/shard_map/ppermute | solution.py:23
  47.9 1.3 %collective-permute-start.7 = (bf16[128,768]{1,0:T(8,128)(2,1)S(1)}, bf16[128,768]{1,0:T(8,128)(2,1)S(1)}, u32[]{:S(2)}, u32[]{:S(2)}) collective-permute-start(bf16[128,768]{1,0:T(8,128)(2,1)S(1)} %bitcast.25), channel_id=1, source_target_pairs={{0,2},{1,3},{2,0},{3,1},{4,6},{5,7},{6,4},{7,5},{8,10},{9,11},{10,... | collective-permute-start | bytes 589832 | tf_op jit(solution)/shard_map/ppermute | solution.py:23
  49.2 2.0 %collective-permute-start.8 = (bf16[128,768]{1,0:T(8,128)(2,1)S(1)}, bf16[128,768]{1,0:T(8,128)(2,1)S(1)}, u32[]{:S(2)}, u32[]{:S(2)}) collective-permute-start(bf16[128,768]{1,0:T(8,128)(2,1)S(1)} %bitcast.26), channel_id=1, source_target_pairs={{0,1},{1,2},{2,3},{3,0},{4,5},{5,6},{6,7},{7,4},{8,9},{9,10},{10,1... | collective-permute-start | bytes 589832 | tf_op jit(solution)/shard_map/ppermute | solution.py:23
  51.2 0.7 collective-permute-start.13
  51.9 12.1 %collective-permute-start.14 = (bf16[256,512]{1,0:T(8,128)(2,1)S(1)}, bf16[256,512]{1,0:T(8,128)(2,1)S(1)}, u32[]{:S(2)}, u32[]{:S(2)}) collective-permute-start(bf16[256,512]{1,0:T(8,128)(2,1)S(1)} %get-tuple-element.71), channel_id=1, source_target_pairs={{0,3},{1,0},{2,1},{3,2},{4,7},{5,4},{6,5},{7,6},{8,11},{9,8},{10,9... | collective-permute-start | bytes 786440 | tf_op jit(solution)/shard_map/ppermute | solution.py:23
  64.0 4.7 %renew.1 = f32[32,256,64]{2,1,0:T(8,128)} custom-call(f32[128,128]{1,0:T(8,128)S(1)} %get-tuple-element.59.decay, f32[128,128]{1,0:T(8,128)S(1)} %get-tuple-element.60.removed, f32[128,128]{1,0:T(8,128)S(1)} %get-tuple-element.61.blended, f32[32,256]{1,0:T(8,128)S(1)} %get-tuple-element.62.along, f32[32,256]{1,0:T(8,128)S(1)} %get-tuple-element.63.value, ...), custom_call_target="tpu_custom_call" | custom-call | tf_op jit(solution)/shard_map/renew/pallas_call | solution.py:482
  68.8 1.6 %collective-permute-done.8.x3 = bf16[128,768]{1,0:T(8,128)(2,1)S(1)} collective-permute-done((bf16[128,768]{1,0:T(8,128)(2,1)S(1)}, bf16[128,768]{1,0:T(8,128)(2,1)S(1)}, u32[]{:S(2)}, u32[]{:S(2)}) %collective-permute-start.8) | collective-permute-done | bytes 196640 | tf_op jit(solution)/shard_map/ppermute | solution.py:23
  70.4 0.8 shard_map.244.a0
  71.2 0.1 collective-permute-start.10
  71.4 1.4 %collective-permute-start.9 = (bf16[192,256]{1,0:T(8,128)(2,1)S(1)}, bf16[192,256]{1,0:T(8,128)(2,1)S(1)}, u32[]{:S(2)}, u32[]{:S(2)}) collective-permute-start(bf16[192,256]{1,0:T(8,128)(2,1)S(1)} %shard_map.244.a0), channel_id=1, source_target_pairs={{0,1},{1,2},{2,3},{3,0},{4,5},{5,6},{6,7},{7,4},{8,9},{9,10},{10,1... | collective-permute-start | bytes 294920 | tf_op jit(solution)/shard_map/ppermute | solution.py:23
  72.8 3.5 %collective-permute-done.10.a2 = bf16[192,256]{1,0:T(8,128)(2,1)S(1)} collective-permute-done((bf16[192,256]{1,0:T(8,128)(2,1)S(1)}, bf16[192,256]{1,0:T(8,128)(2,1)S(1)}, u32[]{:S(2)}, u32[]{:S(2)}) %collective-permute-start.10) | collective-permute-done | bytes 98336 | tf_op jit(solution)/shard_map/ppermute | solution.py:23
  76.3 1.4 %collective-permute-done.9.a1 = bf16[192,256]{1,0:T(8,128)(2,1)S(1)} collective-permute-done((bf16[192,256]{1,0:T(8,128)(2,1)S(1)}, bf16[192,256]{1,0:T(8,128)(2,1)S(1)}, u32[]{:S(2)}, u32[]{:S(2)}) %collective-permute-start.9) | collective-permute-done | bytes 98336 | tf_op jit(solution)/shard_map/ppermute | solution.py:23
  77.7 0.4 shard_map.245
  78.1 0.2 copy.28
  78.3 19.7 %all_to_all.11 = bf16[2,64,768]{2,0,1:T(2,128)(2,1)S(1)} all-to-all(bf16[2,64,768]{2,0,1:T(2,128)(2,1)S(1)} %copy.28), channel_id=1, replica_groups=mesh['ep'=64,'tp'=4] {'ep'}, dimensions={1} | all-to-all | bytes 393216 | tf_op jit(solution)/shard_map/all_to_all | solution.py:474
  98.0 0.8 shard_map.246
  (53 shorter events, 0.4 us)
Async XLA Ops:
  1.4 8.9 %copy-start = (f32[32,4,64,64]{3,2,1,0:T(8,128)S(1)}, f32[32,4,64,64]{3,2,1,0:T(8,128)}, u32[]{:S(2)}) copy-start(f32[32,4,64,64]{3,2,1,0:T(8,128)} %param.41) | copy-start | bytes 6291460
  1.4 8.9 %copy-start.2 = (bf16[2048,256]{1,0:T(8,128)(2,1)S(1)}, bf16[2048,256]{1,0:T(8,128)(2,1)}, u32[]{:S(2)}) copy-start(bf16[2048,256]{1,0:T(8,128)(2,1)} %receptance_weight.1) | copy-start | bytes 3145732
  1.5 8.9 %copy-start.3 = (bf16[2048,256]{1,0:T(8,128)(2,1)S(1)}, bf16[2048,256]{1,0:T(8,128)(2,1)}, u32[]{:S(2)}) copy-start(bf16[2048,256]{1,0:T(8,128)(2,1)} %key_weight.1) | copy-start | bytes 3145732
  1.5 8.9 %copy-start.4 = (bf16[2048,256]{1,0:T(8,128)(2,1)S(1)}, bf16[2048,256]{1,0:T(8,128)(2,1)}, u32[]{:S(2)}) copy-start(bf16[2048,256]{1,0:T(8,128)(2,1)} %value_weight.1) | copy-start | bytes 3145732
  1.5 8.9 %copy-start.5 = (bf16[256,2048]{1,0:T(8,128)(2,1)S(1)}, bf16[256,2048]{1,0:T(8,128)(2,1)}, u32[]{:S(2)}) copy-start(bf16[256,2048]{1,0:T(8,128)(2,1)} %output_weight.1) | copy-start | bytes 3145732
  1.5 8.9 %copy-start.8 = (bf16[2048,128]{1,0:T(8,128)(2,1)S(1)}, bf16[2048,128]{1,0:T(8,128)(2,1)}, u32[]{:S(2)}) copy-start(bf16[2048,128]{1,0:T(8,128)(2,1)} %decay_down.1) | copy-start | bytes 1572868
  1.5 8.9 %copy-start.9 = (bf16[2048,128]{1,0:T(8,128)(2,1)S(1)}, bf16[2048,128]{1,0:T(8,128)(2,1)}, u32[]{:S(2)}) copy-start(bf16[2048,128]{1,0:T(8,128)(2,1)} %strength_down.1) | copy-start | bytes 1572868
  1.5 8.9 %copy-start.10 = (bf16[128,1024]{1,0:T(8,128)(2,1)S(1)}, bf16[128,1024]{1,0:T(8,128)(2,1)}, u32[]{:S(2)}) copy-start(bf16[128,1024]{1,0:T(8,128)(2,1)} %decay_up.1) | copy-start | bytes 786436
  1.5 8.9 %copy-start.11 = (bf16[128,1024]{1,0:T(8,128)(2,1)S(1)}, bf16[128,1024]{1,0:T(8,128)(2,1)}, u32[]{:S(2)}) copy-start(bf16[128,1024]{1,0:T(8,128)(2,1)} %strength_up.1) | copy-start | bytes 786436
  1.5 8.9 %copy-start.12 = (f32[5,2048]{1,0:T(8,128)S(1)}, f32[5,2048]{1,0:T(8,128)}, u32[]{:S(2)}) copy-start(f32[5,2048]{1,0:T(8,128)} %share.1) | copy-start | bytes 122884
  1.6 8.9 %copy-start.13 = (f32[2048]{0:T(1024)S(1)}, f32[2048]{0:T(1024)}, u32[]{:S(2)}) copy-start(f32[2048]{0:T(1024)} %param.26) | copy-start | bytes 24580
  1.6 8.9 %copy-start.15 = (f32[4,64]{1,0:T(4,128)S(1)}, f32[4,64]{1,0:T(4,128)}, u32[]{:S(2)}) copy-start(f32[4,64]{1,0:T(4,128)} %self_weight.1) | copy-start | bytes 3076
  1.6 8.9 %copy-start.16 = (f32[256]{0:T(256)S(1)}, f32[256]{0:T(256)}, u32[]{:S(2)}) copy-start(f32[256]{0:T(256)} %param.33) | copy-start | bytes 3076
  1.6 5.7 %collective-permute-start = (bf16[64,512]{1,0:T(8,128)(2,1)S(1)}, bf16[64,512]{1,0:T(8,128)(2,1)S(1)}, u32[]{:S(2)}, u32[]{:S(2)}) collective-permute-start(bf16[64,512]{1,0:T(8,128)(2,1)S(1)} %shard_map.241.p0.rows), channel_id=1, source_target_pairs={{0,3},{1,0},{2,1},{3,2},{4,7},{5,4},{6,5},{7,6},{8,11},{9,8},{10,9... | collective-permute-start | bytes 196616 | tf_op jit(solution)/shard_map/ppermute | solution.py:23
  5.0 4.7 %collective-permute-start.1 = (bf16[64,512]{1,0:T(8,128)(2,1)S(1)}, bf16[64,512]{1,0:T(8,128)(2,1)S(1)}, u32[]{:S(2)}, u32[]{:S(2)}) collective-permute-start(bf16[64,512]{1,0:T(8,128)(2,1)S(1)} %shard_map.241.p0.rows), channel_id=1, source_target_pairs={{0,2},{1,3},{2,0},{3,1},{4,6},{5,7},{6,4},{7,5},{8,10},{9,11},{10,... | collective-permute-start | bytes 196616 | tf_op jit(solution)/shard_map/ppermute | solution.py:23
  5.5 4.8 %collective-permute-start.2 = (bf16[64,512]{1,0:T(8,128)(2,1)S(1)}, bf16[64,512]{1,0:T(8,128)(2,1)S(1)}, u32[]{:S(2)}, u32[]{:S(2)}) collective-permute-start(bf16[64,512]{1,0:T(8,128)(2,1)S(1)} %shard_map.241.p0.rows), channel_id=1, source_target_pairs={{0,1},{1,2},{2,3},{3,0},{4,5},{5,6},{6,7},{7,4},{8,9},{9,10},{10,1... | collective-permute-start | bytes 196616 | tf_op jit(solution)/shard_map/ppermute | solution.py:23
  12.9 4.0 %collective-permute-start.3 = (bf16[32,512]{1,0:T(8,128)(2,1)S(1)}, bf16[32,512]{1,0:T(8,128)(2,1)S(1)}, u32[]{:S(2)}, u32[]{:S(2)}) collective-permute-start(bf16[32,512]{1,0:T(8,128)(2,1)S(1)} %get-tuple-element.50), channel_id=1, source_target_pairs={{0,1},{1,2},{2,3},{3,0},{4,5},{5,6},{6,7},{7,4},{8,9},{9,10},{10,1... | collective-permute-start | bytes 98312 | tf_op jit(solution)/shard_map/ppermute | solution.py:23
  13.0 4.4 %collective-permute-start.4 = (bf16[32,512]{1,0:T(8,128)(2,1)S(1)}, bf16[32,512]{1,0:T(8,128)(2,1)S(1)}, u32[]{:S(2)}, u32[]{:S(2)}) collective-permute-start(bf16[32,512]{1,0:T(8,128)(2,1)S(1)} %get-tuple-element.51), channel_id=1, source_target_pairs={{0,2},{1,3},{2,0},{3,1},{4,6},{5,7},{6,4},{7,5},{8,10},{9,11},{10,... | collective-permute-start | bytes 98312 | tf_op jit(solution)/shard_map/ppermute | solution.py:23
  14.8 3.1 %collective-permute-start.5 = (bf16[32,512]{1,0:T(8,128)(2,1)S(1)}, bf16[32,512]{1,0:T(8,128)(2,1)S(1)}, u32[]{:S(2)}, u32[]{:S(2)}) collective-permute-start(bf16[32,512]{1,0:T(8,128)(2,1)S(1)} %get-tuple-element.52), channel_id=1, source_target_pairs={{0,3},{1,0},{2,1},{3,2},{4,7},{5,4},{6,5},{7,6},{8,11},{9,8},{10,9... | collective-permute-start | bytes 98312 | tf_op jit(solution)/shard_map/ppermute | solution.py:23
  45.3 25.0 %copy-start.6 = (bf16[1,2048,256]{2,1,0:T(8,128)(2,1)S(1)}, bf16[1,2048,256]{2,1,0:T(8,128)(2,1)}, u32[]{:S(2)}) copy-start(bf16[1,2048,256]{2,1,0:T(8,128)(2,1)} %param.45) | copy-start | bytes 3145732
  45.4 25.0 %copy-start.7 = (bf16[1,2048,256]{2,1,0:T(8,128)(2,1)S(1)}, bf16[1,2048,256]{2,1,0:T(8,128)(2,1)}, u32[]{:S(2)}) copy-start(bf16[1,2048,256]{2,1,0:T(8,128)(2,1)} %param.46) | copy-start | bytes 3145732
  45.4 25.0 %copy-start.14 = (f32[2048]{0:T(1024)S(1)}, f32[2048]{0:T(1024)}, u32[]{:S(2)}) copy-start(f32[2048]{0:T(1024)} %param.42) | copy-start | bytes 24580
  45.4 32.3 %copy-start.1 = (bf16[1,256,2048]{2,1,0:T(8,128)(2,1)S(1)}, bf16[1,256,2048]{2,1,0:T(8,128)(2,1)}, u32[]{:S(2)}) copy-start(bf16[1,256,2048]{2,1,0:T(8,128)(2,1)} %param.47) | copy-start | bytes 3145732
  45.4 6.5 %collective-permute-start.6 = (bf16[128,768]{1,0:T(8,128)(2,1)S(1)}, bf16[128,768]{1,0:T(8,128)(2,1)S(1)}, u32[]{:S(2)}, u32[]{:S(2)}) collective-permute-start(bf16[128,768]{1,0:T(8,128)(2,1)S(1)} %bitcast.24), channel_id=1, source_target_pairs={{0,3},{1,0},{2,1},{3,2},{4,7},{5,4},{6,5},{7,6},{8,11},{9,8},{10,9... | collective-permute-start | bytes 589832 | tf_op jit(solution)/shard_map/ppermute | solution.py:23
  47.9 23.4 %collective-permute-start.12 = (bf16[256,512]{1,0:T(8,128)(2,1)S(1)}, bf16[256,512]{1,0:T(8,128)(2,1)S(1)}, u32[]{:S(2)}, u32[]{:S(2)}) collective-permute-start(bf16[256,512]{1,0:T(8,128)(2,1)S(1)} %get-tuple-element.69), channel_id=1, source_target_pairs={{0,1},{1,2},{2,3},{3,0},{4,5},{5,6},{6,7},{7,4},{8,9},{9,10},{10,1... | collective-permute-start | bytes 786440 | tf_op jit(solution)/shard_map/ppermute | solution.py:23
  47.9 20.8 %collective-permute-start.7 = (bf16[128,768]{1,0:T(8,128)(2,1)S(1)}, bf16[128,768]{1,0:T(8,128)(2,1)S(1)}, u32[]{:S(2)}, u32[]{:S(2)}) collective-permute-start(bf16[128,768]{1,0:T(8,128)(2,1)S(1)} %bitcast.25), channel_id=1, source_target_pairs={{0,2},{1,3},{2,0},{3,1},{4,6},{5,7},{6,4},{7,5},{8,10},{9,11},{10,... | collective-permute-start | bytes 589832 | tf_op jit(solution)/shard_map/ppermute | solution.py:23
  49.2 21.2 %collective-permute-start.8 = (bf16[128,768]{1,0:T(8,128)(2,1)S(1)}, bf16[128,768]{1,0:T(8,128)(2,1)S(1)}, u32[]{:S(2)}, u32[]{:S(2)}) collective-permute-start(bf16[128,768]{1,0:T(8,128)(2,1)S(1)} %bitcast.26), channel_id=1, source_target_pairs={{0,1},{1,2},{2,3},{3,0},{4,5},{5,6},{6,7},{7,4},{8,9},{9,10},{10,1... | collective-permute-start | bytes 589832 | tf_op jit(solution)/shard_map/ppermute | solution.py:23
  51.2 21.6 %collective-permute-start.13 = (bf16[256,512]{1,0:T(8,128)(2,1)S(1)}, bf16[256,512]{1,0:T(8,128)(2,1)S(1)}, u32[]{:S(2)}, u32[]{:S(2)}) collective-permute-start(bf16[256,512]{1,0:T(8,128)(2,1)S(1)} %get-tuple-element.70), channel_id=1, source_target_pairs={{0,2},{1,3},{2,0},{3,1},{4,6},{5,7},{6,4},{7,5},{8,10},{9,11},{10,... | collective-permute-start | bytes 786440 | tf_op jit(solution)/shard_map/ppermute | solution.py:23
  51.9 20.9 %collective-permute-start.14 = (bf16[256,512]{1,0:T(8,128)(2,1)S(1)}, bf16[256,512]{1,0:T(8,128)(2,1)S(1)}, u32[]{:S(2)}, u32[]{:S(2)}) collective-permute-start(bf16[256,512]{1,0:T(8,128)(2,1)S(1)} %get-tuple-element.71), channel_id=1, source_target_pairs={{0,3},{1,0},{2,1},{3,2},{4,7},{5,4},{6,5},{7,6},{8,11},{9,8},{10,9... | collective-permute-start | bytes 786440 | tf_op jit(solution)/shard_map/ppermute | solution.py:23
  71.2 5.1 %collective-permute-start.10 = (bf16[192,256]{1,0:T(8,128)(2,1)S(1)}, bf16[192,256]{1,0:T(8,128)(2,1)S(1)}, u32[]{:S(2)}, u32[]{:S(2)}) collective-permute-start(bf16[192,256]{1,0:T(8,128)(2,1)S(1)} %shard_map.244.a0), channel_id=1, source_target_pairs={{0,2},{1,3},{2,0},{3,1},{4,6},{5,7},{6,4},{7,5},{8,10},{9,11},{10,... | collective-permute-start | bytes 294920 | tf_op jit(solution)/shard_map/ppermute | solution.py:23
  71.3 5.0 %collective-permute-start.11 = (bf16[192,256]{1,0:T(8,128)(2,1)S(1)}, bf16[192,256]{1,0:T(8,128)(2,1)S(1)}, u32[]{:S(2)}, u32[]{:S(2)}) collective-permute-start(bf16[192,256]{1,0:T(8,128)(2,1)S(1)} %shard_map.244.a0), channel_id=1, source_target_pairs={{0,3},{1,0},{2,1},{3,2},{4,7},{5,4},{6,5},{7,6},{8,11},{9,8},{10,9... | collective-permute-start | bytes 294920 | tf_op jit(solution)/shard_map/ppermute | solution.py:23
  71.4 6.3 %collective-permute-start.9 = (bf16[192,256]{1,0:T(8,128)(2,1)S(1)}, bf16[192,256]{1,0:T(8,128)(2,1)S(1)}, u32[]{:S(2)}, u32[]{:S(2)}) collective-permute-start(bf16[192,256]{1,0:T(8,128)(2,1)S(1)} %shard_map.244.a0), channel_id=1, source_target_pairs={{0,1},{1,2},{2,3},{3,0},{4,5},{5,6},{6,7},{7,4},{8,9},{9,10},{10,1... | collective-permute-start | bytes 294920 | tf_op jit(solution)/shard_map/ppermute | solution.py:23
  (3 other events, 26.6 us)

commit v8 on v7

--- a/solution.py
+++ b/solution.py
@@ -315,22 +315,36 @@
     out[...] = total.astype(jnp.bfloat16)
 
 
-def hidden_kernel(at, x0, x1, x2, x3, gain, gate_weight, up_weight, out):
-    pieces = [slots_of(x[...]) for x in (x0, x1, x2, x3)]
-    width = pieces[0].shape[1]
-    places = [lax.rem(at[0] + k, 4) * width for k in range(4)]
-    floats = [x.astype(jnp.float32) for x in pieces]
-    squares = sum(jnp.sum(f * f, axis=1, keepdims=True) for f in floats)
-    scale = lax.rsqrt(squares / (4 * width) + NORM_EPS)
-    gate = jnp.zeros(out.shape, jnp.float32)
-    up = jnp.zeros(out.shape, jnp.float32)
-    for f, place in zip(floats, places):
-        rows = pl.ds(pl.multiple_of(place, width), width)
-        x = (f * scale * gain[:, rows]).astype(jnp.bfloat16)
-        gate = gate + jnp.dot(x, gate_weight[rows, :], preferred_element_type=jnp.float32)
-        up = up + jnp.dot(x, up_weight[rows, :], preferred_element_type=jnp.float32)
-    gate = jnp.minimum(gate, GATE_LIMIT)
-    up = jnp.clip(up, -GATE_LIMIT, GATE_LIMIT)
+def early_kernel(at, x0, x2, x3, gain, gate_weight, up_weight, gate, up, squares):
+    gate_sum = up_sum = total = None
+    for k, piece in ((0, x0), (2, x2), (3, x3)):
+        part = product_of(at, k, piece, gain, gate_weight, up_weight)
+        if total is None:
+            gate_sum, up_sum, total = part
+        else:
+            gate_sum, up_sum, total = gate_sum + part[0], up_sum + part[1], total + part[2]
+    gate[...] = gate_sum
+    up[...] = up_sum
+    squares[...] = jnp.broadcast_to(total, squares.shape)
+
+
+def product_of(at, k, piece, gain, gate_weight, up_weight):
+    x = slots_of(piece[...]).astype(jnp.float32)
+    width = x.shape[1]
+    rows = pl.ds(pl.multiple_of(lax.rem(at[0] + k, 4) * width, width), width)
+    scaled = (x * gain[:, rows]).astype(jnp.bfloat16)
+    return (
+        jnp.dot(scaled, gate_weight[rows, :], preferred_element_type=jnp.float32),
+        jnp.dot(scaled, up_weight[rows, :], preferred_element_type=jnp.float32),
+        jnp.sum(x * x, axis=1, keepdims=True),
+    )
+
+
+def hidden_kernel(at, x1, gate_sum, up_sum, squares, gain, gate_weight, up_weight, out):
+    gate, up, total = product_of(at, 1, x1, gain, gate_weight, up_weight)
+    scale = lax.rsqrt((total + squares[:, :1]) / gate_weight.shape[0] + NORM_EPS)
+    gate = jnp.minimum((gate + gate_sum[...]) * scale, GATE_LIMIT)
+    up = jnp.clip((up + up_sum[...]) * scale, -GATE_LIMIT, GATE_LIMIT)
     out[...] = ((up + 1.0) * gate * jax.nn.sigmoid(GATE_SLOPE * gate)).astype(jnp.bfloat16)
 
 
@@ -446,9 +460,8 @@
         left=3,
     )(at, routes.T, chosen_expert_weight.T, expert_down_weight[0])
 
-    dispatch, combine, down_1, down_2, down_3, *row_pieces = lax.optimization_barrier(
-        (dispatch, combine, down_1, down_2, down_3, *row_pieces)
-    )
+    down_pieces = scattered([None, down_1, down_2, down_3])[1:]
+    dispatch, combine, *row_pieces = lax.optimization_barrier((dispatch, combine, *row_pieces))
     *head_terms, decay, along, value, removed, blended = local_call(
         attention_kernel,
         [bfloat16(sequences, own_columns)] * 4
@@ -464,7 +477,6 @@
     )(at, *row_pieces, *needed, output_weight, flat_state)
     arrived = scattered(head_terms)
     down_pieces = scattered([None, down_1, down_2, down_3])[1:]
-    down_pieces = scattered([None, down_1, down_2, down_3])[1:]
     residual = tokens.astype(jnp.float32) + sum(a.astype(jnp.float32) for a in arrived)
 
     blocks = (2 * experts, 3 * own_columns // 2)
@@ -493,17 +505,16 @@
         compiler_params=pltpu.CompilerParams(vmem_limit_bytes=12 * MIB),
         name="renew",
     )(decay, removed, blended, along, value, pltpu.with_memory_space_constraint(flat_state, pltpu.HBM))
-    new_state, *row_pieces = lax.optimization_barrier((new_state, *row_pieces))
+    new_state, row_pieces[1] = lax.optimization_barrier((new_state, row_pieces[1]))
     new_state = new_state.reshape(state.shape)
+    hidden_columns = expert_gate_weight.shape[2]
+    expert_weights = (vector(second_norm_gain), expert_gate_weight[0], expert_up_weight[0])
+    early = local_call(
+        early_kernel, [float32(slots, hidden_columns)] * 2 + [float32(slots, 128)], 12, scalars=1
+    )(at, row_pieces[0], row_pieces[2], row_pieces[3], *expert_weights)
     activation = local_call(
-        hidden_kernel, bfloat16(slots, expert_gate_weight.shape[2]), 12, scalars=1
-    )(
-        at,
-        *row_pieces,
-        vector(second_norm_gain),
-        expert_gate_weight[0],
-        expert_up_weight[0],
-    )
+        hidden_kernel, bfloat16(slots, hidden_columns), 12, scalars=1
+    )(at, row_pieces[1], *early, *expert_weights)
     act_pieces = scattered([activation] * 4)
     shares = local_call(
         down_kernel, bfloat16(*blocks), 8, scalars=1

time: 99 us -> 99 us (level)
  starting transfers between devices: 28.4 us -> 19 us
  blocking collectives: 46.7 us -> 51.9 us
  waiting for transfers between devices: 10.8 us -> 14.9 us
    ppermute x15, starting transfers between devices: 28.4 us -> 19 us  [from_offset(): lax.ppermute(value, 'tp', [(i, (i - offset) % devices) for i in range(dev...]
    all_to_all x2, blocking collectives: 46.7 us -> 51.9 us  [shards(): lax.all_to_all(value.reshape(2, experts, -1), 'ep', split_axis=1, concat_...]
    ppermute x15, waiting for transfers between devices: 10.8 us -> 14.9 us  [from_offset(): lax.ppermute(value, 'tp', [(i, (i - offset) % devices) for i in range(dev...]
    pallas_call x8 -> x9, Pallas kernels: 6.56 us -> 6.62 us  [call(): pl.pallas_call(kernel, out_shape=shapes, in_specs=[pl.BlockSpec(memory_sp...]
  transfers between devices with their start and end apart: 15 -> 15, of which waited for: 8 -> 12; matrix products, arithmetic and copies ran while one was open for 0% -> 0% of each run, Pallas kernels for 7% -> 7%
where the time goes in v8:
time: 99 us; the launch traced here: 98.7 us
  blocking collectives  51.9 us (52%)
  starting transfers between devices  19 us (19%)
  waiting for transfers between devices  14.9 us (15%)
  Pallas kernels  11.3 us (11%)
  between operations  1 us (1%)
    all_to_all x2, blocking collectives, shards(): lax.all_to_all(value.reshape(2, experts, -1), 'ep', split_axis=1, concat_...  51.9 us
    ppermute x15, starting transfers between devices, from_offset(): lax.ppermute(value, 'tp', [(i, (i - offset) % devices) for i in range(dev...  19 us
    ppermute x15, waiting for transfers between devices, from_offset(): lax.ppermute(value, 'tp', [(i, (i - offset) % devices) for i in range(dev...  14.9 us
    pallas_call x9, Pallas kernels, call(): pl.pallas_call(kernel, out_shape=shapes, in_specs=[pl.BlockSpec(memory_sp...  6.62 us
    pallas_call x1, Pallas kernels, shards(): pl.pallas_call(renew_kernel, out_shape=float32(*flat_state.shape), in_spe...  4.72 us
  transfers between devices with their start and end apart: 15, of which 12 were waited for; matrix products, arithmetic and copies ran while one was open for 0% of the time, Pallas kernels for 7%

profile of v8, /device:TPU:1, one launch (start us, length us, event | category | flops | bytes accessed | tf_op | source)
XLA Modules:
  0.0 98.7 jit_solution(2388633279799884614)
XLA Ops:
  0.6 0.8 shard_map.240.rows
  1.6 2.1 %collective-permute-start.2 = (bf16[64,512]{1,0:T(8,128)(2,1)S(1)}, bf16[64,512]{1,0:T(8,128)(2,1)S(1)}, u32[]{:S(2)}, u32[]{:S(2)}) collective-permute-start(bf16[64,512]{1,0:T(8,128)(2,1)S(1)} %shard_map.241.p0.rows), channel_id=1, source_target_pairs={{0,1},{1,2},{2,3},{3,0},{4,5},{5,6},{6,7},{7,4},{8,9},{9,10},{10,1... | collective-permute-start | bytes 196616 | tf_op jit(solution)/shard_map/ppermute | solution.py:23
  3.7 2.5 %collective-permute-start.1 = (bf16[64,512]{1,0:T(8,128)(2,1)S(1)}, bf16[64,512]{1,0:T(8,128)(2,1)S(1)}, u32[]{:S(2)}, u32[]{:S(2)}) collective-permute-start(bf16[64,512]{1,0:T(8,128)(2,1)S(1)} %shard_map.241.p0.rows), channel_id=1, source_target_pairs={{0,2},{1,3},{2,0},{3,1},{4,6},{5,7},{6,4},{7,5},{8,10},{9,11},{10,... | collective-permute-start | bytes 196616 | tf_op jit(solution)/shard_map/ppermute | solution.py:23
  6.2 1.2 %collective-permute-start = (bf16[64,512]{1,0:T(8,128)(2,1)S(1)}, bf16[64,512]{1,0:T(8,128)(2,1)S(1)}, u32[]{:S(2)}, u32[]{:S(2)}) collective-permute-start(bf16[64,512]{1,0:T(8,128)(2,1)S(1)} %shard_map.241.p0.rows), channel_id=1, source_target_pairs={{0,3},{1,0},{2,1},{3,2},{4,7},{5,4},{6,5},{7,6},{8,11},{9,8},{10,9... | collective-permute-start | bytes 196616 | tf_op jit(solution)/shard_map/ppermute | solution.py:23
  7.4 1.2 %shard_map.239 = (bf16[192,32]{1,0:T(8,128)(2,1)S(1)}, bf16[64,192]{1,0:T(8,128)(2,1)S(1)}, bf16[256,512]{1,0:T(8,128)(2,1)S(1)}, bf16[256,512]{1,0:T(8,128)(2,1)S(1)}, bf16[256,512]{1,0:T(8,128)(2,1)S(1)}) custom-call(s32[1]{0:T(128)} %bitcast.at, s32[4,32]{1,0:T(4,128)} %bitcast.41, f32[4,32]{1,0:T(4,128)} %bitcast.42, bf16[256,2048]{1,0:T(8,128)(2,1)} %bitcast.24), custom_call_target="tpu_custom_call" | custom-call | tf_op jit(solution)/shard_map/pallas_call | solution.py:367
  8.6 0.3 collective-permute-done.1.p2
  8.8 0.8 collective-permute-done.p1
  9.8 2.5 %shard_map.242 = (bf16[32,512]{1,0:T(8,128)(2,1)S(1)}, bf16[32,512]{1,0:T(8,128)(2,1)S(1)}, bf16[32,512]{1,0:T(8,128)(2,1)S(1)}, bf16[32,512]{1,0:T(8,128)(2,1)S...) custom-call(s32[1]{0:T(128)} %bitcast.at, ...), custom_call_target="tpu_custom_call" | custom-call | tf_op jit(solution)/shard_map/pallas_call | solution.py:367
  12.3 3.2 %collective-permute-start.4 = (bf16[32,512]{1,0:T(8,128)(2,1)S(1)}, bf16[32,512]{1,0:T(8,128)(2,1)S(1)}, u32[]{:S(2)}, u32[]{:S(2)}) collective-permute-start(bf16[32,512]{1,0:T(8,128)(2,1)S(1)} %get-tuple-element.45), channel_id=1, source_target_pairs={{0,2},{1,3},{2,0},{3,1},{4,6},{5,7},{6,4},{7,5},{8,10},{9,11},{10,... | collective-permute-start | bytes 98312 | tf_op jit(solution)/shard_map/ppermute | solution.py:23
  15.6 0.6 collective-permute-done.3.a1
  16.3 0.9 collective-permute-done.4.a2
  17.2 1.1 %collective-permute-done.5.a3 = bf16[32,512]{1,0:T(8,128)(2,1)S(1)} collective-permute-done((bf16[32,512]{1,0:T(8,128)(2,1)S(1)}, bf16[32,512]{1,0:T(8,128)(2,1)S(1)}, u32[]{:S(2)}, u32[]{:S(2)}) %collective-permute-start.5) | collective-permute-done | bytes 32800 | tf_op jit(solution)/shard_map/ppermute | solution.py:23
  18.7 27.5 %all_to_all.10 = bf16[2,64,768]{2,0,1:T(2,128)(2,1)S(1)} all-to-all(bf16[2,64,768]{2,0,1:T(2,128)(2,1)S(1)} %copy.26), channel_id=1, replica_groups=mesh['ep'=64,'tp'=4] {'ep'}, dimensions={1} | all-to-all | bytes 393216 | tf_op jit(solution)/shard_map/all_to_all | solution.py:486
  46.3 1.1 %collective-permute-start.6 = (bf16[128,768]{1,0:T(8,128)(2,1)S(1)}, bf16[128,768]{1,0:T(8,128)(2,1)S(1)}, u32[]{:S(2)}, u32[]{:S(2)}) collective-permute-start(bf16[128,768]{1,0:T(8,128)(2,1)S(1)} %bitcast.26), channel_id=1, source_target_pairs={{0,3},{1,0},{2,1},{3,2},{4,7},{5,4},{6,5},{7,6},{8,11},{9,8},{10,9... | collective-permute-start | bytes 589832 | tf_op jit(solution)/shard_map/ppermute | solution.py:23
  47.4 0.4 collective-permute-start.12
  47.9 3.4 %collective-permute-start.7 = (bf16[128,768]{1,0:T(8,128)(2,1)S(1)}, bf16[128,768]{1,0:T(8,128)(2,1)S(1)}, u32[]{:S(2)}, u32[]{:S(2)}) collective-permute-start(bf16[128,768]{1,0:T(8,128)(2,1)S(1)} %bitcast.28), channel_id=1, source_target_pairs={{0,2},{1,3},{2,0},{3,1},{4,6},{5,7},{6,4},{7,5},{8,10},{9,11},{10,... | collective-permute-start | bytes 589832 | tf_op jit(solution)/shard_map/ppermute | solution.py:23
  51.3 1.2 %collective-permute-done.6.x1 = bf16[128,768]{1,0:T(8,128)(2,1)S(1)} collective-permute-done((bf16[128,768]{1,0:T(8,128)(2,1)S(1)}, bf16[128,768]{1,0:T(8,128)(2,1)S(1)}, u32[]{:S(2)}, u32[]{:S(2)}) %collective-permute-start.6) | collective-permute-done | bytes 196640 | tf_op jit(solution)/shard_map/ppermute | solution.py:23
  52.4 2.2 %collective-permute-start.14 = (bf16[256,512]{1,0:T(8,128)(2,1)S(1)}, bf16[256,512]{1,0:T(8,128)(2,1)S(1)}, u32[]{:S(2)}, u32[]{:S(2)}) collective-permute-start(bf16[256,512]{1,0:T(8,128)(2,1)S(1)} %get-tuple-element.65), channel_id=1, source_target_pairs={{0,3},{1,0},{2,1},{3,2},{4,7},{5,4},{6,5},{7,6},{8,11},{9,8},{10,9... | collective-permute-start | bytes 786440 | tf_op jit(solution)/shard_map/ppermute | solution.py:23
  54.7 4.7 %renew.1 = f32[32,256,64]{2,1,0:T(8,128)} custom-call(f32[128,128]{1,0:T(8,128)S(1)} %get-tuple-element.53.decay, f32[128,128]{1,0:T(8,128)S(1)} %get-tuple-element.54.removed, f32[128,128]{1,0:T(8,128)S(1)} %get-tuple-element.55.blended, f32[32,256]{1,0:T(8,128)S(1)} %get-tuple-element.56.along, f32[32,256]{1,0:T(8,128)S(1)} %get-tuple-element.57.value, ...), custom_call_target="tpu_custom_call" | custom-call | tf_op jit(solution)/shard_map/renew/pallas_call | solution.py:494
  59.4 1.6 %collective-permute-done.8.x3 = bf16[128,768]{1,0:T(8,128)(2,1)S(1)} collective-permute-done((bf16[128,768]{1,0:T(8,128)(2,1)S(1)}, bf16[128,768]{1,0:T(8,128)(2,1)S(1)}, u32[]{:S(2)}, u32[]{:S(2)}) %collective-permute-start.8) | collective-permute-done | bytes 196640 | tf_op jit(solution)/shard_map/ppermute | solution.py:23
  61.0 2.3 %collective-permute-done.7.x2 = bf16[128,768]{1,0:T(8,128)(2,1)S(1)} collective-permute-done((bf16[128,768]{1,0:T(8,128)(2,1)S(1)}, bf16[128,768]{1,0:T(8,128)(2,1)S(1)}, u32[]{:S(2)}, u32[]{:S(2)}) %collective-permute-start.7) | collective-permute-done | bytes 196640 | tf_op jit(solution)/shard_map/ppermute | solution.py:23
  63.3 0.5 shard_map.244
  63.8 0.3 shard_map.245.a0
  64.2 1.8 %collective-permute-start.10 = (bf16[192,256]{1,0:T(8,128)(2,1)S(1)}, bf16[192,256]{1,0:T(8,128)(2,1)S(1)}, u32[]{:S(2)}, u32[]{:S(2)}) collective-permute-start(bf16[192,256]{1,0:T(8,128)(2,1)S(1)} %shard_map.245.a0), channel_id=1, source_target_pairs={{0,2},{1,3},{2,0},{3,1},{4,6},{5,7},{6,4},{7,5},{8,10},{9,11},{10,... | collective-permute-start | bytes 294920 | tf_op jit(solution)/shard_map/ppermute | solution.py:23
  66.0 0.8 collective-permute-start.9
  66.7 2.2 %collective-permute-done.13.w2 = bf16[256,512]{1,0:T(8,128)(2,1)S(1)} collective-permute-done((bf16[256,512]{1,0:T(8,128)(2,1)S(1)}, bf16[256,512]{1,0:T(8,128)(2,1)S(1)}, u32[]{:S(2)}, u32[]{:S(2)}) %collective-permute-start.13) | collective-permute-done | bytes 262176 | tf_op jit(solution)/shard_map/ppermute | solution.py:23
  68.9 1.0 collective-permute-done.11.a3
  69.8 1.1 %collective-permute-done.10.a2 = bf16[192,256]{1,0:T(8,128)(2,1)S(1)} collective-permute-done((bf16[192,256]{1,0:T(8,128)(2,1)S(1)}, bf16[192,256]{1,0:T(8,128)(2,1)S(1)}, u32[]{:S(2)}, u32[]{:S(2)}) %collective-permute-start.10) | collective-permute-done | bytes 98336 | tf_op jit(solution)/shard_map/ppermute | solution.py:23
  71.0 1.9 %collective-permute-done.9.a1 = bf16[192,256]{1,0:T(8,128)(2,1)S(1)} collective-permute-done((bf16[192,256]{1,0:T(8,128)(2,1)S(1)}, bf16[192,256]{1,0:T(8,128)(2,1)S(1)}, u32[]{:S(2)}, u32[]{:S(2)}) %collective-permute-start.9) | collective-permute-done | bytes 98336 | tf_op jit(solution)/shard_map/ppermute | solution.py:23
  72.9 0.4 shard_map.246
  73.5 24.4 %all_to_all.11 = bf16[2,64,768]{2,0,1:T(2,128)(2,1)S(1)} all-to-all(bf16[2,64,768]{2,0,1:T(2,128)(2,1)S(1)} %copy.28), channel_id=1, replica_groups=mesh['ep'=64,'tp'=4] {'ep'}, dimensions={1} | all-to-all | bytes 393216 | tf_op jit(solution)/shard_map/all_to_all | solution.py:486
  97.9 0.8 shard_map.247
  (54 shorter events, 1.1 us)
Async XLA Ops:
  1.4 8.2 %copy-start = (f32[32,4,64,64]{3,2,1,0:T(8,128)S(1)}, f32[32,4,64,64]{3,2,1,0:T(8,128)}, u32[]{:S(2)}) copy-start(f32[32,4,64,64]{3,2,1,0:T(8,128)} %param.41) | copy-start | bytes 6291460
  1.4 8.2 %copy-start.4 = (bf16[2048,256]{1,0:T(8,128)(2,1)S(1)}, bf16[2048,256]{1,0:T(8,128)(2,1)}, u32[]{:S(2)}) copy-start(bf16[2048,256]{1,0:T(8,128)(2,1)} %receptance_weight.1) | copy-start | bytes 3145732
  1.5 8.2 %copy-start.5 = (bf16[2048,256]{1,0:T(8,128)(2,1)S(1)}, bf16[2048,256]{1,0:T(8,128)(2,1)}, u32[]{:S(2)}) copy-start(bf16[2048,256]{1,0:T(8,128)(2,1)} %key_weight.1) | copy-start | bytes 3145732
  1.5 8.2 %copy-start.6 = (bf16[2048,256]{1,0:T(8,128)(2,1)S(1)}, bf16[2048,256]{1,0:T(8,128)(2,1)}, u32[]{:S(2)}) copy-start(bf16[2048,256]{1,0:T(8,128)(2,1)} %value_weight.1) | copy-start | bytes 3145732
  1.5 8.2 %copy-start.7 = (bf16[256,2048]{1,0:T(8,128)(2,1)S(1)}, bf16[256,2048]{1,0:T(8,128)(2,1)}, u32[]{:S(2)}) copy-start(bf16[256,2048]{1,0:T(8,128)(2,1)} %output_weight.1) | copy-start | bytes 3145732
  1.5 8.1 %copy-start.8 = (bf16[2048,128]{1,0:T(8,128)(2,1)S(1)}, bf16[2048,128]{1,0:T(8,128)(2,1)}, u32[]{:S(2)}) copy-start(bf16[2048,128]{1,0:T(8,128)(2,1)} %decay_down.1) | copy-start | bytes 1572868
  1.5 8.1 %copy-start.9 = (bf16[2048,128]{1,0:T(8,128)(2,1)S(1)}, bf16[2048,128]{1,0:T(8,128)(2,1)}, u32[]{:S(2)}) copy-start(bf16[2048,128]{1,0:T(8,128)(2,1)} %strength_down.1) | copy-start | bytes 1572868
  1.5 8.1 %copy-start.10 = (bf16[128,1024]{1,0:T(8,128)(2,1)S(1)}, bf16[128,1024]{1,0:T(8,128)(2,1)}, u32[]{:S(2)}) copy-start(bf16[128,1024]{1,0:T(8,128)(2,1)} %decay_up.1) | copy-start | bytes 786436
  1.5 8.1 %copy-start.11 = (bf16[128,1024]{1,0:T(8,128)(2,1)S(1)}, bf16[128,1024]{1,0:T(8,128)(2,1)}, u32[]{:S(2)}) copy-start(bf16[128,1024]{1,0:T(8,128)(2,1)} %strength_up.1) | copy-start | bytes 786436
  1.5 8.1 %copy-start.12 = (f32[5,2048]{1,0:T(8,128)S(1)}, f32[5,2048]{1,0:T(8,128)}, u32[]{:S(2)}) copy-start(f32[5,2048]{1,0:T(8,128)} %share.1) | copy-start | bytes 122884
  1.6 8.1 %copy-start.14 = (f32[2048]{0:T(1024)S(1)}, f32[2048]{0:T(1024)}, u32[]{:S(2)}) copy-start(f32[2048]{0:T(1024)} %param.26) | copy-start | bytes 24580
  1.6 8.1 %copy-start.15 = (f32[4,64]{1,0:T(4,128)S(1)}, f32[4,64]{1,0:T(4,128)}, u32[]{:S(2)}) copy-start(f32[4,64]{1,0:T(4,128)} %self_weight.1) | copy-start | bytes 3076
  1.6 8.1 %copy-start.16 = (f32[256]{0:T(256)S(1)}, f32[256]{0:T(256)}, u32[]{:S(2)}) copy-start(f32[256]{0:T(256)} %param.33) | copy-start | bytes 3076
  1.6 6.9 %collective-permute-start.2 = (bf16[64,512]{1,0:T(8,128)(2,1)S(1)}, bf16[64,512]{1,0:T(8,128)(2,1)S(1)}, u32[]{:S(2)}, u32[]{:S(2)}) collective-permute-start(bf16[64,512]{1,0:T(8,128)(2,1)S(1)} %shard_map.241.p0.rows), channel_id=1, source_target_pairs={{0,1},{1,2},{2,3},{3,0},{4,5},{5,6},{6,7},{7,4},{8,9},{9,10},{10,1... | collective-permute-start | bytes 196616 | tf_op jit(solution)/shard_map/ppermute | solution.py:23
  3.7 5.1 %collective-permute-start.1 = (bf16[64,512]{1,0:T(8,128)(2,1)S(1)}, bf16[64,512]{1,0:T(8,128)(2,1)S(1)}, u32[]{:S(2)}, u32[]{:S(2)}) collective-permute-start(bf16[64,512]{1,0:T(8,128)(2,1)S(1)} %shard_map.241.p0.rows), channel_id=1, source_target_pairs={{0,2},{1,3},{2,0},{3,1},{4,6},{5,7},{6,4},{7,5},{8,10},{9,11},{10,... | collective-permute-start | bytes 196616 | tf_op jit(solution)/shard_map/ppermute | solution.py:23
  6.2 3.4 %collective-permute-start = (bf16[64,512]{1,0:T(8,128)(2,1)S(1)}, bf16[64,512]{1,0:T(8,128)(2,1)S(1)}, u32[]{:S(2)}, u32[]{:S(2)}) collective-permute-start(bf16[64,512]{1,0:T(8,128)(2,1)S(1)} %shard_map.241.p0.rows), channel_id=1, source_target_pairs={{0,3},{1,0},{2,1},{3,2},{4,7},{5,4},{6,5},{7,6},{8,11},{9,8},{10,9... | collective-permute-start | bytes 196616 | tf_op jit(solution)/shard_map/ppermute | solution.py:23
  12.2 4.0 %collective-permute-start.3 = (bf16[32,512]{1,0:T(8,128)(2,1)S(1)}, bf16[32,512]{1,0:T(8,128)(2,1)S(1)}, u32[]{:S(2)}, u32[]{:S(2)}) collective-permute-start(bf16[32,512]{1,0:T(8,128)(2,1)S(1)} %get-tuple-element.44), channel_id=1, source_target_pairs={{0,1},{1,2},{2,3},{3,0},{4,5},{5,6},{6,7},{7,4},{8,9},{9,10},{10,1... | collective-permute-start | bytes 98312 | tf_op jit(solution)/shard_map/ppermute | solution.py:23
  12.3 4.9 %collective-permute-start.4 = (bf16[32,512]{1,0:T(8,128)(2,1)S(1)}, bf16[32,512]{1,0:T(8,128)(2,1)S(1)}, u32[]{:S(2)}, u32[]{:S(2)}) collective-permute-start(bf16[32,512]{1,0:T(8,128)(2,1)S(1)} %get-tuple-element.45), channel_id=1, source_target_pairs={{0,2},{1,3},{2,0},{3,1},{4,6},{5,7},{6,4},{7,5},{8,10},{9,11},{10,... | collective-permute-start | bytes 98312 | tf_op jit(solution)/shard_map/ppermute | solution.py:23
  15.5 2.8 %collective-permute-start.5 = (bf16[32,512]{1,0:T(8,128)(2,1)S(1)}, bf16[32,512]{1,0:T(8,128)(2,1)S(1)}, u32[]{:S(2)}, u32[]{:S(2)}) collective-permute-start(bf16[32,512]{1,0:T(8,128)(2,1)S(1)} %get-tuple-element.46), channel_id=1, source_target_pairs={{0,3},{1,0},{2,1},{3,2},{4,7},{5,4},{6,5},{7,6},{8,11},{9,8},{10,9... | collective-permute-start | bytes 98312 | tf_op jit(solution)/shard_map/ppermute | solution.py:23
  46.3 6.1 %collective-permute-start.6 = (bf16[128,768]{1,0:T(8,128)(2,1)S(1)}, bf16[128,768]{1,0:T(8,128)(2,1)S(1)}, u32[]{:S(2)}, u32[]{:S(2)}) collective-permute-start(bf16[128,768]{1,0:T(8,128)(2,1)S(1)} %bitcast.26), channel_id=1, source_target_pairs={{0,3},{1,0},{2,1},{3,2},{4,7},{5,4},{6,5},{7,6},{8,11},{9,8},{10,9... | collective-permute-start | bytes 589832 | tf_op jit(solution)/shard_map/ppermute | solution.py:23
  47.4 18.6 %collective-permute-start.12 = (bf16[256,512]{1,0:T(8,128)(2,1)S(1)}, bf16[256,512]{1,0:T(8,128)(2,1)S(1)}, u32[]{:S(2)}, u32[]{:S(2)}) collective-permute-start(bf16[256,512]{1,0:T(8,128)(2,1)S(1)} %get-tuple-element.63), channel_id=1, source_target_pairs={{0,1},{1,2},{2,3},{3,0},{4,5},{5,6},{6,7},{7,4},{8,9},{9,10},{10,1... | collective-permute-start | bytes 786440 | tf_op jit(solution)/shard_map/ppermute | solution.py:23
  47.8 13.2 %collective-permute-start.8 = (bf16[128,768]{1,0:T(8,128)(2,1)S(1)}, bf16[128,768]{1,0:T(8,128)(2,1)S(1)}, u32[]{:S(2)}, u32[]{:S(2)}) collective-permute-start(bf16[128,768]{1,0:T(8,128)(2,1)S(1)} %bitcast.27), channel_id=1, source_target_pairs={{0,1},{1,2},{2,3},{3,0},{4,5},{5,6},{6,7},{7,4},{8,9},{9,10},{10,1... | collective-permute-start | bytes 589832 | tf_op jit(solution)/shard_map/ppermute | solution.py:23
  47.9 15.4 %collective-permute-start.7 = (bf16[128,768]{1,0:T(8,128)(2,1)S(1)}, bf16[128,768]{1,0:T(8,128)(2,1)S(1)}, u32[]{:S(2)}, u32[]{:S(2)}) collective-permute-start(bf16[128,768]{1,0:T(8,128)(2,1)S(1)} %bitcast.28), channel_id=1, source_target_pairs={{0,2},{1,3},{2,0},{3,1},{4,6},{5,7},{6,4},{7,5},{8,10},{9,11},{10,... | collective-permute-start | bytes 589832 | tf_op jit(solution)/shard_map/ppermute | solution.py:23
  51.3 17.6 %collective-permute-start.13 = (bf16[256,512]{1,0:T(8,128)(2,1)S(1)}, bf16[256,512]{1,0:T(8,128)(2,1)S(1)}, u32[]{:S(2)}, u32[]{:S(2)}) collective-permute-start(bf16[256,512]{1,0:T(8,128)(2,1)S(1)} %get-tuple-element.64), channel_id=1, source_target_pairs={{0,2},{1,3},{2,0},{3,1},{4,6},{5,7},{6,4},{7,5},{8,10},{9,11},{10,... | collective-permute-start | bytes 786440 | tf_op jit(solution)/shard_map/ppermute | solution.py:23
  52.4 10.8 %copy-start.1 = (bf16[1,2048,256]{2,1,0:T(8,128)(2,1)S(1)}, bf16[1,2048,256]{2,1,0:T(8,128)(2,1)}, u32[]{:S(2)}) copy-start(bf16[1,2048,256]{2,1,0:T(8,128)(2,1)} %param.45) | copy-start | bytes 3145732
  52.4 10.8 %copy-start.2 = (bf16[1,2048,256]{2,1,0:T(8,128)(2,1)S(1)}, bf16[1,2048,256]{2,1,0:T(8,128)(2,1)}, u32[]{:S(2)}) copy-start(bf16[1,2048,256]{2,1,0:T(8,128)(2,1)} %param.46) | copy-start | bytes 3145732
  52.4 10.8 %copy-start.13 = (f32[2048]{0:T(1024)S(1)}, f32[2048]{0:T(1024)}, u32[]{:S(2)}) copy-start(f32[2048]{0:T(1024)} %param.42) | copy-start | bytes 24580
  52.4 16.4 %collective-permute-start.14 = (bf16[256,512]{1,0:T(8,128)(2,1)S(1)}, bf16[256,512]{1,0:T(8,128)(2,1)S(1)}, u32[]{:S(2)}, u32[]{:S(2)}) collective-permute-start(bf16[256,512]{1,0:T(8,128)(2,1)S(1)} %get-tuple-element.65), channel_id=1, source_target_pairs={{0,3},{1,0},{2,1},{3,2},{4,7},{5,4},{6,5},{7,6},{8,11},{9,8},{10,9... | collective-permute-start | bytes 786440 | tf_op jit(solution)/shard_map/ppermute | solution.py:23
  59.4 13.5 %copy-start.3 = (bf16[1,256,2048]{2,1,0:T(8,128)(2,1)S(1)}, bf16[1,256,2048]{2,1,0:T(8,128)(2,1)}, u32[]{:S(2)}) copy-start(bf16[1,256,2048]{2,1,0:T(8,128)(2,1)} %param.47) | copy-start | bytes 3145732
  64.1 5.8 %collective-permute-start.11 = (bf16[192,256]{1,0:T(8,128)(2,1)S(1)}, bf16[192,256]{1,0:T(8,128)(2,1)S(1)}, u32[]{:S(2)}, u32[]{:S(2)}) collective-permute-start(bf16[192,256]{1,0:T(8,128)(2,1)S(1)} %shard_map.245.a0), channel_id=1, source_target_pairs={{0,3},{1,0},{2,1},{3,2},{4,7},{5,4},{6,5},{7,6},{8,11},{9,8},{10,9... | collective-permute-start | bytes 294920 | tf_op jit(solution)/shard_map/ppermute | solution.py:23
  64.2 6.8 %collective-permute-start.10 = (bf16[192,256]{1,0:T(8,128)(2,1)S(1)}, bf16[192,256]{1,0:T(8,128)(2,1)S(1)}, u32[]{:S(2)}, u32[]{:S(2)}) collective-permute-start(bf16[192,256]{1,0:T(8,128)(2,1)S(1)} %shard_map.245.a0), channel_id=1, source_target_pairs={{0,2},{1,3},{2,0},{3,1},{4,6},{5,7},{6,4},{7,5},{8,10},{9,11},{10,... | collective-permute-start | bytes 294920 | tf_op jit(solution)/shard_map/ppermute | solution.py:23
  66.0 7.0 %collective-permute-start.9 = (bf16[192,256]{1,0:T(8,128)(2,1)S(1)}, bf16[192,256]{1,0:T(8,128)(2,1)S(1)}, u32[]{:S(2)}, u32[]{:S(2)}) collective-permute-start(bf16[192,256]{1,0:T(8,128)(2,1)S(1)} %shard_map.245.a0), channel_id=1, source_target_pairs={{0,1},{1,2},{2,3},{3,0},{4,5},{5,6},{6,7},{7,4},{8,9},{9,10},{10,1... | collective-permute-start | bytes 294920 | tf_op jit(solution)/shard_map/ppermute | solution.py:23
  (3 other events, 24.4 us)
